TPU v7x, 32 devices: a whole 2x2x4 slice. The times are simulated.
32 devices in a mesh: dp: 2 (over x), kv: 8 (over z, y), tp: 2 (over core).
Axes of the slice: x: 2, y: 2, z: 4, core: 2. Of those that a mesh axis runs over, the one named last changes fastest.
Arguments:
- tokens: bfloat16 [48, 2048], P('dp', ('kv', 'tp')), may hold values from -21 to 21
- state: float32 [48, 8, 128, 128], P(('dp', 'kv'), 'tp'), may hold values from -3 to 3
- mix_gain: bfloat16 [2048], P(('kv', 'tp')), may hold values from 0.099609375 to 1.8984375
- w_query: bfloat16 [2048, 1024], P('kv', 'tp'), may hold values from -0.125 to 0.125
- w_key: bfloat16 [2048, 1024], P('kv', 'tp'), may hold values from -0.125 to 0.125
- w_value: bfloat16 [2048, 1024], P('kv', 'tp'), may hold values from -0.125 to 0.125
- w_beta: bfloat16 [2048, 8], P('kv', 'tp'), may hold values from -0.125 to 0.125
- w_decay: bfloat16 [2048, 8], P('kv', 'tp'), may hold values from -0.125 to 0.125
- decay_log: float32 [8], P('tp'), may hold values from -1.5 to 1
- head_gain: bfloat16 [128], replicated, may hold values from 0.099609375 to 1.8984375
- w_out: bfloat16 [1024, 2048], P('tp', 'kv'), may hold values from -0.1875 to 0.1875
- ff_gain: bfloat16 [2048], P(('kv', 'tp')), may hold values from 0.099609375 to 1.8984375
- w_up: bfloat16 [2048, 8192], P(None, ('kv', 'tp')), may hold values from -0.125 to 0.125
- w_down: bfloat16 [8192, 2048], P(('kv', 'tp')), may hold values from -0.09375 to 0.09375
Outputs:
- output: bfloat16 [48, 2048], P('dp', ('kv', 'tp'))
- new_state: float32 [48, 8, 128, 128], P(('dp', 'kv'), 'tp')
All inputs are finite; a program needn't handle non-finite values.
Results may differ from a plain program's by a relative error of at most 0.013.
Values may be sent and summed in bfloat16 or wider, within the bound.
No kernel may reach another device: no remote copies, remote signals or barrier semaphores. Data moves between devices by JAX's collectives and lax.ppermute only.
A program may use at most 64 MiB of HBM per device.

v0:
```python
import jax
import jax.numpy as jnp
from jax import lax
from jax.sharding import PartitionSpec as P

D = 2048


def local(
    tokens,
    state,
    mix_gain,
    w_query,
    w_key,
    w_value,
    w_beta,
    w_decay,
    decay_log,
    head_gain,
    w_out,
    ff_gain,
    w_up,
    w_down,
):
    seq_count = state.shape[0]
    heads_local = state.shape[1]
    head_size = state.shape[2]
    tokens_wide, gain_wide = (
        lax.all_gather(tokens, "tp", axis=1, tiled=True),
        lax.all_gather(mix_gain[None, :], "tp", axis=1, tiled=True),
    )
    wide_float = tokens_wide.astype(jnp.float32)
    scaled = (wide_float * gain_wide.astype(jnp.float32)).astype(jnp.bfloat16)
    query_part = jnp.dot(scaled, w_query, preferred_element_type=jnp.float32)
    key_part = jnp.dot(scaled, w_key, preferred_element_type=jnp.float32)
    value_part = jnp.dot(scaled, w_value, preferred_element_type=jnp.float32)
    gate_part = jnp.concatenate(
        [
            jnp.dot(scaled, w_beta, preferred_element_type=jnp.float32),
            jnp.dot(scaled, w_decay, preferred_element_type=jnp.float32),
        ],
        axis=1,
    )
    square_part = jnp.sum(wide_float * wide_float, axis=1)
    query_sum, key_sum, value_sum, gate_sum, square_sum = (
        lax.psum_scatter(query_part, "kv", scatter_dimension=0, tiled=True),
        lax.psum_scatter(key_part, "kv", scatter_dimension=0, tiled=True),
        lax.psum_scatter(value_part, "kv", scatter_dimension=0, tiled=True),
        lax.psum_scatter(gate_part, "kv", scatter_dimension=0, tiled=True),
        lax.psum_scatter(square_part, "kv", scatter_dimension=0, tiled=True),
    )
    inverse = lax.rsqrt(square_sum / D + 1e-06)[:, None]
    query = (inverse * query_sum).reshape(seq_count, heads_local, head_size)
    key_rows = (inverse * key_sum).reshape(seq_count, heads_local, head_size)
    value = (inverse * value_sum).reshape(seq_count, heads_local, head_size)
    gates = inverse * gate_sum
    beta = jax.nn.sigmoid(gates[:, :heads_local])
    decay = -jnp.exp(decay_log)[None, :] * jax.nn.softplus(gates[:, heads_local:])
    qnorm = query * lax.rsqrt(jnp.sum(query * query, axis=-1, keepdims=True) + 1e-06)
    knorm = key_rows * lax.rsqrt(jnp.sum(key_rows * key_rows, axis=-1, keepdims=True) + 1e-06)
    kept = state * jnp.exp(decay)[:, :, None, None]
    predicted = jnp.sum(kept * knorm[:, :, :, None], axis=2)
    new_state = (
        kept + (beta[:, :, None] * knorm)[:, :, :, None] * (value - predicted)[:, :, None, :]
    )
    heads = jnp.sum(new_state * qnorm[:, :, :, None], axis=2) / jnp.sqrt(jnp.float32(head_size))
    normed = (
        heads
        * lax.rsqrt(jnp.mean(heads * heads, axis=-1, keepdims=True) + 1e-06)
        * head_gain.astype(jnp.float32)
    )
    normed = normed.astype(jnp.bfloat16).reshape(seq_count, heads_local * head_size)
    partial_mix = jnp.dot(
        lax.all_gather(normed, "kv", axis=0, tiled=True), w_out, preferred_element_type=jnp.float32
    )
    mixed = lax.psum_scatter(
        partial_mix.astype(jnp.bfloat16), "tp", scatter_dimension=1, tiled=True
    ).astype(jnp.float32)
    resid = (tokens.astype(jnp.float32) + mixed).astype(jnp.bfloat16)
    resid_float = resid.astype(jnp.float32)
    whole_rows = lax.all_gather(resid, ("kv", "tp"), axis=1, tiled=True)
    whole_gain = lax.all_gather(ff_gain[None, :], ("kv", "tp"), axis=1, tiled=True)
    whole_float = whole_rows.astype(jnp.float32)
    inverse2 = lax.rsqrt(jnp.mean(whole_float * whole_float, axis=1, keepdims=True) + 1e-06)
    scaled2 = (whole_float * whole_gain.astype(jnp.float32)).astype(jnp.bfloat16)
    up_rows = jnp.dot(scaled2, w_up, preferred_element_type=jnp.float32) * inverse2
    act = jnp.square(jax.nn.relu(up_rows)).astype(jnp.bfloat16)
    summed = lax.psum_scatter(
        lax.dot_general(w_down, act, (((0,), (1,)), ((), ())), preferred_element_type=jnp.float32),
        ("kv", "tp"),
        scatter_dimension=0,
        tiled=True,
    )
    results = (resid_float + summed.T).astype(jnp.bfloat16)
    return (results, new_state)


def solution(mesh):
    placed = (
        P("dp", ("kv", "tp")),
        P(("dp", "kv"), "tp", None, None),
        P(("kv", "tp")),
        P("kv", "tp"),
        P("kv", "tp"),
        P("kv", "tp"),
        P("kv", "tp"),
        P("kv", "tp"),
        P("tp"),
        P(),
        P("tp", "kv"),
        P(("kv", "tp")),
        P(None, ("kv", "tp")),
        P(("kv", "tp"), None),
    )
    return jax.shard_map(
        local,
        mesh=mesh,
        in_specs=placed,
        out_specs=(P("dp", ("kv", "tp")), P(("dp", "kv"), "tp", None, None)),
        check_vma=False,
    )
```

profile of v0, /device:TPU:0, one launch (start us, length us, event | category | flops | bytes accessed | tf_op | source)
XLA Modules:
  0.0 233.0 jit_solution(6209342007660774955)
XLA Ops:
  7.2 0.0 copy-start
  7.2 0.0 copy-start.1
  7.2 0.0 copy-start.2
  7.2 0.0 all-reduce.8.cloned.1.call-start
  7.2 2.2 all-gather.2
  9.5 2.0 all_gather.15
  11.5 0.6 fusion.9
  12.2 0.8 fusion.21
  13.0 0.8 fusion.23
  13.8 1.7 fusion.19
  15.5 0.0 copy-start.4
  15.5 0.0 copy-start.3
  15.5 1.7 fusion.17
  17.3 1.7 fusion.15
  19.0 0.6 pad_maximum_fusion
  19.6 0.0 all-reduce.8.cloned.1.call-update
  19.6 0.0 reduce-scatter.8.cloned.1.call-start
  19.7 0.7 convert_element_type.45
  20.3 1.2 dynamic-slice
  22.1 0.7 exponential_negate_fusion
  22.7 70.8 %all-reduce.8.cloned.1.call-done = (f32[24,512]{1,0:T(8,128)}, f32[24]{0:T(128)}, f32[24,512]{1,0:T(8,128)}, f32[24,8]{0,1:T(8,128)}, f32[24,512]{1,0:T(8,128)}) async-done(((f32[24,512]{1,0:T(8,128)}, f32[24]{0:T(128)}, f32[24,512]{1,0:T(8,128)}, f32[24,8]{0,1:T(8,128)}, f32[24,512]{1,0:T(8,128)}), (f32[24,512]{1,0:T(8,128)}, f32[24]{0:T(128)}, f32[24,512]{1,0:T(8,128)}, f32[24,8]{0,1:T(8,128)}, ...) | async-done | bytes 148336
  93.5 0.7 fusion.29
  94.3 0.8 dynamic-slice_multiply_fusion.3
  95.0 0.1 fusion.27
  95.1 0.1 copy.20
  95.2 0.9 dynamic-slice_multiply_fusion.2
  96.1 0.1 multiply_reduce_fusion.4
  96.2 0.1 copy.21
  96.3 0.1 multiply_reduce_fusion.3
  96.4 0.1 broadcast_multiply_fusion.2
  96.5 1.4 multiply_reduce_fusion.1
  98.0 0.0 copy-done.1
  98.0 1.4 multiply_reduce_fusion
  99.3 0.1 multiply_reduce_fusion.2
  99.4 0.1 multiply_bitcast_fusion
  99.5 30.6 %all-gather.3 = bf16[8,3,512]{2,1,0:T(4,128)(2,1)S(1)} all-gather(bf16[1,3,512]{2,1,0:T(4,128)(2,1)S(1)} %fusion.25), channel_id=1, replica_groups=mesh['dp'=2,'kv'=8,'tp'=2] {'kv'}, dimensions={0}, use_global_device_ids=true | all-gather | bytes 27648 | tf_op jit(solution)/shard_map/all_gather | solution.py:74
  130.1 0.0 copy-done.2
  130.2 0.2 convolution_convert_fusion
  130.3 0.7 copy.24
  131.0 0.0 reduce-scatter.8.cloned.1.call-update
  131.1 0.0 reduce-scatter.6.cloned.1.call-start
  131.1 0.0 copy-done.4
  131.1 20.4 %all-gather.4 = bf16[16,1,128]{2,1,0:T(2,128)(2,1)S(1)} all-gather(bf16[1,1,128]{2,1,0:T(2,128)(2,1)S(1)} %bitcast.44), channel_id=3, replica_groups=mesh['dp'=2,'kv'=8,'tp'=2] {'kv','tp'}, dimensions={0}, use_global_device_ids=true | all-gather | bytes 4352 | tf_op jit(solution)/shard_map/all_gather | solution.py:82
  151.5 0.0 reduce-scatter.8.cloned.1.call-done
  151.6 0.8 copy.25
  152.4 0.0 copy-done.3
  152.4 17.7 %all_gather.18 = bf16[24,2048]{1,0:T(8,128)(2,1)S(1)} all-gather(bf16[24,128]{1,0:T(8,128)(2,1)S(1)} %add_convert_fusion), channel_id=1, replica_groups=mesh['dp'=2,'kv'=8,'tp'=2] {'kv','tp'}, dimensions={1}, use_global_device_ids=true | all-gather | bytes 104448 | tf_op jit(solution)/shard_map/all_gather | solution.py:81
  170.1 0.1 fusion.4
  170.3 0.0 copy-done
  170.3 3.0 %convolution_bitcast_fusion = f32[2048,24]{0,1:T(8,128)} fusion(bf16[512,2048]{1,0:T(8,128)(2,1)S(1)} %copy-done, bf16[2048,512]{1,0:T(8,128)(2,1)} %param.26, bf16[24,2048]{1,0:T(8,128)(2,1)S(1)} %all_gather.18, f32[2048]{0:T(1024)S(1)} %bitcast.37, f32[24]{0:T(128)S(1)} %add_rsqrt_fusion.2), kind=kOutput, calls=%fused_computation | convolution fusion | flops 100859904 | bytes 4497504 | tf_op jit(solution)/shard_map/dot_general | solution.py:89
  173.3 0.0 reduce-scatter.6.cloned.1.call-update
  173.3 51.8 %reduce-scatter.6.cloned.1.call-done = f32[128,24]{0,1:T(8,128)} async-done(((f32[2048,24]{0,1:T(8,128)}), f32[128,24]{0,1:T(8,128)}) %reduce-scatter.6.cloned.1.call-update) | async-done | bytes 12304 | tf_op jit(solution)/shard_map/reduce_scatter | solution.py:88
  225.1 1.3 fusion.13
  (14 shorter events, 0.2 us)
Async XLA Ops:
  7.2 163.1 %copy-start = (bf16[512,2048]{1,0:T(8,128)(2,1)S(1)}, bf16[512,2048]{1,0:T(8,128)(2,1)}, u32[]{:S(2)}) copy-start(bf16[512,2048]{1,0:T(8,128)(2,1)} %param.27) | copy-start | bytes 6291460
  7.2 90.8 %copy-start.1 = (f32[3,4,128,128]{3,2,1,0:T(8,128)S(1)}, f32[3,4,128,128]{3,2,1,0:T(8,128)}, u32[]{:S(2)}) copy-start(f32[3,4,128,128]{3,2,1,0:T(8,128)} %param.15) | copy-start | bytes 2359300
  7.2 123.0 %copy-start.2 = (bf16[512,256]{1,0:T(8,128)(2,1)S(1)}, bf16[512,256]{1,0:T(8,128)(2,1)}, u32[]{:S(2)}) copy-start(bf16[512,256]{1,0:T(8,128)(2,1)} %param.24) | copy-start | bytes 786436
  7.2 86.3 %all-reduce.8.cloned.1.call-start = ((), (), s32[]{:S(2)}) async-start(), calls=%async_computation.4 | async-start | bytes 304128
  15.5 115.6 %copy-start.4 = (bf16[128]{0:T(256)(128)(2,1)S(1)}, bf16[128]{0:T(256)(128)(2,1)}, u32[]{:S(2)}) copy-start(bf16[128]{0:T(256)(128)(2,1)} %param.25) | copy-start | bytes 772
  15.5 136.9 %copy-start.3 = (bf16[24,128]{1,0:T(8,128)(2,1)S(1)}, bf16[24,128]{1,0:T(8,128)(2,1)}, u32[]{:S(2)}) copy-start(bf16[24,128]{1,0:T(8,128)(2,1)} %param.14) | copy-start | bytes 18436
  19.6 132.0 %reduce-scatter.8.cloned.1.call-start = ((), (), s32[]{:S(2)}) async-start(), calls=%async_computation.3 | async-start | bytes 98304
  131.1 94.1 %reduce-scatter.6.cloned.1.call-start = ((), (), s32[]{:S(2)}) async-start(), calls=%async_computation.2 | async-start | bytes 208896 | tf_op jit(solution)/shard_map/reduce_scatter | solution.py:88
Sparse Core Ops, SparseCore 0:
  19.7 73.7 all-reduce.7
  131.2 7.4 reduce-scatter.7
  173.4 51.6 reduce-scatter.5
where the time goes:
time: 234 us; the launch traced here: 233 us
  waiting for transfers between devices  123 us (53%)
  blocking collectives  73 us (31%)
  between operations  14.4 us (6%)
  matrix products  9.96 us (4%)
  other arithmetic  9.74 us (4%)
  local copies, waits for them, and re-layouts  3.05 us (1%)
    unnamed x5, waiting for transfers between devices  70.9 us
    reduce_scatter x1, waiting for transfers between devices, local(): lax.psum_scatter(lax.dot_general(w_down, act, (((0,), (1,)), ((), ())), p...  51.8 us
    all_gather x1, blocking collectives, local(): lax.all_gather(normed, 'kv', axis=0, tiled=True)  30.6 us
    all_gather x1, blocking collectives, local(): lax.all_gather(ff_gain[None, :], ('kv', 'tp'), axis=1, tiled=True)  20.4 us
    all_gather x1, blocking collectives, local(): whole_rows = lax.all_gather(resid, ('kv', 'tp'), axis=1, tiled=True)  17.7 us
  transfers between devices with their start and end apart: 3, of which 2 were waited for; matrix products, arithmetic and copies ran while one was open for 1% of the time, Pallas kernels for 0%

commit v1 on v0

v1 whole, which is shorter than its diff:
```python
import functools

import jax
import jax.numpy as jnp
from jax import lax
from jax.sharding import PartitionSpec as P

BF = jnp.bfloat16
F32 = jnp.float32


def split_pair(value):
    high = value.astype(BF)
    low = (value - lax.reduce_precision(value, 8, 7)).astype(BF)
    return high, low


def local(
    tokens,
    state,
    mix_gain,
    w_query,
    w_key,
    w_value,
    w_beta,
    w_decay,
    decay_log,
    head_gain,
    w_out,
    ff_gain,
    w_up,
    w_down,
    n_kv,
    n_tp,
):
    rows, width = tokens.shape
    seq, heads, size = state.shape[:3]
    n_all = n_kv * n_tp
    model = width * n_all
    keys = heads * size

    packed = jnp.concatenate([tokens, mix_gain[None, :]], axis=0)
    wide = lax.all_gather(packed, "tp", axis=1, tiled=True)
    tp_at = lax.axis_index("tp")
    out_cols = []
    for step in range(n_tp):
        target = (tp_at + step) % n_tp
        block = lax.dynamic_slice_in_dim(w_out, target * width, width, axis=1)
        if step:
            block = lax.ppermute(block, "tp", [(i, (i + step) % n_tp) for i in range(n_tp)])
        out_cols.append(block)

    wide_float = wide[:rows].astype(F32)
    scaled = (wide_float * wide[rows:].astype(F32)).astype(BF)
    dot = functools.partial(jnp.dot, preferred_element_type=F32)
    gates_part = dot(scaled, jnp.concatenate([w_beta, w_decay], axis=1))
    square_part = jnp.sum(wide_float * wide_float, axis=1, keepdims=True)
    small = jnp.concatenate([gates_part, square_part], axis=1)
    high, low = split_pair(small)
    n_small = small.shape[1]
    pad = jnp.zeros((rows, size - 2 * n_small), BF)
    sent = jnp.concatenate(
        [
            dot(scaled, w_query).astype(BF),
            dot(scaled, w_key).astype(BF),
            dot(scaled, w_value).astype(BF),
            high,
            low,
            pad,
        ],
        axis=1,
    ).reshape(n_kv, seq, 3 * keys + size)
    got = lax.all_to_all(sent, "kv", 0, 0, tiled=False)
    total = jnp.sum(got.astype(F32), axis=0)
    small = total[:, 3 * keys : 3 * keys + n_small] + total[:, 3 * keys + n_small : 3 * keys + 2 * n_small]
    inverse = lax.rsqrt(small[:, 2 * heads :] / model + 1e-06)
    query = (inverse * total[:, :keys]).reshape(seq, heads, size)
    key_rows = (inverse * total[:, keys : 2 * keys]).reshape(seq, heads, size)
    value = (inverse * total[:, 2 * keys : 3 * keys]).reshape(seq, heads, size)
    beta = jax.nn.sigmoid(inverse * small[:, :heads])
    decay = -jnp.exp(decay_log)[None, :] * jax.nn.softplus(inverse * small[:, heads : 2 * heads])
    qnorm = query * lax.rsqrt(jnp.sum(query * query, axis=-1, keepdims=True) + 1e-06)
    knorm = key_rows * lax.rsqrt(jnp.sum(key_rows * key_rows, axis=-1, keepdims=True) + 1e-06)
    kept = state * jnp.exp(decay)[:, :, None, None]
    predicted = jnp.sum(kept * knorm[:, :, :, None], axis=2)
    new_state = kept + (beta[:, :, None] * knorm)[:, :, :, None] * (value - predicted)[:, :, None, :]
    read = jnp.sum(new_state * qnorm[:, :, :, None], axis=2) / jnp.sqrt(jnp.float32(size))
    normed = (
        read
        * lax.rsqrt(jnp.mean(read * read, axis=-1, keepdims=True) + 1e-06)
        * head_gain.astype(F32)
    )
    normed = normed.astype(BF).reshape(seq, keys)
    axes = ("kv", "tp")
    spread = lax.all_to_all(jnp.broadcast_to(normed[None], (n_all, seq, keys)), axes, 0, 0, tiled=False)
    spread = spread.reshape(n_kv, n_tp, seq, keys)
    mixed = 0.0
    for step in range(n_tp):
        heads_of = lax.dynamic_index_in_dim(spread, (tp_at - step) % n_tp, 1, keepdims=False)
        part = dot(heads_of.reshape(rows, keys), out_cols[step])
        mixed = mixed + lax.reduce_precision(part, 8, 7)
    resid = (tokens.astype(F32) + mixed).astype(BF)
    resid_float = resid.astype(F32)
    scaled2 = (resid_float * ff_gain.astype(F32)[None, :]).astype(BF)
    high, low = split_pair(jnp.sum(resid_float * resid_float, axis=1))
    tail_rows = -(-2 * rows // width // 8) * 8
    tail = jnp.concatenate([high, low, jnp.zeros((tail_rows * width - 2 * rows,), BF)])
    tail = tail.reshape(tail_rows, width)
    sent2 = jnp.concatenate([scaled2, tail], axis=0)
    got2 = lax.all_to_all(jnp.broadcast_to(sent2[None], (n_all,) + sent2.shape), axes, 0, 0, tiled=False)
    sums = jnp.sum(got2[:, rows:].reshape(n_all, tail_rows * width)[:, : 2 * rows].astype(F32), axis=0)
    inverse2 = lax.rsqrt((sums[:rows] + sums[rows:]) / model + 1e-06)[:, None]
    whole = got2[:, :rows].transpose(1, 0, 2).reshape(rows, model)
    up_rows = dot(whole, w_up) * inverse2
    act = jnp.square(jax.nn.relu(up_rows)).astype(BF)
    down = dot(act, w_down).astype(BF).reshape(rows, n_all, width).transpose(1, 0, 2)
    got3 = lax.all_to_all(down, axes, 0, 0, tiled=False)
    output = (resid_float + jnp.sum(got3.astype(F32), axis=0)).astype(BF)
    return (output, new_state)


def solution(mesh):
    placed = (
        P("dp", ("kv", "tp")),
        P(("dp", "kv"), "tp", None, None),
        P(("kv", "tp")),
        P("kv", "tp"),
        P("kv", "tp"),
        P("kv", "tp"),
        P("kv", "tp"),
        P("kv", "tp"),
        P("tp"),
        P(),
        P("tp", "kv"),
        P(("kv", "tp")),
        P(None, ("kv", "tp")),
        P(("kv", "tp"), None),
    )
    return jax.shard_map(
        functools.partial(local, n_kv=mesh.shape["kv"], n_tp=mesh.shape["tp"]),
        mesh=mesh,
        in_specs=placed,
        out_specs=(P("dp", ("kv", "tp")), P(("dp", "kv"), "tp", None, None)),
        check_vma=False,
    )
```

time: 234 us -> 62.4 us (0.27)
  waiting for transfers between devices: 123 us -> 12.3 us
  blocking collectives: 73 us -> 22.6 us
  between operations: 14.4 us -> 0.78 us
  starting transfers between devices: 0.12 us -> 11 us
  other arithmetic: 9.74 us -> 5.89 us
  matrix products: 9.96 us -> 6.93 us
    unnamed x5 -> x0, waiting for transfers between devices: 70.9 us -> none
    all_gather x5 -> x1, blocking collectives: 73 us -> 2.11 us  [local(): wide = lax.all_gather(packed, 'tp', axis=1, tiled=True)]
    reduce_scatter x1 -> x0, waiting for transfers between devices: 51.8 us -> none  [local(): lax.psum_scatter(lax.dot_general(w_down, act, (((0,), (1,)), ((), ())), p...]
    all_to_all x0 -> x2, blocking collectives: none -> 20.5 us  [the longest x1 10.5 us: local(): lax.all_to_all(jnp.broadcast_to(sent2[None], (n_all,) + sent2.shape), axe...]
    all_to_all x0 -> x2, waiting for transfers between devices: none -> 12.3 us  [the longest x1 6.46 us: local(): lax.all_to_all(jnp.broadcast_to(normed[None], (n_all, seq, keys)), axes,...]
    all_to_all x0 -> x2, starting transfers between devices: none -> 10.7 us  [the longest x1 7.16 us: local(): got = lax.all_to_all(sent, 'kv', 0, 0, tiled=False)]
    dot_general x7, matrix products: 9.96 us -> 6.93 us  [the longest x1 2.35 us: local(): dot(act, w_down).astype(BF).reshape(rows, n_all, width).transpose(1, 0, 2)]
    unnamed x14 -> x13, local copies, waits for them, and re-layouts: 2.81 us -> 0.23 us
  transfers between devices with their start and end apart: 3 -> 3, of which waited for: 2 -> 2; matrix products, arithmetic and copies ran while one was open for 1% -> 3% of each run, Pallas kernels for 0% -> 0%
where the time goes in v1:
time: 62.4 us; the launch traced here: 61.9 us
  blocking collectives  22.6 us (36%)
  waiting for transfers between devices  12.3 us (20%)
  starting transfers between devices  11 us (18%)
  matrix products  6.93 us (11%)
  other arithmetic  5.89 us (9%)
  local copies, waits for them, and re-layouts  2.36 us (4%)
  between operations  0.78 us (1%)
    all_to_all x1, blocking collectives, local(): lax.all_to_all(jnp.broadcast_to(sent2[None], (n_all,) + sent2.shape), axe...  10.5 us
    all_to_all x1, blocking collectives, local(): got3 = lax.all_to_all(down, axes, 0, 0, tiled=False)  9.96 us
    all_to_all x1, starting transfers between devices, local(): got = lax.all_to_all(sent, 'kv', 0, 0, tiled=False)  7.16 us
    all_to_all x1, waiting for transfers between devices, local(): lax.all_to_all(jnp.broadcast_to(normed[None], (n_all, seq, keys)), axes,...  6.46 us
    all_to_all x1, waiting for transfers between devices, local(): got = lax.all_to_all(sent, 'kv', 0, 0, tiled=False)  5.86 us
    all_to_all x1, starting transfers between devices, local(): lax.all_to_all(jnp.broadcast_to(normed[None], (n_all, seq, keys)), axes,...  3.5 us
    dot_general x1, matrix products, local(): dot(act, w_down).astype(BF).reshape(rows, n_all, width).transpose(1, 0, 2)  2.35 us
    all_gather x1, blocking collectives, local(): wide = lax.all_gather(packed, 'tp', axis=1, tiled=True)  2.11 us
  transfers between devices with their start and end apart: 3, of which 2 were waited for; matrix products, arithmetic and copies ran while one was open for 3% of the time, Pallas kernels for 0%

profile of v1, /device:TPU:0, one launch (start us, length us, event | category | flops | bytes accessed | tf_op | source)
XLA Modules:
  0.0 61.9 jit_solution(8024021234024849064)
XLA Ops:
  0.6 0.0 copy-start
  0.6 0.0 copy-start.1
  0.7 0.9 %pad_maximum_fusion.1 = bf16[25,128]{1,0:T(8,128)(2,1)S(1)} fusion(bf16[1,128]{1,0:T(2,128)(2,1)} %bitcast.53, bf16[24,128]{1,0:T(8,128)(2,1)} %param.14), kind=kLoop, calls=%fused_computation.43 | loop fusion | flops 12800 | bytes 12800 | tf_op jit(solution)/shard_map/concatenate | solution.py:42
  1.5 2.1 %all_gather.3 = bf16[25,256]{1,0:T(8,128)(2,1)S(1)} all-gather(bf16[25,128]{1,0:T(8,128)(2,1)S(1)} %pad_maximum_fusion.1), channel_id=1, replica_groups=mesh['dp'=2,'kv'=8,'tp'=2] {'tp'}, dimensions={1}, use_global_device_ids=true | all-gather | bytes 19200 | tf_op jit(solution)/shard_map/all_gather | solution.py:43
  3.6 0.1 fusion.14
  3.8 0.1 copy.84
  3.8 0.8 %fusion.19 = f32[24,8]{1,0:T(8,128)S(1)} fusion(bf16[256,4]{0,1:T(4,128)(2,1)} %param.21, bf16[256,4]{0,1:T(4,128)(2,1)} %param.20, f32[256]{0:T(256)S(1)} %bitcast.48, bf16[25,256]{1,0:T(8,128)(2,1)S(1)} %all_gather.3), kind=kOutput, calls=%fused_computation.51 | convolution fusion | flops 124928 | bytes 18176 | tf_op jit(solution)/shard_map/dot_general | solution.py:56
  4.7 0.1 fusion.17
  4.8 0.1 fusion.23
  4.8 1.1 %convolution_convert_fusion.2 = bf16[24,512]{1,0:T(8,128)(2,1)S(1)} fusion(bf16[256,512]{1,0:T(8,128)(2,1)} %param.18, f32[256]{0:T(256)S(1)} %bitcast.49, bf16[25,256]{1,0:T(8,128)(2,1)S(1)} %all_gather.3), kind=kOutput, calls=%fused_computation.6 | convolution fusion | flops 6322176 | bytes 300032 | tf_op jit(solution)/shard_map/dot_general | solution.py:65
  5.9 0.0 copy-start.2
  5.9 1.1 %convolution_convert_fusion.1 = bf16[24,512]{1,0:T(8,128)(2,1)S(1)} fusion(bf16[256,512]{1,0:T(8,128)(2,1)} %param.19, f32[256]{0:T(256)S(1)} %bitcast.50, bf16[25,256]{1,0:T(8,128)(2,1)S(1)} %all_gather.3), kind=kOutput, calls=%fused_computation.5 | convolution fusion | flops 6322176 | bytes 300032 | tf_op jit(solution)/shard_map/dot_general | solution.py:66
  7.1 0.0 copy-start.4
  7.1 1.1 %convolution_convert_fusion.3 = bf16[24,512]{1,0:T(8,128)(2,1)S(1)} fusion(bf16[256,512]{1,0:T(8,128)(2,1)} %param.17, f32[256]{0:T(256)S(1)} %bitcast.51, bf16[25,256]{1,0:T(8,128)(2,1)S(1)} %all_gather.3), kind=kOutput, calls=%fused_computation.7 | convolution fusion | flops 6322176 | bytes 300032 | tf_op jit(solution)/shard_map/dot_general | solution.py:64
  8.2 0.1 concatenate.21
  8.3 0.0 copy-start.3
  8.3 0.7 %reshape.114 = bf16[8,3,1664]{2,1,0:T(4,128)(2,1)} reshape(bf16[24,1664]{1,0:T(8,128)(2,1)S(1)} %concatenate.21) | data formatting | bytes 159744 | tf_op jit(solution)/shard_map/reshape | solution.py:72
  9.0 7.2 %all-to-all-start = ((bf16[8,3,1664]{2,1,0:T(4,128)(2,1)}), bf16[8,3,1664]{2,1,0:T(4,128)(2,1)S(1)}, u32[]{:S(2)}, u32[]{:S(2)}) async-start(bf16[8,3,1664]{2,1,0:T(4,128)(2,1)} %reshape.114), calls=%async_computation | async-start | bytes 212992 | tf_op jit(solution)/shard_map/all_to_all | solution.py:73
  16.2 0.7 %convert_element_type.80 = f32[128]{0:T(128)S(1)} convert(bf16[128]{0:T(256)(128)(2,1)} %param.23) | non-fusion elementwise | flops 128 | bytes 768 | tf_op jit(solution)/shard_map/convert_element_type | solution.py:91
  16.8 0.7 %exponential_negate_fusion = f32[4]{0:T(128)S(1)} fusion(f32[4]{0:T(128)} %param.22), kind=kLoop, calls=%fused_computation.77 | loop fusion | flops 4 | bytes 32 | tf_op jit(solution)/shard_map/neg | solution.py:81
  17.5 5.9 %all-to-all-done = bf16[8,3,1664]{2,1,0:T(4,128)(2,1)S(1)} async-done(((bf16[8,3,1664]{2,1,0:T(4,128)(2,1)}), bf16[8,3,1664]{2,1,0:T(4,128)(2,1)S(1)}, u32[]{:S(2)}, u32[]{:S(2)}) %all-to-all-start) | async-done | bytes 79904 | tf_op jit(solution)/shard_map/all_to_all | solution.py:73
  23.3 0.1 convert_reduce_fusion
  23.4 0.1 slice_add_fusion
  23.5 0.2 rsqrt_reduce_fusion
  23.7 0.1 slice_multiply_fusion.2
  23.8 0.1 fusion.25
  23.9 0.1 multiply_reduce_fusion.5
  24.0 0.1 copy.98
  24.1 0.1 copy.86
  24.2 0.1 multiply_reduce_fusion.4
  24.3 0.1 copy.99
  24.4 0.1 copy.88
  24.5 0.1 broadcast_multiply_fusion.2
  24.6 0.0 copy-done.1
  24.6 0.3 multiply_reduce_fusion.1
  24.9 1.4 %multiply_reduce_fusion = (f32[3,4,128]{2,1,0:T(4,128)S(1)}, f32[3,4,128,128]{3,2,1,0:T(8,128)}) fusion(f32[3,4,128]{2,1,0:T(4,128)S(1)} %get-tuple-element.18, f32[3,4,128]{2,1,0:T(4,128)S(1)} %sub.17, f32[3,4,128]{2,1,0:T(4,128)S(1)} %get-tuple-element.4, f32[3,4,128,128]{3,2,1,0:T(8,128)S(1)} %copy-done.1, f32[3,4]{1,0:T(4,128)S(1)} %get-tuple-element.13), kind=kLoop, calls=%fused_computation.15 | loop fusion | flops 981504 | bytes 1597488 | tf_op jit(solution)/shard_map/reduce_sum | solution.py:87
  26.2 0.1 multiply_reduce_fusion.3
  26.3 0.1 copy.89
  26.4 0.1 copy.90
  26.5 0.1 multiply_bitcast_fusion
  26.6 0.6 %broadcast_in_dim.15 = bf16[16,3,512]{2,1,0:T(4,128)(2,1)} broadcast(bf16[3,512]{1,0:T(4,128)(2,1)S(1)} %fusion.18), dimensions={1,2} | broadcast | bytes 52224 | tf_op jit(solution)/shard_map/broadcast_in_dim | solution.py:95
  27.3 3.5 %all-to-all-start.1 = ((bf16[16,3,512]{2,1,0:T(4,128)(2,1)}), bf16[16,3,512]{2,1,0:T(4,128)(2,1)S(1)}, u32[]{:S(2)}, u32[]{:S(2)}) async-start(bf16[16,3,512]{2,1,0:T(4,128)(2,1)} %broadcast_in_dim.15), calls=%async_computation.1 | async-start | bytes 131072 | tf_op jit(solution)/shard_map/all_to_all | solution.py:95
  30.8 0.0 copy-done.2
  30.8 0.4 collective-permute-start
  31.2 0.0 copy-done.4
  31.2 6.5 %all-to-all-done.1 = bf16[16,3,512]{2,1,0:T(4,128)(2,1)S(1)} async-done(((bf16[16,3,512]{2,1,0:T(4,128)(2,1)}), bf16[16,3,512]{2,1,0:T(4,128)(2,1)S(1)}, u32[]{:S(2)}, u32[]{:S(2)}) %all-to-all-start.1) | async-done | bytes 49184 | tf_op jit(solution)/shard_map/all_to_all | solution.py:95
  37.7 0.1 convolution_reduce-precision_fusion.1
  37.9 0.0 collective-permute-done
  37.9 0.0 copy-done.3
  37.9 0.2 multiply_convert_fusion
  38.2 0.1 maximum_bitcast_fusion
  38.3 10.5 %all_to_all.20 = bf16[16,32,128]{2,1,0:T(8,128)(2,1)S(1)} all-to-all(bf16[16,32,128]{2,1,0:T(8,128)(2,1)S(1)} %broadcast_in_dim.17), channel_id=1, replica_groups=mesh['dp'=2,'kv'=8,'tp'=2] {'kv','tp'}, dimensions={0} | all-to-all | bytes 262144 | tf_op jit(solution)/shard_map/all_to_all | solution.py:110
  48.8 0.1 add_rsqrt_fusion.2
  48.9 0.0 copy-done
  48.9 2.3 %fusion = bf16[3,16,8,128]{3,2,1,0:T(8,128)(2,1)S(1)} fusion(bf16[512,2048]{1,0:T(8,128)(2,1)S(1)} %copy-done, bf16[2048,512]{1,0:T(8,128)(2,1)} %param.26, f32[24]{0:T(128)S(1)} %add_rsqrt_fusion.2, bf16[16,32,128]{2,1,0:T(8,128)(2,1)S(1)} %all_to_all.20), kind=kOutput, calls=%fused_computation.1 | convolution fusion | flops 100761600 | bytes 4391424 | tf_op jit(solution)/shard_map/dot_general | solution.py:116
  51.3 10.0 %all_to_all.21 = bf16[16,24,128]{2,1,0:T(8,128)(2,1)S(1)} all-to-all(bf16[16,24,128]{2,1,0:T(8,128)(2,1)S(1)} %bitcast.44), channel_id=1, replica_groups=mesh['dp'=2,'kv'=8,'tp'=2] {'kv','tp'}, dimensions={0} | all-to-all | bytes 196608 | tf_op jit(solution)/shard_map/all_to_all | solution.py:117
  61.3 0.6 add_convert_fusion
  (25 shorter events, 0.3 us)
Async XLA Ops:
  0.6 48.3 %copy-start = (bf16[512,2048]{1,0:T(8,128)(2,1)S(1)}, bf16[512,2048]{1,0:T(8,128)(2,1)}, u32[]{:S(2)}) copy-start(bf16[512,2048]{1,0:T(8,128)(2,1)} %param.27) | copy-start | bytes 6291460
  0.6 23.9 %copy-start.1 = (f32[3,4,128,128]{3,2,1,0:T(8,128)S(1)}, f32[3,4,128,128]{3,2,1,0:T(8,128)}, u32[]{:S(2)}) copy-start(f32[3,4,128,128]{3,2,1,0:T(8,128)} %param.15) | copy-start | bytes 2359300
  5.9 24.9 %copy-start.2 = (bf16[512,256]{1,0:T(8,128)(2,1)S(1)}, bf16[512,256]{1,0:T(8,128)(2,1)}, u32[]{:S(2)}) copy-start(bf16[512,256]{1,0:T(8,128)(2,1)} %param.24) | copy-start | bytes 786436
  7.1 24.1 %copy-start.4 = (bf16[128]{0:T(256)(128)(2,1)S(1)}, bf16[128]{0:T(256)(128)(2,1)}, u32[]{:S(2)}) copy-start(bf16[128]{0:T(256)(128)(2,1)} %param.25) | copy-start | bytes 772
  8.3 29.6 %copy-start.3 = (bf16[24,128]{1,0:T(8,128)(2,1)S(1)}, bf16[24,128]{1,0:T(8,128)(2,1)}, u32[]{:S(2)}) copy-start(bf16[24,128]{1,0:T(8,128)(2,1)} %param.14) | copy-start | bytes 18436
  9.0 14.3 %all-to-all-start = ((bf16[8,3,1664]{2,1,0:T(4,128)(2,1)}), bf16[8,3,1664]{2,1,0:T(4,128)(2,1)S(1)}, u32[]{:S(2)}, u32[]{:S(2)}) async-start(bf16[8,3,1664]{2,1,0:T(4,128)(2,1)} %reshape.114), calls=%async_computation | async-start | bytes 212992 | tf_op jit(solution)/shard_map/all_to_all | solution.py:73
  27.3 10.4 %all-to-all-start.1 = ((bf16[16,3,512]{2,1,0:T(4,128)(2,1)}), bf16[16,3,512]{2,1,0:T(4,128)(2,1)S(1)}, u32[]{:S(2)}, u32[]{:S(2)}) async-start(bf16[16,3,512]{2,1,0:T(4,128)(2,1)} %broadcast_in_dim.15), calls=%async_computation.1 | async-start | bytes 131072 | tf_op jit(solution)/shard_map/all_to_all | solution.py:95
  30.8 7.1 %collective-permute-start = (bf16[512,128]{1,0:T(8,128)(2,1)S(1)}, bf16[512,128]{1,0:T(8,128)(2,1)S(1)}, u32[]{:S(2)}, u32[]{:S(2)}) collective-permute-start(bf16[512,128]{1,0:T(8,128)(2,1)S(1)} %constant_dynamic-slice_fusion), channel_id=1, source_target_pairs={{0,1},{1,0},{2,3},{3,2},{4,5},{5,4},{6,7},{7,6},{8,9},{9,8},{10,11... | collective-permute-start | bytes 393224 | tf_op jit(solution)/shard_map/ppermute | solution.py:50

commit v2 on v1

--- a/solution.py
+++ b/solution.py
@@ -3,6 +3,8 @@
 import jax
 import jax.numpy as jnp
 from jax import lax
+from jax.experimental import pallas as pl
+from jax.experimental.pallas import tpu as pltpu
 from jax.sharding import PartitionSpec as P
 
 BF = jnp.bfloat16
@@ -15,7 +17,7 @@
     return high, low
 
 
-def local(
+def plain(
     tokens,
     state,
     mix_gain,
@@ -119,6 +121,347 @@
     return (output, new_state)
 
 
+LANES = 128
+SHIFT = 64
+
+
+def stage_kernel(*refs, count, cut):
+    sources, targets, sems = refs[:count], refs[count:-1], refs[-1]
+    width = targets[-1].shape[1]
+    tp_at = lax.axis_index("tp")
+    copies = [(source, target) for source, target in zip(sources[:cut], targets[:cut])]
+    for source, near in ((sources[cut], tp_at), (sources[cut], 1 - tp_at)):
+        copies.append((source.at[:, pl.ds(near * width, width)], targets[len(copies)]))
+    copies = [pltpu.make_async_copy(a, b, sems.at[n]) for n, (a, b) in enumerate(copies)]
+    for copy in copies:
+        copy.start()
+    for copy in copies:
+        copy.wait()
+
+
+def load_kernel(*refs):
+    count = len(refs) // 2
+    sems = refs[-1]
+    copies = [pltpu.make_async_copy(refs[n], refs[count + n], sems.at[n]) for n in range(count)]
+    for copy in copies:
+        copy.start()
+    for copy in copies:
+        copy.wait()
+
+
+def project_kernel(
+    own_ref,
+    other_ref,
+    own_gain_ref,
+    other_gain_ref,
+    wq_ref,
+    wk_ref,
+    wv_ref,
+    wb_ref,
+    wd_ref,
+    out_ref,
+    res_ref,
+    pack_ref,
+    *,
+    n_kv,
+    seq,
+    heads,
+):
+    rows = own_ref.shape[0]
+    first = lax.axis_index("tp") == 0
+    own = own_ref[...].astype(F32)
+    other = other_ref[...].astype(F32)
+    own_scaled = own * own_gain_ref[...].astype(F32)
+    other_scaled = other * other_gain_ref[...].astype(F32)
+    scaled = jnp.concatenate(
+        [
+            jnp.where(first, own_scaled, other_scaled),
+            jnp.where(first, other_scaled, own_scaled),
+        ],
+        axis=1,
+    ).astype(BF)
+    dot = functools.partial(jnp.dot, preferred_element_type=F32)
+    for p, weight_ref in enumerate((wq_ref, wk_ref, wv_ref)):
+        product = dot(scaled, weight_ref[...])
+        for h in range(heads):
+            at = (p * heads + h) * rows
+            res_ref[at : at + rows, :] = product[:, h * LANES : (h + 1) * LANES]
+    at = lax.broadcasted_iota(jnp.int32, (LANES, heads), 0)
+    head = lax.broadcasted_iota(jnp.int32, (LANES, heads), 1)
+    place_beta = jnp.where(at == head, 1.0, 0.0).astype(BF)
+    place_decay = jnp.where(at == head + heads, 1.0, 0.0).astype(BF)
+    gate_weights = (dot(place_beta, wb_ref[...]) + dot(place_decay, wd_ref[...])).astype(BF)
+    squares = jnp.sum(own * own + other * other, axis=1, keepdims=True)
+    lanes = lax.broadcasted_iota(jnp.int32, (rows, LANES), 1)
+    gates = lax.dot_general(
+        scaled, gate_weights, (((1,), (1,)), ((), ())), preferred_element_type=F32
+    )
+    small = gates + jnp.where(lanes == 2 * heads, squares, 0.0)
+    high = small.astype(BF).astype(F32)
+    res_ref[3 * heads * rows :, :] = high + pltpu.roll(small - high, SHIFT, 1)
+    per_seq = 3 * heads + 1
+    packet = out_ref.shape[0] // n_kv
+    for s in range(seq):
+        for j in range(per_seq):
+            pack_ref[pl.ds(s * per_seq + j, n_kv, packet), :] = res_ref[
+                pl.ds(j * rows + s, n_kv, seq), :
+            ]
+    for j in range(seq * per_seq, packet):
+        pack_ref[pl.ds(j, n_kv, packet), :] = jnp.zeros((n_kv, LANES), F32)
+    out_ref[...] = pack_ref[...].astype(BF)
+
+
+def delta_kernel(
+    got_ref,
+    state_ref,
+    decay_log_ref,
+    head_gain_ref,
+    ff_gain_ref,
+    spread_ref,
+    new_ref,
+    *,
+    n_kv,
+    seq,
+    heads,
+    model,
+):
+    per_seq = 3 * heads + 1
+    packet = got_ref.shape[0] // n_kv
+    total = got_ref[:packet].astype(F32)
+    for d in range(1, n_kv):
+        total = total + got_ref[d * packet : (d + 1) * packet].astype(F32)
+    lane = lax.broadcasted_iota(jnp.int32, (1, LANES), 1)
+    rate = jnp.zeros((1, LANES), F32)
+    for h in range(heads):
+        rate = jnp.where(lane == heads + h, decay_log_ref[:, h : h + 1], rate)
+    rate = jnp.exp(rate)
+    betas, keeps, values, rows = [], [], [], []
+    for s in range(seq):
+        base = s * per_seq
+        small = total[base + 3 * heads : base + per_seq]
+        small = small + pltpu.roll(small, LANES - SHIFT, 1)
+        inverse = lax.rsqrt(small[:, 2 * heads : 2 * heads + 1] / model + 1e-06)
+        gates = inverse * small
+        betas.append(jax.nn.sigmoid(gates))
+        soft = jnp.maximum(gates, 0.0) + jnp.log1p(jnp.exp(-jnp.abs(gates)))
+        keeps.append(jnp.exp(-rate * soft))
+        query = inverse * total[base : base + heads]
+        key = inverse * total[base + heads : base + 2 * heads]
+        values.append(inverse * total[base + 2 * heads : base + 3 * heads])
+        rows.append(query * lax.rsqrt(jnp.sum(query * query, axis=1, keepdims=True) + 1e-06))
+        rows.append(key * lax.rsqrt(jnp.sum(key * key, axis=1, keepdims=True) + 1e-06))
+    count = 2 * heads * seq
+    padded = -(-count // 8) * 8
+    if padded > count:
+        rows.append(jnp.zeros((padded - count, LANES), F32))
+    columns = jnp.concatenate(rows, axis=0).T
+    reads = []
+    for s in range(seq):
+        for h in range(heads):
+            at = 2 * s * heads + h
+            qcol = columns[:, at : at + 1]
+            kcol = columns[:, at + heads : at + heads + 1]
+            kept = state_ref[s, h] * keeps[s][:, heads + h : heads + h + 1]
+            predicted = jnp.sum(kept * kcol, axis=0, keepdims=True)
+            change = betas[s][:, h : h + 1] * (values[s][h : h + 1] - predicted)
+            new = kept + kcol * change
+            new_ref[s, h] = new
+            reads.append(jnp.sum(new * qcol, axis=0, keepdims=True))
+    read = jnp.concatenate(reads, axis=0) / jnp.sqrt(jnp.float32(LANES))
+    normed = (
+        read
+        * lax.rsqrt(jnp.mean(read * read, axis=1, keepdims=True) + 1e-06)
+        * head_gain_ref[...].astype(F32)
+    )
+    lines = spread_ref.shape[1]
+    fill = lines - seq * heads
+    sent = jnp.concatenate(
+        [normed, jnp.broadcast_to(ff_gain_ref[...].astype(F32), (fill, LANES))], axis=0
+    ).astype(BF)
+    for d in range(spread_ref.shape[0]):
+        spread_ref[d] = sent
+
+
+def mix_kernel(
+    got_ref, tokens_ref, own_ref, other_ref, spread_ref, resid_ref, rows_ref, mixed_ref, *, n_kv, n_tp, seq, heads
+):
+    lines = got_ref.shape[0] // (n_kv * n_tp)
+    rows_ref[...] = got_ref[...].astype(F32)
+    dot = functools.partial(jnp.dot, preferred_element_type=F32)
+    halves = []
+    for t in range(n_tp):
+        blocks = []
+        for h in range(heads):
+            parts = [
+                rows_ref[pl.ds(t * lines + s * heads + h, n_kv, n_tp * lines), :] for s in range(seq)
+            ]
+            blocks.append(jnp.concatenate(parts, axis=0))
+        halves.append(jnp.concatenate(blocks, axis=1))
+    first = lax.axis_index("tp") == 0
+    own = jnp.where(first, halves[0], halves[1]).astype(BF)
+    other = jnp.where(first, halves[1], halves[0]).astype(BF)
+    mixed = dot(own, own_ref[...]).astype(BF).astype(F32) + dot(other, other_ref[...]).astype(BF).astype(F32)
+    for s in range(seq):
+        mixed_ref[pl.ds(s, n_kv, seq), :] = mixed[s * n_kv : (s + 1) * n_kv]
+    resid = (tokens_ref[...].astype(F32) + mixed_ref[...]).astype(BF)
+    resid_ref[...] = resid
+    for d in range(spread_ref.shape[0]):
+        spread_ref[d] = resid
+
+
+def feed_kernel(
+    got_ref, gains_ref, up_ref, down_hbm_ref, out_ref, down_ref, sem, *, gain_line, model
+):
+    copy = pltpu.make_async_copy(down_hbm_ref, down_ref, sem)
+    copy.start()
+    n_all, rows, width = got_ref.shape
+    lines = gains_ref.shape[0] // n_all
+    squares = jnp.zeros((rows, width), F32)
+    blocks = []
+    for d in range(n_all):
+        block = got_ref[d].astype(F32)
+        squares = squares + block * block
+        gain = gains_ref[d * lines : (d + 1) * lines].astype(F32)[gain_line : gain_line + 1]
+        blocks.append((block * gain).astype(BF))
+    inverse = lax.rsqrt(jnp.sum(squares, axis=1, keepdims=True) / model + 1e-06)
+    scaled = jnp.concatenate(blocks, axis=1)
+    up = jnp.dot(scaled, up_ref[...], preferred_element_type=F32) * inverse
+    up = jnp.maximum(up, 0.0)
+    act = (up * up).astype(BF)
+    copy.wait()
+    down = jnp.dot(act, down_ref[...], preferred_element_type=F32)
+    for d in range(n_all):
+        out_ref[d] = down[:, d * width : (d + 1) * width].astype(BF)
+
+
+def fused(
+    tokens,
+    state,
+    mix_gain,
+    w_query,
+    w_key,
+    w_value,
+    w_beta,
+    w_decay,
+    decay_log,
+    head_gain,
+    w_out,
+    ff_gain,
+    w_up,
+    w_down,
+    n_kv,
+    n_tp,
+):
+    rows, width = tokens.shape
+    seq, heads, size = state.shape[:3]
+    n_all = n_kv * n_tp
+    model = width * n_all
+    keys = heads * size
+    per_seq = 3 * heads + 1
+    packet = -(-seq * per_seq // 8) * 8
+    lines = -(-(seq * heads + 1) // 8) * 8
+    axes = ("kv", "tp")
+    swap = [(i, n_tp - 1 - i) for i in range(n_tp)]
+    shape = jax.ShapeDtypeStruct
+    vmem = pl.BlockSpec(memory_space=pltpu.VMEM)
+    params = pltpu.CompilerParams(vmem_limit_bytes=16 * 1024 * 1024)
+
+    gain_row = mix_gain[None, :]
+    other_tokens = lax.ppermute(tokens, "tp", swap)
+    other_gain = lax.ppermute(gain_row, "tp", swap)
+    hbm = pl.BlockSpec(memory_space=pltpu.HBM)
+    in_hbm = functools.partial(pltpu.with_memory_space_constraint, memory_space=pltpu.HBM)
+    loaded = (
+        w_query,
+        w_key,
+        w_value,
+        w_beta.T,
+        w_decay.T,
+        tokens,
+        gain_row,
+        head_gain[None, :],
+        ff_gain[None, :],
+        decay_log[None, :],
+    )
+    staged = pl.pallas_call(
+        functools.partial(stage_kernel, count=len(loaded) + 1, cut=len(loaded)),
+        out_shape=tuple(shape(a.shape, a.dtype) for a in loaded) + (shape((keys, width), BF),) * 2,
+        in_specs=[hbm] * (len(loaded) + 1),
+        out_specs=(vmem,) * (len(loaded) + 2),
+        scratch_shapes=[pltpu.SemaphoreType.DMA((len(loaded) + 2,))],
+        name="stage",
+        compiler_params=params,
+    )(*(in_hbm(a) for a in loaded + (w_out,)))
+    w_query, w_key, w_value, w_beta, w_decay, tokens, gain_row, head_gain, ff_gain, decay_log = staged[:-2]
+    own_cols, gone_cols = staged[-2:]
+    other_cols = lax.ppermute(gone_cols, "tp", swap)
+
+    sent = pl.pallas_call(
+        functools.partial(project_kernel, n_kv=n_kv, seq=seq, heads=heads),
+        out_shape=shape((n_kv * packet, LANES), BF),
+        in_specs=[vmem] * 9,
+        out_specs=vmem,
+        scratch_shapes=[
+            pltpu.VMEM((per_seq * rows, LANES), F32),
+            pltpu.VMEM((n_kv * packet, LANES), F32),
+        ],
+        name="project",
+        compiler_params=params,
+    )(tokens, other_tokens, gain_row, other_gain, w_query, w_key, w_value, w_beta, w_decay)
+    got = lax.all_to_all(sent.reshape(n_kv, packet, LANES), "kv", 0, 0, tiled=False)
+    late = lax.optimization_barrier((state, w_up, sent))[:2]
+    state, w_up = pl.pallas_call(
+        load_kernel,
+        out_shape=tuple(shape(a.shape, a.dtype) for a in late),
+        in_specs=[hbm] * len(late),
+        out_specs=(vmem,) * len(late),
+        scratch_shapes=[pltpu.SemaphoreType.DMA((len(late),))],
+        name="load",
+        compiler_params=params,
+    )(*(in_hbm(a) for a in late))
+    spread, new_state = pl.pallas_call(
+        functools.partial(delta_kernel, n_kv=n_kv, seq=seq, heads=heads, model=model),
+        out_shape=(shape((n_all, lines, LANES), BF), shape(state.shape, F32)),
+        in_specs=[vmem] * 5,
+        out_specs=(vmem, vmem),
+        name="delta",
+        compiler_params=params,
+    )(got.reshape(n_kv * packet, LANES), state, decay_log, head_gain, ff_gain)
+    got = lax.all_to_all(spread, axes, 0, 0, tiled=False).reshape(n_all * lines, LANES)
+    spread, resid = pl.pallas_call(
+        functools.partial(mix_kernel, n_kv=n_kv, n_tp=n_tp, seq=seq, heads=heads),
+        out_shape=(shape((n_all, rows, width), BF), shape((rows, width), BF)),
+        in_specs=[vmem] * 4,
+        out_specs=(vmem, vmem),
+        scratch_shapes=[
+            pltpu.VMEM((n_all * lines, LANES), F32),
+            pltpu.VMEM((rows, width), F32),
+        ],
+        name="mix",
+        compiler_params=params,
+    )(got, tokens, own_cols, other_cols)
+    got2 = lax.all_to_all(spread, axes, 0, 0, tiled=False)
+    down = pl.pallas_call(
+        functools.partial(feed_kernel, gain_line=seq * heads, model=model),
+        out_shape=shape((n_all, rows, width), BF),
+        in_specs=[vmem] * 3 + [hbm],
+        out_specs=vmem,
+        scratch_shapes=[pltpu.VMEM(w_down.shape, BF), pltpu.SemaphoreType.DMA(())],
+        name="feed",
+        compiler_params=params,
+    )(got2, got, w_up, in_hbm(w_down))
+    got3 = lax.all_to_all(down, axes, 0, 0, tiled=False)
+    output = (resid.astype(F32) + jnp.sum(got3.astype(F32), axis=0)).astype(BF)
+    return (output, new_state)
+
+
+def local(*arrays, n_kv, n_tp):
+    tokens, state = arrays[:2]
+    whole_tiles = tokens.shape[1] == LANES and state.shape[2] == LANES and n_kv % 8 == 0 and n_tp == 2
+    form = fused if whole_tiles else plain
+    return form(*arrays, n_kv=n_kv, n_tp=n_tp)
+
+
 def solution(mesh):
     placed = (
         P("dp", ("kv", "tp")),

time: 62.4 us -> 53.7 us (0.86)
  Pallas kernels: 0 us -> 8.6 us
  matrix products: 6.93 us -> 0 us
  other arithmetic: 5.89 us -> 0.62 us
  blocking collectives: 22.6 us -> 19.9 us
  local copies, waits for them, and re-layouts: 2.36 us -> 0 us
    pallas_call x0 -> x6, Pallas kernels: none -> 8.6 us  [the longest x1 2.08 us: fused(): pl.pallas_call(functools.partial(feed_kernel, gain_line=seq * heads, mode...]
    dot_general x7 -> x0, matrix products: 6.93 us -> none  [the longest x1 2.35 us: local(): dot(act, w_down).astype(BF).reshape(rows, n_all, width).transpose(1, 0, 2)]
    reduce_sum x9 -> x1, other arithmetic: 2.14 us -> 0.02 us  [fused(): output = (resid.astype(F32) + jnp.sum(got3.astype(F32), axis=0)).astype(BF)]
    all_gather x1 -> x0, blocking collectives: 2.11 us -> none  [local(): wide = lax.all_gather(packed, 'tp', axis=1, tiled=True)]
    concatenate x2 -> x0, other arithmetic: 0.88 us -> none  [the longest x1 0.87 us: local(): packed = jnp.concatenate([tokens, mix_gain[None, :]], axis=0)]
    convert_element_type x7 -> x1, other arithmetic: 1.43 us -> 0.6 us  [fused(): output = (resid.astype(F32) + jnp.sum(got3.astype(F32), axis=0)).astype(BF)]
    reshape x7 -> x0, local copies, waits for them, and re-layouts: 0.83 us -> none  [the longest x1 0.69 us: local(): sent = jnp.concatenate([dot(scaled, w_query).astype(BF), dot(scaled, w_ke...]
    broadcast_in_dim x5 -> x0, local copies, waits for them, and re-layouts: 0.76 us -> none  [the longest x1 0.65 us: local(): jnp.broadcast_to(normed[None], (n_all, seq, keys))]
  transfers between devices with their start and end apart: 3 -> 5, of which waited for: 2 -> 2; matrix products, arithmetic and copies ran while one was open for 3% -> 0% of each run, Pallas kernels for 0% -> 10%
where the time goes in v2:
time: 53.7 us; the launch traced here: 53.2 us
  blocking collectives  19.9 us (37%)
  waiting for transfers between devices  12 us (22%)
  starting transfers between devices  11.4 us (21%)
  Pallas kernels  8.6 us (16%)
  between operations  0.71 us (1%)
  other arithmetic  0.62 us (1%)
    all_to_all x1, blocking collectives, fused(): got3 = lax.all_to_all(down, axes, 0, 0, tiled=False)  9.96 us
    all_to_all x1, blocking collectives, fused(): got2 = lax.all_to_all(spread, axes, 0, 0, tiled=False)  9.96 us
    all_to_all x1, starting transfers between devices, fused(): lax.all_to_all(sent.reshape(n_kv, packet, LANES), 'kv', 0, 0, tiled=False)  7.24 us
    all_to_all x1, waiting for transfers between devices, fused(): lax.all_to_all(spread, axes, 0, 0, tiled=False)  6.85 us
    all_to_all x1, waiting for transfers between devices, fused(): lax.all_to_all(sent.reshape(n_kv, packet, LANES), 'kv', 0, 0, tiled=False)  5.13 us
    all_to_all x1, starting transfers between devices, fused(): lax.all_to_all(spread, axes, 0, 0, tiled=False)  3.5 us
    pallas_call x1, Pallas kernels, fused(): pl.pallas_call(functools.partial(feed_kernel, gain_line=seq * heads, mode...  2.08 us
    pallas_call x1, Pallas kernels, fused(): pl.pallas_call(functools.partial(delta_kernel, n_kv=n_kv, seq=seq, heads=...  1.92 us
  transfers between devices with their start and end apart: 5, of which 2 were waited for; matrix products, arithmetic and copies ran while one was open for 0% of the time, Pallas kernels for 10%

profile of v2, /device:TPU:0, one launch (start us, length us, event | category | flops | bytes accessed | tf_op | source)
XLA Modules:
  0.0 53.2 jit_solution(14704161338730180106)
XLA Ops:
  0.6 0.6 %collective-permute-start = (bf16[24,128]{1,0:T(8,128)(2,1)}, bf16[24,128]{1,0:T(8,128)(2,1)S(1)}, u32[]{:S(2)}, u32[]{:S(2)}) collective-permute-start(bf16[24,128]{1,0:T(8,128)(2,1)} %refs_5_.1), channel_id=1, source_target_pairs={{0,1},{1,0},{2,3},{3,2},{4,5},{5,4},{6,7},{7,6},{8,9},{9,8},{10,11... | collective-permute-start | bytes 18440 | tf_op jit(solution)/shard_map/ppermute | solution.py:370
  1.2 0.1 collective-permute-start.1
  1.3 1.4 %stage.1 = (bf16[256,512]{1,0:T(8,128)(2,1)S(1)}, bf16[256,512]{1,0:T(8,128)(2,1)S(1)}, bf16[256,512]{1,0:T(8,128)(2,1)S(1)}, bf16[4,256]{1,0:T(4,128)(2,1)S(1)}...) custom-call(bf16[256,512]{1,0:T(8,128)(2,1)} %refs_0_.1, ...), custom_call_target="tpu_custom_call" | custom-call | tf_op jit(solution)/shard_map/stage/pallas_call | solution.py:386
  2.6 0.0 collective-permute-done.1.other_gain_ref
  2.7 0.0 collective-permute-done.other_ref
  2.7 1.2 %project.1 = bf16[320,128]{1,0:T(8,128)(2,1)} custom-call(bf16[24,128]{1,0:T(8,128)(2,1)S(1)} %get-tuple-element.22.own_ref.tokens_ref, bf16[24,128]{1,0:T(8,128)(2,1)S(1)} %collective-permute-done.other_ref, bf16[1,128]{1,0:T(2,128)(2,1)S(1)} %get-tuple-element.23.own_gain_ref, bf16[1,128]{1,0:T(2,128)(2,1)S(1)} %collective-permute-done.1.other_gain_ref, ...), custom_call_target="tpu_custom_call" | custom-call | tf_op jit(solution)/shard_map/project/pallas_call | solution.py:399
  3.8 7.2 %all-to-all-start = ((bf16[8,40,128]{2,1,0:T(8,128)(2,1)}), bf16[8,40,128]{2,1,0:T(8,128)(2,1)S(1)}, u32[]{:S(2)}, u32[]{:S(2)}) async-start(bf16[8,40,128]{2,1,0:T(8,128)(2,1)} %bitcast.6), calls=%async_computation | async-start | bytes 163840 | tf_op jit(solution)/shard_map/all_to_all | solution.py:411
  11.1 0.0 collective-permute-start.2
  11.1 1.9 %load.1 = (f32[3,4,128,128]{3,2,1,0:T(8,128)S(1)}, bf16[2048,512]{1,0:T(8,128)(2,1)S(1)}) custom-call(f32[3,4,128,128]{3,2,1,0:T(8,128)} %refs_0_.2, bf16[2048,512]{1,0:T(8,128)(2,1)} %refs_1_.2), custom_call_target="tpu_custom_call" | custom-call | tf_op jit(solution)/shard_map/load/pallas_call | solution.py:413
  12.9 5.1 %all-to-all-done = bf16[8,40,128]{2,1,0:T(8,128)(2,1)S(1)} async-done(((bf16[8,40,128]{2,1,0:T(8,128)(2,1)}), bf16[8,40,128]{2,1,0:T(8,128)(2,1)S(1)}, u32[]{:S(2)}, u32[]{:S(2)}) %all-to-all-start) | async-done | bytes 81952 | tf_op jit(solution)/shard_map/all_to_all | solution.py:411
  18.1 1.9 %delta.1 = (bf16[16,16,128]{2,1,0:T(8,128)(2,1)}, f32[3,4,128,128]{3,2,1,0:T(8,128)}) custom-call(bf16[320,128]{1,0:T(8,128)(2,1)S(1)} %bitcast.11, f32[3,4,128,128]{3,2,1,0:T(8,128)S(1)} %get-tuple-element.31.state_ref, f32[1,4]{1,0:T(1,128)S(1)} %get-tuple-element.32.decay_log_ref, bf16[1,128]{1,0:T(2,128)(2,1)S(1)} %get-tuple-element.33.head_gain_ref, ...), custom_call_target="tpu_custom_call" | custom-call | tf_op jit(solution)/shard_map/delta/pallas_call | solution.py:422
  20.0 3.5 %all-to-all-start.1 = ((bf16[16,16,128]{2,1,0:T(8,128)(2,1)}), bf16[16,16,128]{2,1,0:T(8,128)(2,1)S(1)}, u32[]{:S(2)}, u32[]{:S(2)}) async-start(bf16[16,16,128]{2,1,0:T(8,128)(2,1)} %get-tuple-element.35), calls=%async_computation.1 | async-start | bytes 131072 | tf_op jit(solution)/shard_map/all_to_all | solution.py:430
  23.5 0.0 collective-permute-done.2.other_ref
  23.5 6.8 %all-to-all-done.1 = bf16[16,16,128]{2,1,0:T(8,128)(2,1)S(1)} async-done(((bf16[16,16,128]{2,1,0:T(8,128)(2,1)}), bf16[16,16,128]{2,1,0:T(8,128)(2,1)S(1)}, u32[]{:S(2)}, u32[]{:S(2)}) %all-to-all-start.1) | async-done | bytes 65568 | tf_op jit(solution)/shard_map/all_to_all | solution.py:430
  30.4 0.2 mix.1
  30.6 10.0 %all_to_all.20.got_ref = bf16[16,24,128]{2,1,0:T(8,128)(2,1)S(1)} all-to-all(bf16[16,24,128]{2,1,0:T(8,128)(2,1)S(1)} %get-tuple-element.39), channel_id=1, replica_groups=mesh['dp'=2,'kv'=8,'tp'=2] {'kv','tp'}, dimensions={0} | all-to-all | bytes 196608 | tf_op jit(solution)/shard_map/all_to_all | solution.py:443
  40.6 2.1 %feed.1 = bf16[16,24,128]{2,1,0:T(8,128)(2,1)S(1)} custom-call(bf16[16,24,128]{2,1,0:T(8,128)(2,1)S(1)} %all_to_all.20.got_ref, bf16[256,128]{1,0:T(8,128)(2,1)S(1)} %bitcast.10, bf16[2048,512]{1,0:T(8,128)(2,1)S(1)} %get-tuple-element.40.up_ref, bf16[512,2048]{1,0:T(8,128)(2,1)} %down_hbm_ref.1), custom_call_target="tpu_custom_call" | custom-call | tf_op jit(solution)/shard_map/feed/pallas_call | solution.py:444
  42.6 10.0 %all_to_all.21 = bf16[16,24,128]{2,1,0:T(8,128)(2,1)S(1)} all-to-all(bf16[16,24,128]{2,1,0:T(8,128)(2,1)S(1)} %feed.1), channel_id=1, replica_groups=mesh['dp'=2,'kv'=8,'tp'=2] {'kv','tp'}, dimensions={0} | all-to-all | bytes 196608 | tf_op jit(solution)/shard_map/all_to_all | solution.py:453
  52.6 0.6 %add_convert_fusion = bf16[24,128]{1,0:T(8,128)(2,1)} fusion(f32[24,128]{1,0:T(8,128)S(1)} %convert_reduce_fusion, bf16[24,128]{1,0:T(8,128)(2,1)S(1)} %get-tuple-element.38), kind=kLoop, calls=%fused_computation.1 | loop fusion | flops 9216 | bytes 24576 | tf_op jit(solution)/shard_map/convert_element_type | solution.py:454
  (1 shorter events, 0.0 us)
Async XLA Ops:
  0.6 2.0 %collective-permute-start = (bf16[24,128]{1,0:T(8,128)(2,1)}, bf16[24,128]{1,0:T(8,128)(2,1)S(1)}, u32[]{:S(2)}, u32[]{:S(2)}) collective-permute-start(bf16[24,128]{1,0:T(8,128)(2,1)} %refs_5_.1), channel_id=1, source_target_pairs={{0,1},{1,0},{2,3},{3,2},{4,5},{5,4},{6,7},{7,6},{8,9},{9,8},{10,11... | collective-permute-start | bytes 18440 | tf_op jit(solution)/shard_map/ppermute | solution.py:370
  1.2 1.5 %collective-permute-start.1 = (bf16[1,128]{1,0:T(2,128)(2,1)}, bf16[1,128]{1,0:T(2,128)(2,1)S(1)}, u32[]{:S(2)}, u32[]{:S(2)}) collective-permute-start(bf16[1,128]{1,0:T(2,128)(2,1)} %bitcast.17), channel_id=1, source_target_pairs={{0,1},{1,0},{2,3},{3,2},{4,5},{5,4},{6,7},{7,6},{8,9},{9,8},{10,11... | collective-permute-start | bytes 776 | tf_op jit(solution)/shard_map/ppermute | solution.py:371
  3.8 14.3 %all-to-all-start = ((bf16[8,40,128]{2,1,0:T(8,128)(2,1)}), bf16[8,40,128]{2,1,0:T(8,128)(2,1)S(1)}, u32[]{:S(2)}, u32[]{:S(2)}) async-start(bf16[8,40,128]{2,1,0:T(8,128)(2,1)} %bitcast.6), calls=%async_computation | async-start | bytes 163840 | tf_op jit(solution)/shard_map/all_to_all | solution.py:411
  11.1 12.4 %collective-permute-start.2 = (bf16[512,128]{1,0:T(8,128)(2,1)S(1)}, bf16[512,128]{1,0:T(8,128)(2,1)S(1)}, u32[]{:S(2)}, u32[]{:S(2)}) collective-permute-start(bf16[512,128]{1,0:T(8,128)(2,1)S(1)} %get-tuple-element.37), channel_id=1, source_target_pairs={{0,1},{1,0},{2,3},{3,2},{4,5},{5,4},{6,7},{7,6},{8,9},{9,8},{10,11... | collective-permute-start | bytes 393224 | tf_op jit(solution)/shard_map/ppermute | solution.py:397
  20.0 10.4 %all-to-all-start.1 = ((bf16[16,16,128]{2,1,0:T(8,128)(2,1)}), bf16[16,16,128]{2,1,0:T(8,128)(2,1)S(1)}, u32[]{:S(2)}, u32[]{:S(2)}) async-start(bf16[16,16,128]{2,1,0:T(8,128)(2,1)} %get-tuple-element.35), calls=%async_computation.1 | async-start | bytes 131072 | tf_op jit(solution)/shard_map/all_to_all | solution.py:430

commit v3 on v2

--- a/solution.py
+++ b/solution.py
@@ -125,34 +125,39 @@
 SHIFT = 64
 
 
-def stage_kernel(*refs, count, cut):
-    sources, targets, sems = refs[:count], refs[count:-1], refs[-1]
-    width = targets[-1].shape[1]
-    tp_at = lax.axis_index("tp")
-    copies = [(source, target) for source, target in zip(sources[:cut], targets[:cut])]
-    for source, near in ((sources[cut], tp_at), (sources[cut], 1 - tp_at)):
-        copies.append((source.at[:, pl.ds(near * width, width)], targets[len(copies)]))
-    copies = [pltpu.make_async_copy(a, b, sems.at[n]) for n, (a, b) in enumerate(copies)]
+def prepare_kernel(
+    tokens_ref,
+    gain_ref,
+    beta_ref,
+    decay_ref,
+    scaled_ref,
+    squares_ref,
+    beta_out_ref,
+    decay_out_ref,
+    tokens_in_ref,
+    gain_in_ref,
+    sems,
+):
+    pairs = (
+        (tokens_ref, tokens_in_ref),
+        (gain_ref, gain_in_ref),
+        (beta_ref, beta_out_ref),
+        (decay_ref, decay_out_ref),
+    )
+    copies = [pltpu.make_async_copy(a, b, sems.at[n]) for n, (a, b) in enumerate(pairs)]
     for copy in copies:
         copy.start()
     for copy in copies:
         copy.wait()
-
-
-def load_kernel(*refs):
-    count = len(refs) // 2
-    sems = refs[-1]
-    copies = [pltpu.make_async_copy(refs[n], refs[count + n], sems.at[n]) for n in range(count)]
-    for copy in copies:
-        copy.start()
-    for copy in copies:
-        copy.wait()
+    tokens = tokens_in_ref[...].astype(F32)
+    scaled_ref[...] = (tokens * gain_in_ref[...].astype(F32)).astype(BF)
+    squares_ref[...] = tokens * tokens
 
 
 def project_kernel(
     own_ref,
+    squares_ref,
     other_ref,
-    own_gain_ref,
     other_gain_ref,
     wq_ref,
     wk_ref,
@@ -169,9 +174,8 @@
 ):
     rows = own_ref.shape[0]
     first = lax.axis_index("tp") == 0
-    own = own_ref[...].astype(F32)
+    own_scaled = own_ref[...].astype(F32)
     other = other_ref[...].astype(F32)
-    own_scaled = own * own_gain_ref[...].astype(F32)
     other_scaled = other * other_gain_ref[...].astype(F32)
     scaled = jnp.concatenate(
         [
@@ -191,7 +195,7 @@
     place_beta = jnp.where(at == head, 1.0, 0.0).astype(BF)
     place_decay = jnp.where(at == head + heads, 1.0, 0.0).astype(BF)
     gate_weights = (dot(place_beta, wb_ref[...]) + dot(place_decay, wd_ref[...])).astype(BF)
-    squares = jnp.sum(own * own + other * other, axis=1, keepdims=True)
+    squares = jnp.sum(squares_ref[...] + other * other, axis=1, keepdims=True)
     lanes = lax.broadcasted_iota(jnp.int32, (rows, LANES), 1)
     gates = lax.dot_general(
         scaled, gate_weights, (((1,), (1,)), ((), ())), preferred_element_type=F32
@@ -293,14 +297,18 @@
         blocks = []
         for h in range(heads):
             parts = [
-                rows_ref[pl.ds(t * lines + s * heads + h, n_kv, n_tp * lines), :] for s in range(seq)
+                rows_ref[pl.ds(t * n_kv * lines + s * heads + h, n_kv, lines), :] for s in range(seq)
             ]
             blocks.append(jnp.concatenate(parts, axis=0))
         halves.append(jnp.concatenate(blocks, axis=1))
-    first = lax.axis_index("tp") == 0
+    tp_at = lax.axis_index("tp")
+    width = resid_ref.shape[1]
+    cols = pl.ds(pl.multiple_of(tp_at * width, width), width)
+    first = tp_at == 0
     own = jnp.where(first, halves[0], halves[1]).astype(BF)
     other = jnp.where(first, halves[1], halves[0]).astype(BF)
-    mixed = dot(own, own_ref[...]).astype(BF).astype(F32) + dot(other, other_ref[...]).astype(BF).astype(F32)
+    mixed = dot(own, own_ref[:, cols]).astype(BF).astype(F32)
+    mixed = mixed + dot(other, other_ref[:, cols]).astype(BF).astype(F32)
     for s in range(seq):
         mixed_ref[pl.ds(s, n_kv, seq), :] = mixed[s * n_kv : (s + 1) * n_kv]
     resid = (tokens_ref[...].astype(F32) + mixed_ref[...]).astype(BF)
@@ -310,15 +318,28 @@
 
 
 def feed_kernel(
-    got_ref, gains_ref, up_ref, down_hbm_ref, out_ref, down_ref, sem, *, gain_line, model
-):
-    copy = pltpu.make_async_copy(down_hbm_ref, down_ref, sem)
+    got_ref,
+    gains_ref,
+    up_ref,
+    down_ref,
+    state_ref,
+    out_ref,
+    new_ref,
+    sem,
+    *,
+    gain_line,
+    model,
+    n_tp,
+):
+    copy = pltpu.make_async_copy(state_ref, new_ref, sem)
     copy.start()
     n_all, rows, width = got_ref.shape
+    n_kv = n_all // n_tp
     lines = gains_ref.shape[0] // n_all
     squares = jnp.zeros((rows, width), F32)
     blocks = []
-    for d in range(n_all):
+    for at in range(n_all):
+        d = (at % n_tp) * n_kv + at // n_tp
         block = got_ref[d].astype(F32)
         squares = squares + block * block
         gain = gains_ref[d * lines : (d + 1) * lines].astype(F32)[gain_line : gain_line + 1]
@@ -328,10 +349,11 @@
     up = jnp.dot(scaled, up_ref[...], preferred_element_type=F32) * inverse
     up = jnp.maximum(up, 0.0)
     act = (up * up).astype(BF)
+    down = jnp.dot(act, down_ref[...], preferred_element_type=F32)
+    for at in range(n_all):
+        d = (at % n_tp) * n_kv + at // n_tp
+        out_ref[d] = down[:, at * width : (at + 1) * width].astype(BF)
     copy.wait()
-    down = jnp.dot(act, down_ref[...], preferred_element_type=F32)
-    for d in range(n_all):
-        out_ref[d] = down[:, d * width : (d + 1) * width].astype(BF)
 
 
 def fused(
@@ -360,10 +382,11 @@
     per_seq = 3 * heads + 1
     packet = -(-seq * per_seq // 8) * 8
     lines = -(-(seq * heads + 1) // 8) * 8
-    axes = ("kv", "tp")
+    axes = ("tp", "kv")
     swap = [(i, n_tp - 1 - i) for i in range(n_tp)]
     shape = jax.ShapeDtypeStruct
     vmem = pl.BlockSpec(memory_space=pltpu.VMEM)
+    cost = pl.CostEstimate(flops=4 * 10**9, bytes_accessed=8 * 10**6, transcendentals=0)
     params = pltpu.CompilerParams(vmem_limit_bytes=16 * 1024 * 1024)
 
     gain_row = mix_gain[None, :]
@@ -371,30 +394,27 @@
     other_gain = lax.ppermute(gain_row, "tp", swap)
     hbm = pl.BlockSpec(memory_space=pltpu.HBM)
     in_hbm = functools.partial(pltpu.with_memory_space_constraint, memory_space=pltpu.HBM)
-    loaded = (
-        w_query,
-        w_key,
-        w_value,
-        w_beta.T,
-        w_decay.T,
-        tokens,
-        gain_row,
-        head_gain[None, :],
-        ff_gain[None, :],
-        decay_log[None, :],
-    )
-    staged = pl.pallas_call(
-        functools.partial(stage_kernel, count=len(loaded) + 1, cut=len(loaded)),
-        out_shape=tuple(shape(a.shape, a.dtype) for a in loaded) + (shape((keys, width), BF),) * 2,
-        in_specs=[hbm] * (len(loaded) + 1),
-        out_specs=(vmem,) * (len(loaded) + 2),
-        scratch_shapes=[pltpu.SemaphoreType.DMA((len(loaded) + 2,))],
-        name="stage",
+    other_out = lax.ppermute(w_out, "tp", swap)
+    beta_rows, decay_rows = w_beta.T, w_decay.T
+    own_scaled, squares, beta_rows, decay_rows = pl.pallas_call(
+        prepare_kernel,
+        out_shape=(
+            shape(tokens.shape, BF),
+            shape(tokens.shape, F32),
+            shape(beta_rows.shape, BF),
+            shape(decay_rows.shape, BF),
+        ),
+        in_specs=[hbm] * 4,
+        out_specs=(vmem,) * 4,
+        scratch_shapes=[
+            pltpu.VMEM(tokens.shape, BF),
+            pltpu.VMEM(gain_row.shape, BF),
+            pltpu.SemaphoreType.DMA((4,)),
+        ],
+        name="prepare",
+        cost_estimate=cost,
         compiler_params=params,
-    )(*(in_hbm(a) for a in loaded + (w_out,)))
-    w_query, w_key, w_value, w_beta, w_decay, tokens, gain_row, head_gain, ff_gain, decay_log = staged[:-2]
-    own_cols, gone_cols = staged[-2:]
-    other_cols = lax.ppermute(gone_cols, "tp", swap)
+    )(in_hbm(tokens), in_hbm(gain_row), in_hbm(beta_rows), in_hbm(decay_rows))
 
     sent = pl.pallas_call(
         functools.partial(project_kernel, n_kv=n_kv, seq=seq, heads=heads),
@@ -406,27 +426,20 @@
             pltpu.VMEM((n_kv * packet, LANES), F32),
         ],
         name="project",
+        cost_estimate=cost,
         compiler_params=params,
-    )(tokens, other_tokens, gain_row, other_gain, w_query, w_key, w_value, w_beta, w_decay)
+    )(own_scaled, squares, other_tokens, other_gain, w_query, w_key, w_value, beta_rows, decay_rows)
+    sent, other_out = lax.optimization_barrier((sent, other_out))
     got = lax.all_to_all(sent.reshape(n_kv, packet, LANES), "kv", 0, 0, tiled=False)
-    late = lax.optimization_barrier((state, w_up, sent))[:2]
-    state, w_up = pl.pallas_call(
-        load_kernel,
-        out_shape=tuple(shape(a.shape, a.dtype) for a in late),
-        in_specs=[hbm] * len(late),
-        out_specs=(vmem,) * len(late),
-        scratch_shapes=[pltpu.SemaphoreType.DMA((len(late),))],
-        name="load",
-        compiler_params=params,
-    )(*(in_hbm(a) for a in late))
     spread, new_state = pl.pallas_call(
         functools.partial(delta_kernel, n_kv=n_kv, seq=seq, heads=heads, model=model),
         out_shape=(shape((n_all, lines, LANES), BF), shape(state.shape, F32)),
         in_specs=[vmem] * 5,
         out_specs=(vmem, vmem),
         name="delta",
+        cost_estimate=cost,
         compiler_params=params,
-    )(got.reshape(n_kv * packet, LANES), state, decay_log, head_gain, ff_gain)
+    )(got.reshape(n_kv * packet, LANES), state, decay_log[None, :], head_gain[None, :], ff_gain[None, :])
     got = lax.all_to_all(spread, axes, 0, 0, tiled=False).reshape(n_all * lines, LANES)
     spread, resid = pl.pallas_call(
         functools.partial(mix_kernel, n_kv=n_kv, n_tp=n_tp, seq=seq, heads=heads),
@@ -438,18 +451,19 @@
             pltpu.VMEM((rows, width), F32),
         ],
         name="mix",
+        cost_estimate=cost,
         compiler_params=params,
-    )(got, tokens, own_cols, other_cols)
+    )(got, tokens, w_out, other_out)
     got2 = lax.all_to_all(spread, axes, 0, 0, tiled=False)
-    down = pl.pallas_call(
-        functools.partial(feed_kernel, gain_line=seq * heads, model=model),
-        out_shape=shape((n_all, rows, width), BF),
-        in_specs=[vmem] * 3 + [hbm],
-        out_specs=vmem,
-        scratch_shapes=[pltpu.VMEM(w_down.shape, BF), pltpu.SemaphoreType.DMA(())],
+    down, new_state = pl.pallas_call(
+        functools.partial(feed_kernel, gain_line=seq * heads, model=model, n_tp=n_tp),
+        out_shape=(shape((n_all, rows, width), BF), shape(state.shape, F32)),
+        in_specs=[vmem] * 5,
+        out_specs=(vmem, hbm),
+        scratch_shapes=[pltpu.SemaphoreType.DMA(())],
         name="feed",
         compiler_params=params,
-    )(got2, got, w_up, in_hbm(w_down))
+    )(got2, got, w_up, w_down, new_state)
     got3 = lax.all_to_all(down, axes, 0, 0, tiled=False)
     output = (resid.astype(F32) + jnp.sum(got3.astype(F32), axis=0)).astype(BF)
     return (output, new_state)

time: 53.7 us -> 49.6 us (0.924)
  blocking collectives: 19.9 us -> 42.8 us
  waiting for transfers between devices: 12 us -> 0.01 us
  starting transfers between devices: 11.4 us -> 1.07 us
  Pallas kernels: 8.6 us -> 3.8 us
    all_to_all x0 -> x2, blocking collectives: none -> 23 us  [the longest x1 13.7 us: fused(): lax.all_to_all(sent.reshape(n_kv, packet, LANES), 'kv', 0, 0, tiled=False)]
    all_to_all x2 -> x0, waiting for transfers between devices: 12 us -> none  [the longest x1 6.85 us: fused(): lax.all_to_all(spread, axes, 0, 0, tiled=False)]
    all_to_all x2 -> x0, starting transfers between devices: 10.7 us -> none  [the longest x1 7.24 us: fused(): lax.all_to_all(sent.reshape(n_kv, packet, LANES), 'kv', 0, 0, tiled=False)]
    pallas_call x2 -> x1, Pallas kernels: 3.24 us -> 0.84 us  [fused(): pl.pallas_call(prepare_kernel, out_shape=(shape(tokens.shape, BF), shape(...]
    pallas_call x1, Pallas kernels: 2.08 us -> 1.11 us  [fused(): pl.pallas_call(functools.partial(feed_kernel, gain_line=seq * heads, mode...]
    pallas_call x1, Pallas kernels: 1.92 us -> 1.15 us  [fused(): pl.pallas_call(functools.partial(delta_kernel, n_kv=n_kv, seq=seq, heads=...]
    pallas_call x1, Pallas kernels: 1.15 us -> 0.5 us  [fused(): pl.pallas_call(functools.partial(project_kernel, n_kv=n_kv, seq=seq, head...]
  transfers between devices with their start and end apart: 5 -> 3, of which waited for: 2 -> 0; matrix products, arithmetic and copies ran while one was open for 0% -> 0% of each run, Pallas kernels for 10% -> 3%
where the time goes in v3:
time: 49.6 us; the launch traced here: 49.4 us
  blocking collectives  42.8 us (86%)
  Pallas kernels  3.8 us (8%)
  starting transfers between devices  1.07 us (2%)
  between operations  0.73 us (1%)
  other arithmetic  0.62 us (1%)
    all_to_all x1, blocking collectives, fused(): lax.all_to_all(sent.reshape(n_kv, packet, LANES), 'kv', 0, 0, tiled=False)  13.7 us
    all_to_all x1, blocking collectives, fused(): got2 = lax.all_to_all(spread, axes, 0, 0, tiled=False)  10 us
    all_to_all x1, blocking collectives, fused(): got3 = lax.all_to_all(down, axes, 0, 0, tiled=False)  9.77 us
    all_to_all x1, blocking collectives, fused(): lax.all_to_all(spread, axes, 0, 0, tiled=False)  9.3 us
    pallas_call x1, Pallas kernels, fused(): pl.pallas_call(functools.partial(delta_kernel, n_kv=n_kv, seq=seq, heads=...  1.15 us
    pallas_call x1, Pallas kernels, fused(): pl.pallas_call(functools.partial(feed_kernel, gain_line=seq * heads, mode...  1.11 us
  transfers between devices with their start and end apart: 3, of which 0 were waited for; matrix products, arithmetic and copies ran while one was open for 0% of the time, Pallas kernels for 3%

profile of v3, /device:TPU:0, one launch (start us, length us, event | category | flops | bytes accessed | tf_op | source)
XLA Modules:
  0.0 49.4 jit_solution(10907215756642747936)
XLA Ops:
  0.6 0.6 %collective-permute-start.1 = (bf16[1,128]{1,0:T(2,128)(2,1)}, bf16[1,128]{1,0:T(2,128)(2,1)S(1)}, u32[]{:S(2)}, u32[]{:S(2)}) collective-permute-start(bf16[1,128]{1,0:T(2,128)(2,1)} %bitcast.18), channel_id=1, source_target_pairs={{0,1},{1,0},{2,3},{3,2},{4,5},{5,4},{6,7},{7,6},{8,9},{9,8},{10,11... | collective-permute-start | bytes 776 | tf_op jit(solution)/shard_map/ppermute | solution.py:394
  1.2 0.1 collective-permute-start
  1.3 0.4 collective-permute-start.2
  1.7 0.0 copy-start.3
  1.7 0.0 copy-start.4
  1.7 0.0 copy-start.5
  1.7 0.8 %prepare.1 = (bf16[24,128]{1,0:T(8,128)(2,1)S(1)}, f32[24,128]{1,0:T(8,128)S(1)}, bf16[4,256]{1,0:T(4,128)(2,1)S(1)}, bf16[4,256]{1,0:T(4,128)(2,1)S(1)}) custom-call(bf16[24,128]{1,0:T(8,128)(2,1)} %tokens_ref.3, bf16[1,128]{1,0:T(2,128)(2,1)} %bitcast.19, bf16[4,256]{1,0:T(4,128)(2,1)} %bitcast.16, bf16[4,256]{1,0:T(4,128)(2,1)} %bitcast.17), custom_call_target="tpu_custom_call" | custom-call | flops 4000000000 | bytes 8000000 | tf_op jit(solution)/shard_map/prepare/pallas_call | solution.py:399
  2.6 0.0 collective-permute-done.1.other_gain_ref
  2.6 0.0 collective-permute-done.other_ref
  2.6 0.1 copy-done.3
  2.7 0.1 copy-done.4
  2.8 0.1 copy-done.5
  2.9 0.0 copy-start.2
  2.9 0.0 copy-start.8
  2.9 0.0 copy-start.9
  2.9 0.0 copy-start.10
  2.9 0.5 %project.1 = bf16[320,128]{1,0:T(8,128)(2,1)S(1)} custom-call(bf16[24,128]{1,0:T(8,128)(2,1)S(1)} %get-tuple-element.14.own_ref, f32[24,128]{1,0:T(8,128)S(1)} %get-tuple-element.15.squares_ref, bf16[24,128]{1,0:T(8,128)(2,1)S(1)} %collective-permute-done.other_ref, bf16[1,128]{1,0:T(2,128)(2,1)S(1)} %collective-permute-done.1.other_gain_ref, ...), custom_call_target="tpu_custom_call" | custom-call | flops 4000000000 | bytes 8000000 | tf_op jit(solution)/shard_map/project/pallas_call | solution.py:419
  3.4 0.0 collective-permute-done.2.other_ref
  3.4 13.7 %all_to_all.20 = bf16[8,40,128]{2,1,0:T(8,128)(2,1)S(1)} all-to-all(bf16[8,40,128]{2,1,0:T(8,128)(2,1)S(1)} %bitcast.11), channel_id=1, replica_groups=mesh['dp'=2,'kv'=8,'tp'=2] {'kv'}, dimensions={0} | all-to-all | bytes 163840 | tf_op jit(solution)/shard_map/all_to_all | solution.py:433
  17.1 0.0 copy-done.2
  17.1 0.0 copy-done.8
  17.1 0.0 copy-done.9
  17.1 0.0 copy-done.10
  17.1 0.0 copy-start.6
  17.1 0.0 copy-start.7
  17.2 1.2 %delta.1 = (bf16[16,16,128]{2,1,0:T(8,128)(2,1)S(1)}, f32[3,4,128,128]{3,2,1,0:T(8,128)S(1)}) custom-call(bf16[320,128]{1,0:T(8,128)(2,1)S(1)} %bitcast.12, f32[3,4,128,128]{3,2,1,0:T(8,128)S(1)} %copy-done.2, f32[1,4]{1,0:T(1,128)S(1)} %bitcast.13, bf16[1,128]{1,0:T(2,128)(2,1)S(1)} %bitcast.14, bf16[1,128]{1,0:T(2,128)(2,1)S(1)} %bitcast.15), custom_call_target="tpu_custom_call" | custom-call | flops 4000000000 | bytes 8000000 | tf_op jit(solution)/shard_map/delta/pallas_call | solution.py:434
  18.3 9.3 %all_to_all.21 = bf16[16,16,128]{2,1,0:T(8,128)(2,1)S(1)} all-to-all(bf16[16,16,128]{2,1,0:T(8,128)(2,1)S(1)} %get-tuple-element.19), channel_id=1, replica_groups=mesh['dp'=2,'kv'=8,'tp'=2] {'tp','kv'}, dimensions={0} | all-to-all | bytes 131072 | tf_op jit(solution)/shard_map/all_to_all | solution.py:443
  27.6 0.0 copy-done.6
  27.6 0.0 copy-done.7
  27.6 0.0 copy-start
  27.6 0.0 copy-start.1
  27.6 0.2 mix.1
  27.8 10.0 %all_to_all.22.got_ref = bf16[16,24,128]{2,1,0:T(8,128)(2,1)S(1)} all-to-all(bf16[16,24,128]{2,1,0:T(8,128)(2,1)S(1)} %get-tuple-element.22), channel_id=1, replica_groups=mesh['dp'=2,'kv'=8,'tp'=2] {'tp','kv'}, dimensions={0} | all-to-all | bytes 196608 | tf_op jit(solution)/shard_map/all_to_all | solution.py:457
  37.9 0.0 copy-done
  37.9 0.0 copy-done.1
  37.9 1.1 %feed.1 = (bf16[16,24,128]{2,1,0:T(8,128)(2,1)S(1)}, f32[3,4,128,128]{3,2,1,0:T(8,128)}) custom-call(bf16[16,24,128]{2,1,0:T(8,128)(2,1)S(1)} %all_to_all.22.got_ref, bf16[256,128]{1,0:T(8,128)(2,1)S(1)} %bitcast.10, bf16[2048,512]{1,0:T(8,128)(2,1)S(1)} %copy-done, bf16[512,2048]{1,0:T(8,128)(2,1)S(1)} %copy-done.1, ...), custom_call_target="tpu_custom_call" | custom-call | tf_op jit(solution)/shard_map/feed/pallas_call | solution.py:458
  39.0 9.8 %all_to_all.23 = bf16[16,24,128]{2,1,0:T(8,128)(2,1)S(1)} all-to-all(bf16[16,24,128]{2,1,0:T(8,128)(2,1)S(1)} %get-tuple-element.24), channel_id=1, replica_groups=mesh['dp'=2,'kv'=8,'tp'=2] {'tp','kv'}, dimensions={0} | all-to-all | bytes 196608 | tf_op jit(solution)/shard_map/all_to_all | solution.py:467
  48.8 0.6 %add_convert_fusion = bf16[24,128]{1,0:T(8,128)(2,1)} fusion(f32[24,128]{1,0:T(8,128)S(1)} %convert_reduce_fusion, bf16[24,128]{1,0:T(8,128)(2,1)S(1)} %get-tuple-element.21), kind=kLoop, calls=%fused_computation.1 | loop fusion | flops 9216 | bytes 24576 | tf_op jit(solution)/shard_map/convert_element_type | solution.py:468
  (1 shorter events, 0.0 us)
Async XLA Ops:
  0.6 1.9 %collective-permute-start.1 = (bf16[1,128]{1,0:T(2,128)(2,1)}, bf16[1,128]{1,0:T(2,128)(2,1)S(1)}, u32[]{:S(2)}, u32[]{:S(2)}) collective-permute-start(bf16[1,128]{1,0:T(2,128)(2,1)} %bitcast.18), channel_id=1, source_target_pairs={{0,1},{1,0},{2,3},{3,2},{4,5},{5,4},{6,7},{7,6},{8,9},{9,8},{10,11... | collective-permute-start | bytes 776 | tf_op jit(solution)/shard_map/ppermute | solution.py:394
  1.2 1.4 %collective-permute-start = (bf16[24,128]{1,0:T(8,128)(2,1)}, bf16[24,128]{1,0:T(8,128)(2,1)S(1)}, u32[]{:S(2)}, u32[]{:S(2)}) collective-permute-start(bf16[24,128]{1,0:T(8,128)(2,1)} %tokens_ref.3), channel_id=1, source_target_pairs={{0,1},{1,0},{2,3},{3,2},{4,5},{5,4},{6,7},{7,6},{8,9},{9,8},{10,11... | collective-permute-start | bytes 18440 | tf_op jit(solution)/shard_map/ppermute | solution.py:393
  1.3 2.1 %collective-permute-start.2 = (bf16[512,256]{1,0:T(8,128)(2,1)}, bf16[512,256]{1,0:T(8,128)(2,1)S(1)}, u32[]{:S(2)}, u32[]{:S(2)}) collective-permute-start(bf16[512,256]{1,0:T(8,128)(2,1)} %own_ref.1), channel_id=1, source_target_pairs={{0,1},{1,0},{2,3},{3,2},{4,5},{5,4},{6,7},{7,6},{8,9},{9,8},{10,11... | collective-permute-start | bytes 786440 | tf_op jit(solution)/shard_map/ppermute | solution.py:397
  1.7 0.9 %copy-start.3 = (bf16[256,512]{1,0:T(8,128)(2,1)S(1)}, bf16[256,512]{1,0:T(8,128)(2,1)}, u32[]{:S(2)}) copy-start(bf16[256,512]{1,0:T(8,128)(2,1)} %wq_ref.1) | copy-start | bytes 786436
  1.7 1.1 %copy-start.4 = (bf16[256,512]{1,0:T(8,128)(2,1)S(1)}, bf16[256,512]{1,0:T(8,128)(2,1)}, u32[]{:S(2)}) copy-start(bf16[256,512]{1,0:T(8,128)(2,1)} %wk_ref.1) | copy-start | bytes 786436
  1.7 1.2 %copy-start.5 = (bf16[256,512]{1,0:T(8,128)(2,1)S(1)}, bf16[256,512]{1,0:T(8,128)(2,1)}, u32[]{:S(2)}) copy-start(bf16[256,512]{1,0:T(8,128)(2,1)} %wv_ref.1) | copy-start | bytes 786436
  2.9 14.2 %copy-start.2 = (f32[3,4,128,128]{3,2,1,0:T(8,128)S(1)}, f32[3,4,128,128]{3,2,1,0:T(8,128)}, u32[]{:S(2)}) copy-start(f32[3,4,128,128]{3,2,1,0:T(8,128)} %state_ref.1) | copy-start | bytes 2359300
  2.9 14.2 %copy-start.8 = (f32[4]{0:T(128)S(1)}, f32[4]{0:T(128)}, u32[]{:S(2)}) copy-start(f32[4]{0:T(128)} %param.22) | copy-start | bytes 52
  2.9 14.2 %copy-start.9 = (bf16[128]{0:T(256)(128)(2,1)S(1)}, bf16[128]{0:T(256)(128)(2,1)}, u32[]{:S(2)}) copy-start(bf16[128]{0:T(256)(128)(2,1)} %param.23) | copy-start | bytes 772
  2.9 14.2 %copy-start.10 = (bf16[128]{0:T(256)(128)(2,1)S(1)}, bf16[128]{0:T(256)(128)(2,1)}, u32[]{:S(2)}) copy-start(bf16[128]{0:T(256)(128)(2,1)} %param.25) | copy-start | bytes 772
  17.1 10.5 %copy-start.6 = (bf16[512,256]{1,0:T(8,128)(2,1)S(1)}, bf16[512,256]{1,0:T(8,128)(2,1)}, u32[]{:S(2)}) copy-start(bf16[512,256]{1,0:T(8,128)(2,1)} %own_ref.1) | copy-start | bytes 786436
  17.1 10.5 %copy-start.7 = (bf16[24,128]{1,0:T(8,128)(2,1)S(1)}, bf16[24,128]{1,0:T(8,128)(2,1)}, u32[]{:S(2)}) copy-start(bf16[24,128]{1,0:T(8,128)(2,1)} %tokens_ref.3) | copy-start | bytes 18436
  27.6 10.2 %copy-start = (bf16[2048,512]{1,0:T(8,128)(2,1)S(1)}, bf16[2048,512]{1,0:T(8,128)(2,1)}, u32[]{:S(2)}) copy-start(bf16[2048,512]{1,0:T(8,128)(2,1)} %up_ref.1) | copy-start | bytes 6291460
  27.6 10.2 %copy-start.1 = (bf16[512,2048]{1,0:T(8,128)(2,1)S(1)}, bf16[512,2048]{1,0:T(8,128)(2,1)}, u32[]{:S(2)}) copy-start(bf16[512,2048]{1,0:T(8,128)(2,1)} %down_ref.1) | copy-start | bytes 6291460

commit v4 on v3

--- a/solution.py
+++ b/solution.py
@@ -125,38 +125,24 @@
 SHIFT = 64
 
 
-def prepare_kernel(
-    tokens_ref,
-    gain_ref,
-    beta_ref,
-    decay_ref,
-    scaled_ref,
-    squares_ref,
-    beta_out_ref,
-    decay_out_ref,
-    tokens_in_ref,
-    gain_in_ref,
-    sems,
-):
-    pairs = (
-        (tokens_ref, tokens_in_ref),
-        (gain_ref, gain_in_ref),
-        (beta_ref, beta_out_ref),
-        (decay_ref, decay_out_ref),
-    )
-    copies = [pltpu.make_async_copy(a, b, sems.at[n]) for n, (a, b) in enumerate(pairs)]
-    for copy in copies:
-        copy.start()
-    for copy in copies:
-        copy.wait()
-    tokens = tokens_in_ref[...].astype(F32)
-    scaled_ref[...] = (tokens * gain_in_ref[...].astype(F32)).astype(BF)
-    squares_ref[...] = tokens * tokens
+def place_kernel(out_ref):
+    lane = lax.broadcasted_iota(jnp.int32, out_ref.shape, 0)
+    head = lax.broadcasted_iota(jnp.int32, out_ref.shape, 1)
+    out_ref[...] = jnp.where(lane == head, 1.0, 0.0).astype(BF)
+
+
+def packet_line(s, j, seq, heads):
+    if j < 2 * heads:
+        return 2 * heads * s + j
+    if j < 3 * heads:
+        return 2 * heads * seq + heads * s + j - 2 * heads
+    return 3 * heads * seq + s
 
 
 def project_kernel(
+    place_ref,
     own_ref,
-    squares_ref,
+    own_gain_ref,
     other_ref,
     other_gain_ref,
     wq_ref,
@@ -174,7 +160,8 @@
 ):
     rows = own_ref.shape[0]
     first = lax.axis_index("tp") == 0
-    own_scaled = own_ref[...].astype(F32)
+    own = own_ref[...].astype(F32)
+    own_scaled = own * own_gain_ref[...].astype(F32)
     other = other_ref[...].astype(F32)
     other_scaled = other * other_gain_ref[...].astype(F32)
     scaled = jnp.concatenate(
@@ -190,12 +177,9 @@
         for h in range(heads):
             at = (p * heads + h) * rows
             res_ref[at : at + rows, :] = product[:, h * LANES : (h + 1) * LANES]
-    at = lax.broadcasted_iota(jnp.int32, (LANES, heads), 0)
-    head = lax.broadcasted_iota(jnp.int32, (LANES, heads), 1)
-    place_beta = jnp.where(at == head, 1.0, 0.0).astype(BF)
-    place_decay = jnp.where(at == head + heads, 1.0, 0.0).astype(BF)
-    gate_weights = (dot(place_beta, wb_ref[...]) + dot(place_decay, wd_ref[...])).astype(BF)
-    squares = jnp.sum(squares_ref[...] + other * other, axis=1, keepdims=True)
+    gate_weights = dot(place_ref[:, :heads], wb_ref[...])
+    gate_weights = (gate_weights + dot(place_ref[:, heads:], wd_ref[...])).astype(BF)
+    squares = jnp.sum(own * own + other * other, axis=1, keepdims=True)
     lanes = lax.broadcasted_iota(jnp.int32, (rows, LANES), 1)
     gates = lax.dot_general(
         scaled, gate_weights, (((1,), (1,)), ((), ())), preferred_element_type=F32
@@ -207,9 +191,8 @@
     packet = out_ref.shape[0] // n_kv
     for s in range(seq):
         for j in range(per_seq):
-            pack_ref[pl.ds(s * per_seq + j, n_kv, packet), :] = res_ref[
-                pl.ds(j * rows + s, n_kv, seq), :
-            ]
+            line = packet_line(s, j, seq, heads)
+            pack_ref[pl.ds(line, n_kv, packet), :] = res_ref[pl.ds(j * rows + s, n_kv, seq), :]
     for j in range(seq * per_seq, packet):
         pack_ref[pl.ds(j, n_kv, packet), :] = jnp.zeros((n_kv, LANES), F32)
     out_ref[...] = pack_ref[...].astype(BF)
@@ -229,48 +212,60 @@
     heads,
     model,
 ):
-    per_seq = 3 * heads + 1
     packet = got_ref.shape[0] // n_kv
     total = got_ref[:packet].astype(F32)
     for d in range(1, n_kv):
         total = total + got_ref[d * packet : (d + 1) * packet].astype(F32)
+    pair = 2 * heads
+    stack = total[: pair * seq]
+    columns = stack.T
+    lengths = jnp.sum(stack * stack, axis=1, keepdims=True)
+    first = 3 * heads * seq
+    start = first - first % 8
+    small = total[start:]
+    small = small + pltpu.roll(small, LANES - SHIFT, 1)
+    inverses = lax.rsqrt(small[:, pair : pair + 1] / model + 1e-06)
     lane = lax.broadcasted_iota(jnp.int32, (1, LANES), 1)
     rate = jnp.zeros((1, LANES), F32)
     for h in range(heads):
         rate = jnp.where(lane == heads + h, decay_log_ref[:, h : h + 1], rate)
-    rate = jnp.exp(rate)
-    betas, keeps, values, rows = [], [], [], []
-    for s in range(seq):
-        base = s * per_seq
-        small = total[base + 3 * heads : base + per_seq]
-        small = small + pltpu.roll(small, LANES - SHIFT, 1)
-        inverse = lax.rsqrt(small[:, 2 * heads : 2 * heads + 1] / model + 1e-06)
-        gates = inverse * small
-        betas.append(jax.nn.sigmoid(gates))
-        soft = jnp.maximum(gates, 0.0) + jnp.log1p(jnp.exp(-jnp.abs(gates)))
-        keeps.append(jnp.exp(-rate * soft))
-        query = inverse * total[base : base + heads]
-        key = inverse * total[base + heads : base + 2 * heads]
-        values.append(inverse * total[base + 2 * heads : base + 3 * heads])
-        rows.append(query * lax.rsqrt(jnp.sum(query * query, axis=1, keepdims=True) + 1e-06))
-        rows.append(key * lax.rsqrt(jnp.sum(key * key, axis=1, keepdims=True) + 1e-06))
-    count = 2 * heads * seq
-    padded = -(-count // 8) * 8
-    if padded > count:
-        rows.append(jnp.zeros((padded - count, LANES), F32))
-    columns = jnp.concatenate(rows, axis=0).T
+    gates = inverses * small
+    betas = jax.nn.sigmoid(gates)
+    soft = jnp.maximum(gates, 0.0) + jnp.log1p(jnp.exp(-jnp.abs(gates)))
+    keeps = jnp.exp(-jnp.exp(rate) * soft)
+    row = lax.broadcasted_iota(jnp.int32, (pair, LANES), 0)
+    at_lane = lax.broadcasted_iota(jnp.int32, (pair, LANES), 1)
+    head = jnp.where(row < heads, row, row - heads)
     reads = []
     for s in range(seq):
+        line = first - start + s
+        inverse = inverses[line : line + 1]
+        beta = jnp.where(at_lane == head, betas[line : line + 1], 0.0)
+        beta = jnp.sum(beta, axis=1, keepdims=True)
+        keep = jnp.where(at_lane == head + heads, keeps[line : line + 1], 0.0)
+        keep = jnp.sum(keep, axis=1, keepdims=True)
+        vectors = stack[pair * s : pair * (s + 1)]
+        length = lengths[pair * s : pair * (s + 1)]
+        scale = inverse * lax.rsqrt(inverse * inverse * length + 1e-06)
+        high = vectors.astype(BF)
+        low = (vectors - high.astype(F32)).astype(BF)
+        parts = jnp.concatenate([high, low], axis=0)
+        found = jnp.zeros((pair, LANES), F32)
         for h in range(heads):
-            at = 2 * s * heads + h
-            qcol = columns[:, at : at + 1]
-            kcol = columns[:, at + heads : at + heads + 1]
-            kept = state_ref[s, h] * keeps[s][:, heads + h : heads + h + 1]
-            predicted = jnp.sum(kept * kcol, axis=0, keepdims=True)
-            change = betas[s][:, h : h + 1] * (values[s][h : h + 1] - predicted)
-            new = kept + kcol * change
-            new_ref[s, h] = new
-            reads.append(jnp.sum(new * qcol, axis=0, keepdims=True))
+            block = state_ref[s, h]
+            near = block.astype(BF)
+            rest = (block - near.astype(F32)).astype(BF)
+            both = jnp.dot(parts, near, preferred_element_type=F32)
+            both = both + jnp.dot(parts, rest, preferred_element_type=F32)
+            found = jnp.where(head == h, both[:pair] + both[pair:], found)
+        found = found * (keep * scale)
+        value = inverse * total[pair * seq + heads * s : pair * seq + heads * (s + 1)]
+        change = (beta[:heads] * scale[heads:]) * (value - found[heads:])
+        cross = jnp.sum(vectors[:heads] * vectors[heads:], axis=1, keepdims=True)
+        reads.append(found[:heads] + (scale[:heads] * cross) * change)
+        for h in range(heads):
+            kcol = columns[:, pair * s + heads + h : pair * s + heads + h + 1]
+            new_ref[s, h] = keep[h : h + 1] * state_ref[s, h] + kcol * change[h : h + 1]
     read = jnp.concatenate(reads, axis=0) / jnp.sqrt(jnp.float32(LANES))
     normed = (
         read
@@ -325,14 +320,19 @@
     state_ref,
     out_ref,
     new_ref,
-    sem,
+    sems,
     *,
     gain_line,
     model,
     n_tp,
 ):
-    copy = pltpu.make_async_copy(state_ref, new_ref, sem)
-    copy.start()
+    copies = [
+        pltpu.make_async_copy(state_ref.at[n, m], new_ref.at[n, m], sems.at[n, m])
+        for n in range(state_ref.shape[0])
+        for m in range(state_ref.shape[1])
+    ]
+    for copy in copies:
+        copy.start()
     n_all, rows, width = got_ref.shape
     n_kv = n_all // n_tp
     lines = gains_ref.shape[0] // n_all
@@ -353,7 +353,8 @@
     for at in range(n_all):
         d = (at % n_tp) * n_kv + at // n_tp
         out_ref[d] = down[:, at * width : (at + 1) * width].astype(BF)
-    copy.wait()
+    for copy in copies:
+        copy.wait()
 
 
 def fused(
@@ -393,33 +394,20 @@
     other_tokens = lax.ppermute(tokens, "tp", swap)
     other_gain = lax.ppermute(gain_row, "tp", swap)
     hbm = pl.BlockSpec(memory_space=pltpu.HBM)
-    in_hbm = functools.partial(pltpu.with_memory_space_constraint, memory_space=pltpu.HBM)
     other_out = lax.ppermute(w_out, "tp", swap)
-    beta_rows, decay_rows = w_beta.T, w_decay.T
-    own_scaled, squares, beta_rows, decay_rows = pl.pallas_call(
-        prepare_kernel,
-        out_shape=(
-            shape(tokens.shape, BF),
-            shape(tokens.shape, F32),
-            shape(beta_rows.shape, BF),
-            shape(decay_rows.shape, BF),
-        ),
-        in_specs=[hbm] * 4,
-        out_specs=(vmem,) * 4,
-        scratch_shapes=[
-            pltpu.VMEM(tokens.shape, BF),
-            pltpu.VMEM(gain_row.shape, BF),
-            pltpu.SemaphoreType.DMA((4,)),
-        ],
-        name="prepare",
+    place = pl.pallas_call(
+        place_kernel,
+        out_shape=shape((LANES, 2 * heads), BF),
+        out_specs=vmem,
+        name="place",
         cost_estimate=cost,
         compiler_params=params,
-    )(in_hbm(tokens), in_hbm(gain_row), in_hbm(beta_rows), in_hbm(decay_rows))
+    )()
 
     sent = pl.pallas_call(
         functools.partial(project_kernel, n_kv=n_kv, seq=seq, heads=heads),
         out_shape=shape((n_kv * packet, LANES), BF),
-        in_specs=[vmem] * 9,
+        in_specs=[vmem] * 10,
         out_specs=vmem,
         scratch_shapes=[
             pltpu.VMEM((per_seq * rows, LANES), F32),
@@ -428,7 +416,18 @@
         name="project",
         cost_estimate=cost,
         compiler_params=params,
-    )(own_scaled, squares, other_tokens, other_gain, w_query, w_key, w_value, beta_rows, decay_rows)
+    )(
+        place,
+        tokens,
+        gain_row,
+        other_tokens,
+        other_gain,
+        w_query,
+        w_key,
+        w_value,
+        w_beta.T,
+        w_decay.T,
+    )
     sent, other_out = lax.optimization_barrier((sent, other_out))
     got = lax.all_to_all(sent.reshape(n_kv, packet, LANES), "kv", 0, 0, tiled=False)
     spread, new_state = pl.pallas_call(
@@ -460,7 +459,7 @@
         out_shape=(shape((n_all, rows, width), BF), shape(state.shape, F32)),
         in_specs=[vmem] * 5,
         out_specs=(vmem, hbm),
-        scratch_shapes=[pltpu.SemaphoreType.DMA(())],
+        scratch_shapes=[pltpu.SemaphoreType.DMA((seq, heads))],
         name="feed",
         compiler_params=params,
     )(got2, got, w_up, w_down, new_state)

time: 49.6 us -> 49.2 us (level)
  Pallas kernels: 3.8 us -> 2.49 us
  waiting for transfers between devices: 0.01 us -> 0.86 us
    pallas_call x1, Pallas kernels: 0.84 us -> 0.01 us  [fused(): pl.pallas_call(place_kernel, out_shape=shape((LANES, 2 * heads), BF), out...]
  transfers between devices with their start and end apart: 3 -> 3, of which waited for: 0 -> 2; matrix products, arithmetic and copies ran while one was open for 0% -> 0% of each run, Pallas kernels for 3% -> 1%
where the time goes in v4:
time: 49.2 us; the launch traced here: 48.9 us
  blocking collectives  43 us (87%)
  Pallas kernels  2.49 us (5%)
  starting transfers between devices  1.07 us (2%)
  waiting for transfers between devices  0.86 us (2%)
  between operations  0.81 us (2%)
  other arithmetic  0.62 us (1%)
    all_to_all x1, blocking collectives, fused(): lax.all_to_all(sent.reshape(n_kv, packet, LANES), 'kv', 0, 0, tiled=False)  13.9 us
    all_to_all x1, blocking collectives, fused(): got2 = lax.all_to_all(spread, axes, 0, 0, tiled=False)  10 us
    all_to_all x1, blocking collectives, fused(): got3 = lax.all_to_all(down, axes, 0, 0, tiled=False)  9.77 us
    all_to_all x1, blocking collectives, fused(): lax.all_to_all(spread, axes, 0, 0, tiled=False)  9.31 us
    pallas_call x1, Pallas kernels, fused(): pl.pallas_call(functools.partial(feed_kernel, gain_line=seq * heads, mode...  1.03 us
  transfers between devices with their start and end apart: 3, of which 2 were waited for; matrix products, arithmetic and copies ran while one was open for 0% of the time, Pallas kernels for 1%

profile of v4, /device:TPU:0, one launch (start us, length us, event | category | flops | bytes accessed | tf_op | source)
XLA Modules:
  0.0 48.9 jit_solution(7530945557069499492)
XLA Ops:
  0.6 0.0 copy-start.3
  0.6 0.0 copy-start.4
  0.7 0.0 copy-start.5
  0.7 0.0 copy-start.7
  0.7 0.0 copy-start.8
  0.7 0.0 copy-start.9
  0.7 0.0 copy-start.10
  0.7 0.6 %collective-permute-start.1 = (bf16[1,128]{1,0:T(2,128)(2,1)}, bf16[1,128]{1,0:T(2,128)(2,1)S(1)}, u32[]{:S(2)}, u32[]{:S(2)}) collective-permute-start(bf16[1,128]{1,0:T(2,128)(2,1)} %bitcast.15), channel_id=1, source_target_pairs={{0,1},{1,0},{2,3},{3,2},{4,5},{5,4},{6,7},{7,6},{8,9},{9,8},{10,11... | collective-permute-start | bytes 776 | tf_op jit(solution)/shard_map/ppermute | solution.py:395
  1.3 0.1 collective-permute-start
  1.3 0.4 collective-permute-start.2
  1.8 0.4 collective-permute-done.1.other_gain_ref
  2.2 0.4 collective-permute-done.other_ref
  2.6 0.0 copy-done.3
  2.6 0.0 copy-done.4
  2.6 0.0 copy-done.5
  2.7 0.0 copy-done.7
  2.7 0.0 copy-done.8
  2.7 0.0 copy-done.9
  2.7 0.0 copy-done.10
  2.7 0.0 copy-start.2
  2.7 0.0 copy-start.11
  2.7 0.0 copy-start.12
  2.7 0.0 copy-start.13
  2.7 0.5 %project.1 = bf16[320,128]{1,0:T(8,128)(2,1)S(1)} custom-call(bf16[128,8]{1,0:T(8,128)(2,1)S(1)} %place.1.place_ref, bf16[24,128]{1,0:T(8,128)(2,1)S(1)} %copy-done.7, bf16[1,128]{1,0:T(2,128)(2,1)S(1)} %bitcast.16, bf16[24,128]{1,0:T(8,128)(2,1)S(1)} %collective-permute-done.other_ref, bf16[1,128]{1,0:T(2,128)(2,1)S(1)} %collective-permute-done.1.other_gain_ref, ...), custom_call_target="tpu_custom_call" | custom-call | flops 4000000000 | bytes 8000000 | tf_op jit(solution)/shard_map/project/pallas_call | solution.py:407
  3.2 0.0 collective-permute-done.2.other_ref
  3.2 13.9 %all_to_all.20 = bf16[8,40,128]{2,1,0:T(8,128)(2,1)S(1)} all-to-all(bf16[8,40,128]{2,1,0:T(8,128)(2,1)S(1)} %bitcast.11), channel_id=1, replica_groups=mesh['dp'=2,'kv'=8,'tp'=2] {'kv'}, dimensions={0} | all-to-all | bytes 163840 | tf_op jit(solution)/shard_map/all_to_all | solution.py:432
  17.1 0.0 copy-done.2
  17.1 0.0 copy-done.11
  17.1 0.0 copy-done.12
  17.1 0.0 copy-done.13
  17.2 0.0 copy-start.6
  17.2 0.8 %delta.1 = (bf16[16,16,128]{2,1,0:T(8,128)(2,1)S(1)}, f32[3,4,128,128]{3,2,1,0:T(8,128)S(1)}) custom-call(bf16[320,128]{1,0:T(8,128)(2,1)S(1)} %bitcast.12, f32[3,4,128,128]{3,2,1,0:T(8,128)S(1)} %copy-done.2, f32[1,4]{1,0:T(1,128)S(1)} %bitcast.17, bf16[1,128]{1,0:T(2,128)(2,1)S(1)} %bitcast.18, bf16[1,128]{1,0:T(2,128)(2,1)S(1)} %bitcast.19), custom_call_target="tpu_custom_call" | custom-call | flops 4000000000 | bytes 8000000 | tf_op jit(solution)/shard_map/delta/pallas_call | solution.py:433
  17.9 9.3 %all_to_all.21 = bf16[16,16,128]{2,1,0:T(8,128)(2,1)S(1)} all-to-all(bf16[16,16,128]{2,1,0:T(8,128)(2,1)S(1)} %get-tuple-element.11), channel_id=1, replica_groups=mesh['dp'=2,'kv'=8,'tp'=2] {'tp','kv'}, dimensions={0} | all-to-all | bytes 131072 | tf_op jit(solution)/shard_map/all_to_all | solution.py:442
  27.2 0.0 copy-done.6
  27.2 0.0 copy-start
  27.2 0.0 copy-start.1
  27.2 0.2 mix.1
  27.4 10.0 %all_to_all.22.got_ref = bf16[16,24,128]{2,1,0:T(8,128)(2,1)S(1)} all-to-all(bf16[16,24,128]{2,1,0:T(8,128)(2,1)S(1)} %get-tuple-element.14), channel_id=1, replica_groups=mesh['dp'=2,'kv'=8,'tp'=2] {'tp','kv'}, dimensions={0} | all-to-all | bytes 196608 | tf_op jit(solution)/shard_map/all_to_all | solution.py:456
  37.5 0.0 copy-done
  37.5 0.0 copy-done.1
  37.5 1.0 %feed.1 = (bf16[16,24,128]{2,1,0:T(8,128)(2,1)S(1)}, f32[3,4,128,128]{3,2,1,0:T(8,128)}) custom-call(bf16[16,24,128]{2,1,0:T(8,128)(2,1)S(1)} %all_to_all.22.got_ref, bf16[256,128]{1,0:T(8,128)(2,1)S(1)} %bitcast.10, bf16[2048,512]{1,0:T(8,128)(2,1)S(1)} %copy-done, bf16[512,2048]{1,0:T(8,128)(2,1)S(1)} %copy-done.1, ...), custom_call_target="tpu_custom_call" | custom-call | tf_op jit(solution)/shard_map/feed/pallas_call | solution.py:457
  38.5 9.8 %all_to_all.23 = bf16[16,24,128]{2,1,0:T(8,128)(2,1)S(1)} all-to-all(bf16[16,24,128]{2,1,0:T(8,128)(2,1)S(1)} %get-tuple-element.16), channel_id=1, replica_groups=mesh['dp'=2,'kv'=8,'tp'=2] {'tp','kv'}, dimensions={0} | all-to-all | bytes 196608 | tf_op jit(solution)/shard_map/all_to_all | solution.py:466
  48.3 0.6 %add_convert_fusion = bf16[24,128]{1,0:T(8,128)(2,1)} fusion(f32[24,128]{1,0:T(8,128)S(1)} %convert_reduce_fusion, bf16[24,128]{1,0:T(8,128)(2,1)S(1)} %get-tuple-element.13), kind=kLoop, calls=%fused_computation.1 | loop fusion | flops 9216 | bytes 24576 | tf_op jit(solution)/shard_map/convert_element_type | solution.py:467
  (2 shorter events, 0.0 us)
Async XLA Ops:
  0.6 2.0 %copy-start.3 = (bf16[256,512]{1,0:T(8,128)(2,1)S(1)}, bf16[256,512]{1,0:T(8,128)(2,1)}, u32[]{:S(2)}) copy-start(bf16[256,512]{1,0:T(8,128)(2,1)} %wq_ref.1) | copy-start | bytes 786436
  0.6 2.0 %copy-start.4 = (bf16[256,512]{1,0:T(8,128)(2,1)S(1)}, bf16[256,512]{1,0:T(8,128)(2,1)}, u32[]{:S(2)}) copy-start(bf16[256,512]{1,0:T(8,128)(2,1)} %wk_ref.1) | copy-start | bytes 786436
  0.7 2.0 %copy-start.5 = (bf16[256,512]{1,0:T(8,128)(2,1)S(1)}, bf16[256,512]{1,0:T(8,128)(2,1)}, u32[]{:S(2)}) copy-start(bf16[256,512]{1,0:T(8,128)(2,1)} %wv_ref.1) | copy-start | bytes 786436
  0.7 2.0 %copy-start.7 = (bf16[24,128]{1,0:T(8,128)(2,1)S(1)}, bf16[24,128]{1,0:T(8,128)(2,1)}, u32[]{:S(2)}) copy-start(bf16[24,128]{1,0:T(8,128)(2,1)} %tokens_ref.1) | copy-start | bytes 18436
  0.7 2.0 %copy-start.8 = (bf16[256,4]{0,1:T(4,128)(2,1)S(1)}, bf16[256,4]{0,1:T(4,128)(2,1)}, u32[]{:S(2)}) copy-start(bf16[256,4]{0,1:T(4,128)(2,1)} %param.20) | copy-start | bytes 6148
  0.7 2.0 %copy-start.9 = (bf16[256,4]{0,1:T(4,128)(2,1)S(1)}, bf16[256,4]{0,1:T(4,128)(2,1)}, u32[]{:S(2)}) copy-start(bf16[256,4]{0,1:T(4,128)(2,1)} %param.21) | copy-start | bytes 6148
  0.7 2.0 %copy-start.10 = (bf16[128]{0:T(256)(128)(2,1)S(1)}, bf16[128]{0:T(256)(128)(2,1)}, u32[]{:S(2)}) copy-start(bf16[128]{0:T(256)(128)(2,1)} %param.16) | copy-start | bytes 772
  0.7 1.5 %collective-permute-start.1 = (bf16[1,128]{1,0:T(2,128)(2,1)}, bf16[1,128]{1,0:T(2,128)(2,1)S(1)}, u32[]{:S(2)}, u32[]{:S(2)}) collective-permute-start(bf16[1,128]{1,0:T(2,128)(2,1)} %bitcast.15), channel_id=1, source_target_pairs={{0,1},{1,0},{2,3},{3,2},{4,5},{5,4},{6,7},{7,6},{8,9},{9,8},{10,11... | collective-permute-start | bytes 776 | tf_op jit(solution)/shard_map/ppermute | solution.py:395
  1.3 1.4 %collective-permute-start = (bf16[24,128]{1,0:T(8,128)(2,1)}, bf16[24,128]{1,0:T(8,128)(2,1)S(1)}, u32[]{:S(2)}, u32[]{:S(2)}) collective-permute-start(bf16[24,128]{1,0:T(8,128)(2,1)} %tokens_ref.1), channel_id=1, source_target_pairs={{0,1},{1,0},{2,3},{3,2},{4,5},{5,4},{6,7},{7,6},{8,9},{9,8},{10,11... | collective-permute-start | bytes 18440 | tf_op jit(solution)/shard_map/ppermute | solution.py:394
  1.3 1.9 %collective-permute-start.2 = (bf16[512,256]{1,0:T(8,128)(2,1)}, bf16[512,256]{1,0:T(8,128)(2,1)S(1)}, u32[]{:S(2)}, u32[]{:S(2)}) collective-permute-start(bf16[512,256]{1,0:T(8,128)(2,1)} %own_ref.3), channel_id=1, source_target_pairs={{0,1},{1,0},{2,3},{3,2},{4,5},{5,4},{6,7},{7,6},{8,9},{9,8},{10,11... | collective-permute-start | bytes 786440 | tf_op jit(solution)/shard_map/ppermute | solution.py:397
  2.7 14.4 %copy-start.2 = (f32[3,4,128,128]{3,2,1,0:T(8,128)S(1)}, f32[3,4,128,128]{3,2,1,0:T(8,128)}, u32[]{:S(2)}) copy-start(f32[3,4,128,128]{3,2,1,0:T(8,128)} %state_ref.1) | copy-start | bytes 2359300
  2.7 14.4 %copy-start.11 = (f32[4]{0:T(128)S(1)}, f32[4]{0:T(128)}, u32[]{:S(2)}) copy-start(f32[4]{0:T(128)} %param.22) | copy-start | bytes 52
  2.7 14.4 %copy-start.12 = (bf16[128]{0:T(256)(128)(2,1)S(1)}, bf16[128]{0:T(256)(128)(2,1)}, u32[]{:S(2)}) copy-start(bf16[128]{0:T(256)(128)(2,1)} %param.23) | copy-start | bytes 772
  2.7 14.4 %copy-start.13 = (bf16[128]{0:T(256)(128)(2,1)S(1)}, bf16[128]{0:T(256)(128)(2,1)}, u32[]{:S(2)}) copy-start(bf16[128]{0:T(256)(128)(2,1)} %param.25) | copy-start | bytes 772
  17.2 10.1 %copy-start.6 = (bf16[512,256]{1,0:T(8,128)(2,1)S(1)}, bf16[512,256]{1,0:T(8,128)(2,1)}, u32[]{:S(2)}) copy-start(bf16[512,256]{1,0:T(8,128)(2,1)} %own_ref.3) | copy-start | bytes 786436
  27.2 10.2 %copy-start = (bf16[2048,512]{1,0:T(8,128)(2,1)S(1)}, bf16[2048,512]{1,0:T(8,128)(2,1)}, u32[]{:S(2)}) copy-start(bf16[2048,512]{1,0:T(8,128)(2,1)} %up_ref.1) | copy-start | bytes 6291460
  27.2 10.2 %copy-start.1 = (bf16[512,2048]{1,0:T(8,128)(2,1)S(1)}, bf16[512,2048]{1,0:T(8,128)(2,1)}, u32[]{:S(2)}) copy-start(bf16[512,2048]{1,0:T(8,128)(2,1)} %down_ref.1) | copy-start | bytes 6291460

commit v5 on v4

--- a/solution.py
+++ b/solution.py
@@ -151,7 +151,7 @@
     wb_ref,
     wd_ref,
     out_ref,
-    res_ref,
+    tokens_ref,
     pack_ref,
     *,
     n_kv,
@@ -160,40 +160,43 @@
 ):
     rows = own_ref.shape[0]
     first = lax.axis_index("tp") == 0
-    own = own_ref[...].astype(F32)
-    own_scaled = own * own_gain_ref[...].astype(F32)
-    other = other_ref[...].astype(F32)
-    other_scaled = other * other_gain_ref[...].astype(F32)
-    scaled = jnp.concatenate(
-        [
-            jnp.where(first, own_scaled, other_scaled),
-            jnp.where(first, other_scaled, own_scaled),
-        ],
-        axis=1,
-    ).astype(BF)
+    own_rows = own_ref[...].astype(F32)
+    other_rows = other_ref[...].astype(F32)
+    tokens_ref[:rows, :] = jnp.where(first, own_rows, other_rows)
+    tokens_ref[rows:, :] = jnp.where(first, other_rows, own_rows)
+    own_gain = own_gain_ref[...].astype(F32)
+    other_gain = other_gain_ref[...].astype(F32)
+    gains = jnp.where(first, own_gain, other_gain), jnp.where(first, other_gain, own_gain)
+    halves, squares = [], 0.0
+    for t, gain in enumerate(gains):
+        half = [tokens_ref[pl.ds(t * rows + s, n_kv, seq), :] for s in range(seq)]
+        half = jnp.concatenate(half, axis=0)
+        squares = squares + half * half
+        halves.append((half * gain).astype(BF))
+    squares = jnp.sum(squares, axis=1, keepdims=True)
+    scaled = jnp.concatenate(halves, axis=1)
     dot = functools.partial(jnp.dot, preferred_element_type=F32)
+    gate_weights = dot(place_ref[:, :heads], wb_ref[...])
+    gate_weights = (gate_weights + dot(place_ref[:, heads:], wd_ref[...])).astype(BF)
+    gates = lax.dot_general(
+        scaled, gate_weights, (((1,), (1,)), ((), ())), preferred_element_type=F32
+    )
+    lanes = lax.broadcasted_iota(jnp.int32, (rows, LANES), 1)
+    small = gates + jnp.where(lanes == 2 * heads, squares, 0.0)
+    high = small.astype(BF).astype(F32)
+    packet = out_ref.shape[0] // n_kv
+
+    def pack(j, block):
+        for s in range(seq):
+            line = packet_line(s, j, seq, heads)
+            pack_ref[pl.ds(line, n_kv, packet), :] = block[s * n_kv : (s + 1) * n_kv]
+
     for p, weight_ref in enumerate((wq_ref, wk_ref, wv_ref)):
         product = dot(scaled, weight_ref[...])
         for h in range(heads):
-            at = (p * heads + h) * rows
-            res_ref[at : at + rows, :] = product[:, h * LANES : (h + 1) * LANES]
-    gate_weights = dot(place_ref[:, :heads], wb_ref[...])
-    gate_weights = (gate_weights + dot(place_ref[:, heads:], wd_ref[...])).astype(BF)
-    squares = jnp.sum(own * own + other * other, axis=1, keepdims=True)
-    lanes = lax.broadcasted_iota(jnp.int32, (rows, LANES), 1)
-    gates = lax.dot_general(
-        scaled, gate_weights, (((1,), (1,)), ((), ())), preferred_element_type=F32
-    )
-    small = gates + jnp.where(lanes == 2 * heads, squares, 0.0)
-    high = small.astype(BF).astype(F32)
-    res_ref[3 * heads * rows :, :] = high + pltpu.roll(small - high, SHIFT, 1)
-    per_seq = 3 * heads + 1
-    packet = out_ref.shape[0] // n_kv
-    for s in range(seq):
-        for j in range(per_seq):
-            line = packet_line(s, j, seq, heads)
-            pack_ref[pl.ds(line, n_kv, packet), :] = res_ref[pl.ds(j * rows + s, n_kv, seq), :]
-    for j in range(seq * per_seq, packet):
+            pack(p * heads + h, product[:, h * LANES : (h + 1) * LANES])
+    pack(3 * heads, high + pltpu.roll(small - high, SHIFT, 1))
+    for j in range(seq * (3 * heads + 1), packet):
         pack_ref[pl.ds(j, n_kv, packet), :] = jnp.zeros((n_kv, LANES), F32)
     out_ref[...] = pack_ref[...].astype(BF)
 
@@ -282,9 +285,23 @@
 
 
 def mix_kernel(
-    got_ref, tokens_ref, own_ref, other_ref, spread_ref, resid_ref, rows_ref, mixed_ref, *, n_kv, n_tp, seq, heads
+    got_ref,
+    tokens_ref,
+    other_tokens_ref,
+    own_ref,
+    other_ref,
+    spread_ref,
+    resid_ref,
+    rows_ref,
+    mixed_ref,
+    *,
+    n_kv,
+    n_tp,
+    seq,
+    heads,
 ):
     lines = got_ref.shape[0] // (n_kv * n_tp)
+    rows, width = tokens_ref.shape
     rows_ref[...] = got_ref[...].astype(F32)
     dot = functools.partial(jnp.dot, preferred_element_type=F32)
     halves = []
@@ -296,19 +313,24 @@
             ]
             blocks.append(jnp.concatenate(parts, axis=0))
         halves.append(jnp.concatenate(blocks, axis=1))
-    tp_at = lax.axis_index("tp")
-    width = resid_ref.shape[1]
-    cols = pl.ds(pl.multiple_of(tp_at * width, width), width)
-    first = tp_at == 0
+    first = lax.axis_index("tp") == 0
     own = jnp.where(first, halves[0], halves[1]).astype(BF)
     other = jnp.where(first, halves[1], halves[0]).astype(BF)
-    mixed = dot(own, own_ref[:, cols]).astype(BF).astype(F32)
-    mixed = mixed + dot(other, other_ref[:, cols]).astype(BF).astype(F32)
-    for s in range(seq):
-        mixed_ref[pl.ds(s, n_kv, seq), :] = mixed[s * n_kv : (s + 1) * n_kv]
-    resid = (tokens_ref[...].astype(F32) + mixed_ref[...]).astype(BF)
-    resid_ref[...] = resid
-    for d in range(spread_ref.shape[0]):
+    mixed = dot(own, own_ref[...]).astype(BF).astype(F32)
+    mixed = mixed + dot(other, other_ref[...]).astype(BF).astype(F32)
+    own_tokens = tokens_ref[...].astype(F32)
+    other_tokens = other_tokens_ref[...].astype(F32)
+    tokens = jnp.where(first, own_tokens, other_tokens), jnp.where(first, other_tokens, own_tokens)
+    resids = []
+    for t in range(n_tp):
+        for s in range(seq):
+            mixed_ref[pl.ds(t * rows + s, n_kv, seq), :] = mixed[
+                s * n_kv : (s + 1) * n_kv, t * width : (t + 1) * width
+            ]
+        resids.append(tokens[t] + mixed_ref[t * rows : (t + 1) * rows, :])
+    resid_ref[...] = jnp.where(first, resids[0], resids[1]).astype(BF)
+    resid = jnp.concatenate(resids, axis=1).astype(BF)
+    for d in range(n_kv):
         spread_ref[d] = resid
 
 
@@ -333,17 +355,19 @@
     ]
     for copy in copies:
         copy.start()
-    n_all, rows, width = got_ref.shape
+    n_all, rows, width = out_ref.shape
     n_kv = n_all // n_tp
     lines = gains_ref.shape[0] // n_all
-    squares = jnp.zeros((rows, width), F32)
+    squares = jnp.zeros((rows, n_tp * width), F32)
     blocks = []
-    for at in range(n_all):
-        d = (at % n_tp) * n_kv + at // n_tp
+    for d in range(n_kv):
         block = got_ref[d].astype(F32)
         squares = squares + block * block
-        gain = gains_ref[d * lines : (d + 1) * lines].astype(F32)[gain_line : gain_line + 1]
-        blocks.append((block * gain).astype(BF))
+        starts = [(t * n_kv + d) * lines for t in range(n_tp)]
+        gain = [
+            gains_ref[at : at + lines].astype(F32)[gain_line : gain_line + 1] for at in starts
+        ]
+        blocks.append((block * jnp.concatenate(gain, axis=1)).astype(BF))
     inverse = lax.rsqrt(jnp.sum(squares, axis=1, keepdims=True) / model + 1e-06)
     scaled = jnp.concatenate(blocks, axis=1)
     up = jnp.dot(scaled, up_ref[...], preferred_element_type=F32) * inverse
@@ -410,7 +434,7 @@
         in_specs=[vmem] * 10,
         out_specs=vmem,
         scratch_shapes=[
-            pltpu.VMEM((per_seq * rows, LANES), F32),
+            pltpu.VMEM((n_tp * rows, LANES), F32),
             pltpu.VMEM((n_kv * packet, LANES), F32),
         ],
         name="project",
@@ -442,18 +466,18 @@
     got = lax.all_to_all(spread, axes, 0, 0, tiled=False).reshape(n_all * lines, LANES)
     spread, resid = pl.pallas_call(
         functools.partial(mix_kernel, n_kv=n_kv, n_tp=n_tp, seq=seq, heads=heads),
-        out_shape=(shape((n_all, rows, width), BF), shape((rows, width), BF)),
-        in_specs=[vmem] * 4,
+        out_shape=(shape((n_kv, rows, n_tp * width), BF), shape((rows, width), BF)),
+        in_specs=[vmem] * 5,
         out_specs=(vmem, vmem),
         scratch_shapes=[
             pltpu.VMEM((n_all * lines, LANES), F32),
-            pltpu.VMEM((rows, width), F32),
+            pltpu.VMEM((n_tp * rows, width), F32),
         ],
         name="mix",
         cost_estimate=cost,
         compiler_params=params,
-    )(got, tokens, w_out, other_out)
-    got2 = lax.all_to_all(spread, axes, 0, 0, tiled=False)
+    )(got, tokens, other_tokens, w_out, other_out)
+    got2 = lax.all_to_all(spread, "kv", 0, 0, tiled=False)
     down, new_state = pl.pallas_call(
         functools.partial(feed_kernel, gain_line=seq * heads, model=model, n_tp=n_tp),
         out_shape=(shape((n_all, rows, width), BF), shape(state.shape, F32)),

time: 49.2 us -> 48.9 us (level)
  no operation moved by 1% of the time
where the time goes in v5:
time: 48.9 us; the launch traced here: 48.7 us
  blocking collectives  42.7 us (87%)
  Pallas kernels  2.49 us (5%)
  starting transfers between devices  1.07 us (2%)
  waiting for transfers between devices  0.86 us (2%)
  between operations  0.82 us (2%)
  other arithmetic  0.62 us (1%)
    all_to_all x1, blocking collectives, fused(): lax.all_to_all(sent.reshape(n_kv, packet, LANES), 'kv', 0, 0, tiled=False)  13.9 us
    all_to_all x1, blocking collectives, fused(): got2 = lax.all_to_all(spread, 'kv', 0, 0, tiled=False)  9.78 us
    all_to_all x1, blocking collectives, fused(): got3 = lax.all_to_all(down, axes, 0, 0, tiled=False)  9.77 us
    all_to_all x1, blocking collectives, fused(): lax.all_to_all(spread, axes, 0, 0, tiled=False)  9.31 us
    pallas_call x1, Pallas kernels, fused(): pl.pallas_call(functools.partial(feed_kernel, gain_line=seq * heads, mode...  1.03 us
  transfers between devices with their start and end apart: 3, of which 2 were waited for; matrix products, arithmetic and copies ran while one was open for 0% of the time, Pallas kernels for 1%

profile of v5, /device:TPU:0, one launch (start us, length us, event | category | flops | bytes accessed | tf_op | source)
XLA Modules:
  0.0 48.7 jit_solution(13615917309948043291)
XLA Ops:
  0.6 0.0 copy-start.3
  0.6 0.0 copy-start.4
  0.7 0.0 copy-start.5
  0.7 0.0 copy-start.7
  0.7 0.0 copy-start.8
  0.7 0.0 copy-start.9
  0.7 0.0 copy-start.10
  0.7 0.6 %collective-permute-start.1 = (bf16[1,128]{1,0:T(2,128)(2,1)}, bf16[1,128]{1,0:T(2,128)(2,1)S(1)}, u32[]{:S(2)}, u32[]{:S(2)}) collective-permute-start(bf16[1,128]{1,0:T(2,128)(2,1)} %bitcast.15), channel_id=1, source_target_pairs={{0,1},{1,0},{2,3},{3,2},{4,5},{5,4},{6,7},{7,6},{8,9},{9,8},{10,11... | collective-permute-start | bytes 776 | tf_op jit(solution)/shard_map/ppermute | solution.py:419
  1.3 0.1 collective-permute-start
  1.3 0.4 collective-permute-start.2
  1.8 0.4 collective-permute-done.1.other_gain_ref
  2.2 0.4 collective-permute-done.other_ref.other_tokens_ref
  2.6 0.0 copy-done.3
  2.6 0.0 copy-done.4
  2.6 0.0 copy-done.5
  2.7 0.0 copy-done.7
  2.7 0.0 copy-done.8
  2.7 0.0 copy-done.9
  2.7 0.0 copy-done.10
  2.7 0.0 copy-start.2
  2.7 0.0 copy-start.11
  2.7 0.0 copy-start.12
  2.7 0.0 copy-start.13
  2.7 0.5 project.1
  3.2 0.0 collective-permute-done.2.other_ref
  3.2 13.9 %all_to_all.20 = bf16[8,40,128]{2,1,0:T(8,128)(2,1)S(1)} all-to-all(bf16[8,40,128]{2,1,0:T(8,128)(2,1)S(1)} %bitcast.11), channel_id=1, replica_groups=mesh['dp'=2,'kv'=8,'tp'=2] {'kv'}, dimensions={0} | all-to-all | bytes 163840 | tf_op jit(solution)/shard_map/all_to_all | solution.py:456
  17.1 0.0 copy-done.2
  17.1 0.0 copy-done.11
  17.1 0.0 copy-done.12
  17.1 0.0 copy-done.13
  17.2 0.0 copy-start.6
  17.2 0.8 %delta.1 = (bf16[16,16,128]{2,1,0:T(8,128)(2,1)S(1)}, f32[3,4,128,128]{3,2,1,0:T(8,128)S(1)}) custom-call(bf16[320,128]{1,0:T(8,128)(2,1)S(1)} %bitcast.12, f32[3,4,128,128]{3,2,1,0:T(8,128)S(1)} %copy-done.2, f32[1,4]{1,0:T(1,128)S(1)} %bitcast.17, bf16[1,128]{1,0:T(2,128)(2,1)S(1)} %bitcast.18, bf16[1,128]{1,0:T(2,128)(2,1)S(1)} %bitcast.19), custom_call_target="tpu_custom_call" | custom-call | flops 4000000000 | bytes 8000000 | tf_op jit(solution)/shard_map/delta/pallas_call | solution.py:457
  17.9 9.3 %all_to_all.21 = bf16[16,16,128]{2,1,0:T(8,128)(2,1)S(1)} all-to-all(bf16[16,16,128]{2,1,0:T(8,128)(2,1)S(1)} %get-tuple-element.11), channel_id=1, replica_groups=mesh['dp'=2,'kv'=8,'tp'=2] {'tp','kv'}, dimensions={0} | all-to-all | bytes 131072 | tf_op jit(solution)/shard_map/all_to_all | solution.py:466
  27.2 0.0 copy-done.6
  27.2 0.0 copy-start
  27.2 0.0 copy-start.1
  27.2 0.2 mix.1
  27.5 9.8 %all_to_all.22.got_ref = bf16[8,24,256]{2,1,0:T(8,128)(2,1)S(1)} all-to-all(bf16[8,24,256]{2,1,0:T(8,128)(2,1)S(1)} %get-tuple-element.14), channel_id=1, replica_groups=mesh['dp'=2,'kv'=8,'tp'=2] {'kv'}, dimensions={0} | all-to-all | bytes 196608 | tf_op jit(solution)/shard_map/all_to_all | solution.py:480
  37.2 0.0 copy-done
  37.2 0.0 copy-done.1
  37.2 1.0 %feed.1 = (bf16[16,24,128]{2,1,0:T(8,128)(2,1)S(1)}, f32[3,4,128,128]{3,2,1,0:T(8,128)}) custom-call(bf16[8,24,256]{2,1,0:T(8,128)(2,1)S(1)} %all_to_all.22.got_ref, bf16[256,128]{1,0:T(8,128)(2,1)S(1)} %bitcast.10, bf16[2048,512]{1,0:T(8,128)(2,1)S(1)} %copy-done, bf16[512,2048]{1,0:T(8,128)(2,1)S(1)} %copy-done.1, ...), custom_call_target="tpu_custom_call" | custom-call | tf_op jit(solution)/shard_map/feed/pallas_call | solution.py:481
  38.3 9.8 %all_to_all.23 = bf16[16,24,128]{2,1,0:T(8,128)(2,1)S(1)} all-to-all(bf16[16,24,128]{2,1,0:T(8,128)(2,1)S(1)} %get-tuple-element.16), channel_id=1, replica_groups=mesh['dp'=2,'kv'=8,'tp'=2] {'tp','kv'}, dimensions={0} | all-to-all | bytes 196608 | tf_op jit(solution)/shard_map/all_to_all | solution.py:490
  48.1 0.6 %add_convert_fusion = bf16[24,128]{1,0:T(8,128)(2,1)} fusion(f32[24,128]{1,0:T(8,128)S(1)} %convert_reduce_fusion, bf16[24,128]{1,0:T(8,128)(2,1)S(1)} %get-tuple-element.13), kind=kLoop, calls=%fused_computation.1 | loop fusion | flops 9216 | bytes 24576 | tf_op jit(solution)/shard_map/convert_element_type | solution.py:491
  (2 shorter events, 0.0 us)
Async XLA Ops:
  0.6 2.0 %copy-start.3 = (bf16[256,512]{1,0:T(8,128)(2,1)S(1)}, bf16[256,512]{1,0:T(8,128)(2,1)}, u32[]{:S(2)}) copy-start(bf16[256,512]{1,0:T(8,128)(2,1)} %wq_ref.1) | copy-start | bytes 786436
  0.6 2.0 %copy-start.4 = (bf16[256,512]{1,0:T(8,128)(2,1)S(1)}, bf16[256,512]{1,0:T(8,128)(2,1)}, u32[]{:S(2)}) copy-start(bf16[256,512]{1,0:T(8,128)(2,1)} %wk_ref.1) | copy-start | bytes 786436
  0.7 2.0 %copy-start.5 = (bf16[256,512]{1,0:T(8,128)(2,1)S(1)}, bf16[256,512]{1,0:T(8,128)(2,1)}, u32[]{:S(2)}) copy-start(bf16[256,512]{1,0:T(8,128)(2,1)} %wv_ref.1) | copy-start | bytes 786436
  0.7 2.0 %copy-start.7 = (bf16[24,128]{1,0:T(8,128)(2,1)S(1)}, bf16[24,128]{1,0:T(8,128)(2,1)}, u32[]{:S(2)}) copy-start(bf16[24,128]{1,0:T(8,128)(2,1)} %tokens_ref.1) | copy-start | bytes 18436
  0.7 2.0 %copy-start.8 = (bf16[256,4]{0,1:T(4,128)(2,1)S(1)}, bf16[256,4]{0,1:T(4,128)(2,1)}, u32[]{:S(2)}) copy-start(bf16[256,4]{0,1:T(4,128)(2,1)} %param.20) | copy-start | bytes 6148
  0.7 2.0 %copy-start.9 = (bf16[256,4]{0,1:T(4,128)(2,1)S(1)}, bf16[256,4]{0,1:T(4,128)(2,1)}, u32[]{:S(2)}) copy-start(bf16[256,4]{0,1:T(4,128)(2,1)} %param.21) | copy-start | bytes 6148
  0.7 2.0 %copy-start.10 = (bf16[128]{0:T(256)(128)(2,1)S(1)}, bf16[128]{0:T(256)(128)(2,1)}, u32[]{:S(2)}) copy-start(bf16[128]{0:T(256)(128)(2,1)} %param.16) | copy-start | bytes 772
  0.7 1.5 %collective-permute-start.1 = (bf16[1,128]{1,0:T(2,128)(2,1)}, bf16[1,128]{1,0:T(2,128)(2,1)S(1)}, u32[]{:S(2)}, u32[]{:S(2)}) collective-permute-start(bf16[1,128]{1,0:T(2,128)(2,1)} %bitcast.15), channel_id=1, source_target_pairs={{0,1},{1,0},{2,3},{3,2},{4,5},{5,4},{6,7},{7,6},{8,9},{9,8},{10,11... | collective-permute-start | bytes 776 | tf_op jit(solution)/shard_map/ppermute | solution.py:419
  1.3 1.4 %collective-permute-start = (bf16[24,128]{1,0:T(8,128)(2,1)}, bf16[24,128]{1,0:T(8,128)(2,1)S(1)}, u32[]{:S(2)}, u32[]{:S(2)}) collective-permute-start(bf16[24,128]{1,0:T(8,128)(2,1)} %tokens_ref.1), channel_id=1, source_target_pairs={{0,1},{1,0},{2,3},{3,2},{4,5},{5,4},{6,7},{7,6},{8,9},{9,8},{10,11... | collective-permute-start | bytes 18440 | tf_op jit(solution)/shard_map/ppermute | solution.py:418
  1.3 1.9 %collective-permute-start.2 = (bf16[512,256]{1,0:T(8,128)(2,1)}, bf16[512,256]{1,0:T(8,128)(2,1)S(1)}, u32[]{:S(2)}, u32[]{:S(2)}) collective-permute-start(bf16[512,256]{1,0:T(8,128)(2,1)} %own_ref.3), channel_id=1, source_target_pairs={{0,1},{1,0},{2,3},{3,2},{4,5},{5,4},{6,7},{7,6},{8,9},{9,8},{10,11... | collective-permute-start | bytes 786440 | tf_op jit(solution)/shard_map/ppermute | solution.py:421
  2.7 14.4 %copy-start.2 = (f32[3,4,128,128]{3,2,1,0:T(8,128)S(1)}, f32[3,4,128,128]{3,2,1,0:T(8,128)}, u32[]{:S(2)}) copy-start(f32[3,4,128,128]{3,2,1,0:T(8,128)} %state_ref.1) | copy-start | bytes 2359300
  2.7 14.4 %copy-start.11 = (f32[4]{0:T(128)S(1)}, f32[4]{0:T(128)}, u32[]{:S(2)}) copy-start(f32[4]{0:T(128)} %param.22) | copy-start | bytes 52
  2.7 14.4 %copy-start.12 = (bf16[128]{0:T(256)(128)(2,1)S(1)}, bf16[128]{0:T(256)(128)(2,1)}, u32[]{:S(2)}) copy-start(bf16[128]{0:T(256)(128)(2,1)} %param.23) | copy-start | bytes 772
  2.7 14.4 %copy-start.13 = (bf16[128]{0:T(256)(128)(2,1)S(1)}, bf16[128]{0:T(256)(128)(2,1)}, u32[]{:S(2)}) copy-start(bf16[128]{0:T(256)(128)(2,1)} %param.25) | copy-start | bytes 772
  17.2 10.1 %copy-start.6 = (bf16[512,256]{1,0:T(8,128)(2,1)S(1)}, bf16[512,256]{1,0:T(8,128)(2,1)}, u32[]{:S(2)}) copy-start(bf16[512,256]{1,0:T(8,128)(2,1)} %own_ref.3) | copy-start | bytes 786436
  27.2 10.0 %copy-start = (bf16[2048,512]{1,0:T(8,128)(2,1)S(1)}, bf16[2048,512]{1,0:T(8,128)(2,1)}, u32[]{:S(2)}) copy-start(bf16[2048,512]{1,0:T(8,128)(2,1)} %up_ref.1) | copy-start | bytes 6291460
  27.2 10.0 %copy-start.1 = (bf16[512,2048]{1,0:T(8,128)(2,1)S(1)}, bf16[512,2048]{1,0:T(8,128)(2,1)}, u32[]{:S(2)}) copy-start(bf16[512,2048]{1,0:T(8,128)(2,1)} %down_ref.1) | copy-start | bytes 6291460

commit v6 on v5

--- a/solution.py
+++ b/solution.py
@@ -123,6 +123,20 @@
 
 LANES = 128
 SHIFT = 64
+ORDERS = {
+    8: (4, 5, 6, 0, 7, 1, 3, 2),
+    16: (11, 8, 13, 3, 9, 0, 15, 1, 10, 5, 6, 2, 12, 14, 7, 4),
+}
+
+
+def ring(count):
+    return ORDERS.get(count, tuple(range(count)))
+
+
+def exchange(blocks, axes):
+    return lax.all_to_all(
+        blocks, axes, 0, 0, tiled=False, axis_index_groups=[list(ring(blocks.shape[0]))]
+    )
 
 
 def place_kernel(out_ref):
@@ -198,7 +212,8 @@
     pack(3 * heads, high + pltpu.roll(small - high, SHIFT, 1))
     for j in range(seq * (3 * heads + 1), packet):
         pack_ref[pl.ds(j, n_kv, packet), :] = jnp.zeros((n_kv, LANES), F32)
-    out_ref[...] = pack_ref[...].astype(BF)
+    for k, d in enumerate(ring(n_kv)):
+        out_ref[k * packet : (k + 1) * packet] = pack_ref[d * packet : (d + 1) * packet].astype(BF)
 
 
 def delta_kernel(
@@ -302,7 +317,9 @@
 ):
     lines = got_ref.shape[0] // (n_kv * n_tp)
     rows, width = tokens_ref.shape
-    rows_ref[...] = got_ref[...].astype(F32)
+    for k, member in enumerate(ring(n_kv * n_tp)):
+        at = ((member % n_tp) * n_kv + member // n_tp) * lines
+        rows_ref[at : at + lines] = got_ref[k * lines : (k + 1) * lines].astype(F32)
     dot = functools.partial(jnp.dot, preferred_element_type=F32)
     halves = []
     for t in range(n_tp):
@@ -361,9 +378,9 @@
     squares = jnp.zeros((rows, n_tp * width), F32)
     blocks = []
     for d in range(n_kv):
-        block = got_ref[d].astype(F32)
+        block = got_ref[ring(n_kv).index(d)].astype(F32)
         squares = squares + block * block
-        starts = [(t * n_kv + d) * lines for t in range(n_tp)]
+        starts = [ring(n_all).index(d * n_tp + t) * lines for t in range(n_tp)]
         gain = [
             gains_ref[at : at + lines].astype(F32)[gain_line : gain_line + 1] for at in starts
         ]
@@ -374,9 +391,8 @@
     up = jnp.maximum(up, 0.0)
     act = (up * up).astype(BF)
     down = jnp.dot(act, down_ref[...], preferred_element_type=F32)
-    for at in range(n_all):
-        d = (at % n_tp) * n_kv + at // n_tp
-        out_ref[d] = down[:, at * width : (at + 1) * width].astype(BF)
+    for k, at in enumerate(ring(n_all)):
+        out_ref[k] = down[:, at * width : (at + 1) * width].astype(BF)
     for copy in copies:
         copy.wait()
 
@@ -407,7 +423,7 @@
     per_seq = 3 * heads + 1
     packet = -(-seq * per_seq // 8) * 8
     lines = -(-(seq * heads + 1) // 8) * 8
-    axes = ("tp", "kv")
+    axes = ("kv", "tp")
     swap = [(i, n_tp - 1 - i) for i in range(n_tp)]
     shape = jax.ShapeDtypeStruct
     vmem = pl.BlockSpec(memory_space=pltpu.VMEM)
@@ -453,7 +469,7 @@
         w_decay.T,
     )
     sent, other_out = lax.optimization_barrier((sent, other_out))
-    got = lax.all_to_all(sent.reshape(n_kv, packet, LANES), "kv", 0, 0, tiled=False)
+    got = exchange(sent.reshape(n_kv, packet, LANES), "kv")
     spread, new_state = pl.pallas_call(
         functools.partial(delta_kernel, n_kv=n_kv, seq=seq, heads=heads, model=model),
         out_shape=(shape((n_all, lines, LANES), BF), shape(state.shape, F32)),
@@ -463,7 +479,7 @@
         cost_estimate=cost,
         compiler_params=params,
     )(got.reshape(n_kv * packet, LANES), state, decay_log[None, :], head_gain[None, :], ff_gain[None, :])
-    got = lax.all_to_all(spread, axes, 0, 0, tiled=False).reshape(n_all * lines, LANES)
+    got = exchange(spread, axes).reshape(n_all * lines, LANES)
     spread, resid = pl.pallas_call(
         functools.partial(mix_kernel, n_kv=n_kv, n_tp=n_tp, seq=seq, heads=heads),
         out_shape=(shape((n_kv, rows, n_tp * width), BF), shape((rows, width), BF)),
@@ -477,7 +493,7 @@
         cost_estimate=cost,
         compiler_params=params,
     )(got, tokens, other_tokens, w_out, other_out)
-    got2 = lax.all_to_all(spread, "kv", 0, 0, tiled=False)
+    got2 = exchange(spread, "kv")
     down, new_state = pl.pallas_call(
         functools.partial(feed_kernel, gain_line=seq * heads, model=model, n_tp=n_tp),
         out_shape=(shape((n_all, rows, width), BF), shape(state.shape, F32)),
@@ -487,7 +503,7 @@
         name="feed",
         compiler_params=params,
     )(got2, got, w_up, w_down, new_state)
-    got3 = lax.all_to_all(down, axes, 0, 0, tiled=False)
+    got3 = exchange(down, axes)
     output = (resid.astype(F32) + jnp.sum(got3.astype(F32), axis=0)).astype(BF)
     return (output, new_state)
 

time: 48.9 us -> 45 us (0.920)
  blocking collectives: 42.7 us -> 38.7 us
    all_to_all x4, blocking collectives: 42.7 us -> 38.7 us  [exchange(): lax.all_to_all(blocks, axes, 0, 0, tiled=False, axis_index_groups=[list(r...]
where the time goes in v6:
time: 45 us; the launch traced here: 44.8 us
  blocking collectives  38.7 us (86%)
  Pallas kernels  2.65 us (6%)
  starting transfers between devices  1.07 us (2%)
  waiting for transfers between devices  0.86 us (2%)
  between operations  0.82 us (2%)
  other arithmetic  0.62 us (1%)
    all_to_all x4, blocking collectives, exchange(): lax.all_to_all(blocks, axes, 0, 0, tiled=False, axis_index_groups=[list(r...  38.7 us
    pallas_call x1, Pallas kernels, fused(): pl.pallas_call(functools.partial(feed_kernel, gain_line=seq * heads, mode...  1.19 us
  transfers between devices with their start and end apart: 3, of which 2 were waited for; matrix products, arithmetic and copies ran while one was open for 0% of the time, Pallas kernels for 1%

profile of v6, /device:TPU:0, one launch (start us, length us, event | category | flops | bytes accessed | tf_op | source)
XLA Modules:
  0.0 44.8 jit_solution(8980714072720318057)
XLA Ops:
  0.6 0.0 copy-start.3
  0.6 0.0 copy-start.4
  0.7 0.0 copy-start.5
  0.7 0.0 copy-start.7
  0.7 0.0 copy-start.8
  0.7 0.0 copy-start.9
  0.7 0.0 copy-start.10
  0.7 0.6 %collective-permute-start.1 = (bf16[1,128]{1,0:T(2,128)(2,1)}, bf16[1,128]{1,0:T(2,128)(2,1)S(1)}, u32[]{:S(2)}, u32[]{:S(2)}) collective-permute-start(bf16[1,128]{1,0:T(2,128)(2,1)} %bitcast.15), channel_id=1, source_target_pairs={{0,1},{1,0},{2,3},{3,2},{4,5},{5,4},{6,7},{7,6},{8,9},{9,8},{10,11... | collective-permute-start | bytes 776 | tf_op jit(solution)/shard_map/ppermute | solution.py:435
  1.3 0.1 collective-permute-start
  1.3 0.4 collective-permute-start.2
  1.8 0.4 collective-permute-done.1.other_gain_ref
  2.2 0.4 collective-permute-done.other_ref.other_tokens_ref
  2.6 0.0 copy-done.3
  2.6 0.0 copy-done.4
  2.6 0.0 copy-done.5
  2.7 0.0 copy-done.7
  2.7 0.0 copy-done.8
  2.7 0.0 copy-done.9
  2.7 0.0 copy-done.10
  2.7 0.0 copy-start.2
  2.7 0.0 copy-start.11
  2.7 0.0 copy-start.12
  2.7 0.0 copy-start.13
  2.7 0.5 %project.1 = bf16[320,128]{1,0:T(8,128)(2,1)S(1)} custom-call(bf16[128,8]{1,0:T(8,128)(2,1)S(1)} %place.1.place_ref, bf16[24,128]{1,0:T(8,128)(2,1)S(1)} %copy-done.7, bf16[1,128]{1,0:T(2,128)(2,1)S(1)} %bitcast.16, bf16[24,128]{1,0:T(8,128)(2,1)S(1)} %collective-permute-done.other_ref.other_tokens_ref, ...), custom_call_target="tpu_custom_call" | custom-call | flops 4000000000 | bytes 8000000 | tf_op jit(solution)/shard_map/project/pallas_call | solution.py:447
  3.2 0.0 collective-permute-done.2.other_ref
  3.2 11.7 %all_to_all.20 = bf16[8,40,128]{2,1,0:T(8,128)(2,1)S(1)} all-to-all(bf16[8,40,128]{2,1,0:T(8,128)(2,1)S(1)} %bitcast.11), channel_id=1, replica_groups={{8,10,12,0,14,2,6,4},{9,11,13,1,15,3,7,5},{24,26,28,16,30,18,22,20},{25..., dimensions={0} | all-to-all | bytes 163840 | tf_op jit(solution)/shard_map/all_to_all | solution.py:137
  14.9 0.0 copy-done.2
  14.9 0.0 copy-done.11
  14.9 0.0 copy-done.12
  14.9 0.0 copy-done.13
  14.9 0.0 copy-start.6
  14.9 0.8 %delta.1 = (bf16[16,16,128]{2,1,0:T(8,128)(2,1)S(1)}, f32[3,4,128,128]{3,2,1,0:T(8,128)S(1)}) custom-call(bf16[320,128]{1,0:T(8,128)(2,1)S(1)} %bitcast.12, f32[3,4,128,128]{3,2,1,0:T(8,128)S(1)} %copy-done.2, f32[1,4]{1,0:T(1,128)S(1)} %bitcast.17, bf16[1,128]{1,0:T(2,128)(2,1)S(1)} %bitcast.18, bf16[1,128]{1,0:T(2,128)(2,1)S(1)} %bitcast.19), custom_call_target="tpu_custom_call" | custom-call | flops 4000000000 | bytes 8000000 | tf_op jit(solution)/shard_map/delta/pallas_call | solution.py:473
  15.7 8.5 %all_to_all.21 = bf16[16,16,128]{2,1,0:T(8,128)(2,1)S(1)} all-to-all(bf16[16,16,128]{2,1,0:T(8,128)(2,1)S(1)} %get-tuple-element.11), channel_id=1, replica_groups={{11,8,13,3,9,0,15,1,10,5,6,2,12,14,7,4},{27,24,29,19,25,16,31,17,26,21,..., dimensions={0} | all-to-all | bytes 131072 | tf_op jit(solution)/shard_map/all_to_all | solution.py:137
  24.2 0.0 copy-done.6
  24.2 0.0 copy-start
  24.2 0.0 copy-start.1
  24.2 0.2 mix.1
  24.4 9.5 %all_to_all.22.got_ref = bf16[8,24,256]{2,1,0:T(8,128)(2,1)S(1)} all-to-all(bf16[8,24,256]{2,1,0:T(8,128)(2,1)S(1)} %get-tuple-element.14), channel_id=1, replica_groups={{8,10,12,0,14,2,6,4},{9,11,13,1,15,3,7,5},{24,26,28,16,30,18,22,20},{25..., dimensions={0} | all-to-all | bytes 196608 | tf_op jit(solution)/shard_map/all_to_all | solution.py:137
  34.0 0.0 copy-done
  34.0 0.0 copy-done.1
  34.0 1.2 %feed.1 = (bf16[16,24,128]{2,1,0:T(8,128)(2,1)S(1)}, f32[3,4,128,128]{3,2,1,0:T(8,128)}) custom-call(bf16[8,24,256]{2,1,0:T(8,128)(2,1)S(1)} %all_to_all.22.got_ref, bf16[256,128]{1,0:T(8,128)(2,1)S(1)} %bitcast.10, bf16[2048,512]{1,0:T(8,128)(2,1)S(1)} %copy-done, bf16[512,2048]{1,0:T(8,128)(2,1)S(1)} %copy-done.1, ...), custom_call_target="tpu_custom_call" | custom-call | tf_op jit(solution)/shard_map/feed/pallas_call | solution.py:497
  35.2 9.0 %all_to_all.23 = bf16[16,24,128]{2,1,0:T(8,128)(2,1)S(1)} all-to-all(bf16[16,24,128]{2,1,0:T(8,128)(2,1)S(1)} %get-tuple-element.16), channel_id=1, replica_groups={{11,8,13,3,9,0,15,1,10,5,6,2,12,14,7,4},{27,24,29,19,25,16,31,17,26,21,..., dimensions={0} | all-to-all | bytes 196608 | tf_op jit(solution)/shard_map/all_to_all | solution.py:137
  44.2 0.6 %add_convert_fusion = bf16[24,128]{1,0:T(8,128)(2,1)} fusion(f32[24,128]{1,0:T(8,128)S(1)} %convert_reduce_fusion, bf16[24,128]{1,0:T(8,128)(2,1)S(1)} %get-tuple-element.13), kind=kLoop, calls=%fused_computation.1 | loop fusion | flops 9216 | bytes 24576 | tf_op jit(solution)/shard_map/convert_element_type | solution.py:507
  (2 shorter events, 0.0 us)
Async XLA Ops:
  0.6 2.0 %copy-start.3 = (bf16[256,512]{1,0:T(8,128)(2,1)S(1)}, bf16[256,512]{1,0:T(8,128)(2,1)}, u32[]{:S(2)}) copy-start(bf16[256,512]{1,0:T(8,128)(2,1)} %wq_ref.1) | copy-start | bytes 786436
  0.6 2.0 %copy-start.4 = (bf16[256,512]{1,0:T(8,128)(2,1)S(1)}, bf16[256,512]{1,0:T(8,128)(2,1)}, u32[]{:S(2)}) copy-start(bf16[256,512]{1,0:T(8,128)(2,1)} %wk_ref.1) | copy-start | bytes 786436
  0.7 2.0 %copy-start.5 = (bf16[256,512]{1,0:T(8,128)(2,1)S(1)}, bf16[256,512]{1,0:T(8,128)(2,1)}, u32[]{:S(2)}) copy-start(bf16[256,512]{1,0:T(8,128)(2,1)} %wv_ref.1) | copy-start | bytes 786436
  0.7 2.0 %copy-start.7 = (bf16[24,128]{1,0:T(8,128)(2,1)S(1)}, bf16[24,128]{1,0:T(8,128)(2,1)}, u32[]{:S(2)}) copy-start(bf16[24,128]{1,0:T(8,128)(2,1)} %tokens_ref.1) | copy-start | bytes 18436
  0.7 2.0 %copy-start.8 = (bf16[256,4]{0,1:T(4,128)(2,1)S(1)}, bf16[256,4]{0,1:T(4,128)(2,1)}, u32[]{:S(2)}) copy-start(bf16[256,4]{0,1:T(4,128)(2,1)} %param.20) | copy-start | bytes 6148
  0.7 2.0 %copy-start.9 = (bf16[256,4]{0,1:T(4,128)(2,1)S(1)}, bf16[256,4]{0,1:T(4,128)(2,1)}, u32[]{:S(2)}) copy-start(bf16[256,4]{0,1:T(4,128)(2,1)} %param.21) | copy-start | bytes 6148
  0.7 2.0 %copy-start.10 = (bf16[128]{0:T(256)(128)(2,1)S(1)}, bf16[128]{0:T(256)(128)(2,1)}, u32[]{:S(2)}) copy-start(bf16[128]{0:T(256)(128)(2,1)} %param.16) | copy-start | bytes 772
  0.7 1.5 %collective-permute-start.1 = (bf16[1,128]{1,0:T(2,128)(2,1)}, bf16[1,128]{1,0:T(2,128)(2,1)S(1)}, u32[]{:S(2)}, u32[]{:S(2)}) collective-permute-start(bf16[1,128]{1,0:T(2,128)(2,1)} %bitcast.15), channel_id=1, source_target_pairs={{0,1},{1,0},{2,3},{3,2},{4,5},{5,4},{6,7},{7,6},{8,9},{9,8},{10,11... | collective-permute-start | bytes 776 | tf_op jit(solution)/shard_map/ppermute | solution.py:435
  1.3 1.4 %collective-permute-start = (bf16[24,128]{1,0:T(8,128)(2,1)}, bf16[24,128]{1,0:T(8,128)(2,1)S(1)}, u32[]{:S(2)}, u32[]{:S(2)}) collective-permute-start(bf16[24,128]{1,0:T(8,128)(2,1)} %tokens_ref.1), channel_id=1, source_target_pairs={{0,1},{1,0},{2,3},{3,2},{4,5},{5,4},{6,7},{7,6},{8,9},{9,8},{10,11... | collective-permute-start | bytes 18440 | tf_op jit(solution)/shard_map/ppermute | solution.py:434
  1.3 1.9 %collective-permute-start.2 = (bf16[512,256]{1,0:T(8,128)(2,1)}, bf16[512,256]{1,0:T(8,128)(2,1)S(1)}, u32[]{:S(2)}, u32[]{:S(2)}) collective-permute-start(bf16[512,256]{1,0:T(8,128)(2,1)} %own_ref.3), channel_id=1, source_target_pairs={{0,1},{1,0},{2,3},{3,2},{4,5},{5,4},{6,7},{7,6},{8,9},{9,8},{10,11... | collective-permute-start | bytes 786440 | tf_op jit(solution)/shard_map/ppermute | solution.py:437
  2.7 12.2 %copy-start.2 = (f32[3,4,128,128]{3,2,1,0:T(8,128)S(1)}, f32[3,4,128,128]{3,2,1,0:T(8,128)}, u32[]{:S(2)}) copy-start(f32[3,4,128,128]{3,2,1,0:T(8,128)} %state_ref.1) | copy-start | bytes 2359300
  2.7 12.2 %copy-start.11 = (f32[4]{0:T(128)S(1)}, f32[4]{0:T(128)}, u32[]{:S(2)}) copy-start(f32[4]{0:T(128)} %param.22) | copy-start | bytes 52
  2.7 12.2 %copy-start.12 = (bf16[128]{0:T(256)(128)(2,1)S(1)}, bf16[128]{0:T(256)(128)(2,1)}, u32[]{:S(2)}) copy-start(bf16[128]{0:T(256)(128)(2,1)} %param.23) | copy-start | bytes 772
  2.7 12.2 %copy-start.13 = (bf16[128]{0:T(256)(128)(2,1)S(1)}, bf16[128]{0:T(256)(128)(2,1)}, u32[]{:S(2)}) copy-start(bf16[128]{0:T(256)(128)(2,1)} %param.25) | copy-start | bytes 772
  14.9 9.3 %copy-start.6 = (bf16[512,256]{1,0:T(8,128)(2,1)S(1)}, bf16[512,256]{1,0:T(8,128)(2,1)}, u32[]{:S(2)}) copy-start(bf16[512,256]{1,0:T(8,128)(2,1)} %own_ref.3) | copy-start | bytes 786436
  24.2 9.8 %copy-start = (bf16[2048,512]{1,0:T(8,128)(2,1)S(1)}, bf16[2048,512]{1,0:T(8,128)(2,1)}, u32[]{:S(2)}) copy-start(bf16[2048,512]{1,0:T(8,128)(2,1)} %up_ref.1) | copy-start | bytes 6291460
  24.2 9.8 %copy-start.1 = (bf16[512,2048]{1,0:T(8,128)(2,1)S(1)}, bf16[512,2048]{1,0:T(8,128)(2,1)}, u32[]{:S(2)}) copy-start(bf16[512,2048]{1,0:T(8,128)(2,1)} %down_ref.1) | copy-start | bytes 6291460

commit v7 on v6

--- a/solution.py
+++ b/solution.py
@@ -124,19 +124,21 @@
 LANES = 128
 SHIFT = 64
 ORDERS = {
-    8: (4, 5, 6, 0, 7, 1, 3, 2),
+    8: (5, 7, 6, 4, 3, 1, 2, 0),
     16: (11, 8, 13, 3, 9, 0, 15, 1, 10, 5, 6, 2, 12, 14, 7, 4),
 }
 
 
-def ring(count):
-    return ORDERS.get(count, tuple(range(count)))
-
-
-def exchange(blocks, axes):
-    return lax.all_to_all(
-        blocks, axes, 0, 0, tiled=False, axis_index_groups=[list(ring(blocks.shape[0]))]
-    )
+FIRST = {8: (5, 7, 6, 4, 3, 1, 2, 0)}
+
+
+def ring(count, first=False):
+    return (FIRST if first else ORDERS).get(count, tuple(range(count)))
+
+
+def exchange(blocks, axes, first=False):
+    group = list(ring(blocks.shape[0], first))
+    return lax.all_to_all(blocks, axes, 0, 0, tiled=False, axis_index_groups=[group])
 
 
 def place_kernel(out_ref):
@@ -212,7 +214,7 @@
     pack(3 * heads, high + pltpu.roll(small - high, SHIFT, 1))
     for j in range(seq * (3 * heads + 1), packet):
         pack_ref[pl.ds(j, n_kv, packet), :] = jnp.zeros((n_kv, LANES), F32)
-    for k, d in enumerate(ring(n_kv)):
+    for k, d in enumerate(ring(n_kv, True)):
         out_ref[k * packet : (k + 1) * packet] = pack_ref[d * packet : (d + 1) * packet].astype(BF)
 
 
@@ -469,7 +471,7 @@
         w_decay.T,
     )
     sent, other_out = lax.optimization_barrier((sent, other_out))
-    got = exchange(sent.reshape(n_kv, packet, LANES), "kv")
+    got = exchange(sent.reshape(n_kv, packet, LANES), "kv", True)
     spread, new_state = pl.pallas_call(
         functools.partial(delta_kernel, n_kv=n_kv, seq=seq, heads=heads, model=model),
         out_shape=(shape((n_all, lines, LANES), BF), shape(state.shape, F32)),

time: 45 us -> 43.2 us (0.960)
  blocking collectives: 38.7 us -> 36.9 us
    all_to_all x4, blocking collectives: 38.7 us -> 36.9 us  [exchange(): lax.all_to_all(blocks, axes, 0, 0, tiled=False, axis_index_groups=[group])]
where the time goes in v7:
time: 43.2 us; the launch traced here: 43 us
  blocking collectives  36.9 us (85%)
  Pallas kernels  2.65 us (6%)
  starting transfers between devices  1.07 us (2%)
  waiting for transfers between devices  0.86 us (2%)
  between operations  0.82 us (2%)
  other arithmetic  0.62 us (1%)
    all_to_all x4, blocking collectives, exchange(): lax.all_to_all(blocks, axes, 0, 0, tiled=False, axis_index_groups=[group])  36.9 us
    pallas_call x1, Pallas kernels, fused(): pl.pallas_call(functools.partial(feed_kernel, gain_line=seq * heads, mode...  1.19 us
  transfers between devices with their start and end apart: 3, of which 2 were waited for; matrix products, arithmetic and copies ran while one was open for 0% of the time, Pallas kernels for 1%

profile of v7, /device:TPU:0, one launch (start us, length us, event | category | flops | bytes accessed | tf_op | source)
XLA Modules:
  0.0 43.0 jit_solution(8732032141628075407)
XLA Ops:
  0.6 0.0 copy-start.3
  0.6 0.0 copy-start.4
  0.7 0.0 copy-start.5
  0.7 0.0 copy-start.7
  0.7 0.0 copy-start.8
  0.7 0.0 copy-start.9
  0.7 0.0 copy-start.10
  0.7 0.6 %collective-permute-start.1 = (bf16[1,128]{1,0:T(2,128)(2,1)}, bf16[1,128]{1,0:T(2,128)(2,1)S(1)}, u32[]{:S(2)}, u32[]{:S(2)}) collective-permute-start(bf16[1,128]{1,0:T(2,128)(2,1)} %bitcast.15), channel_id=1, source_target_pairs={{0,1},{1,0},{2,3},{3,2},{4,5},{5,4},{6,7},{7,6},{8,9},{9,8},{10,11... | collective-permute-start | bytes 776 | tf_op jit(solution)/shard_map/ppermute | solution.py:437
  1.3 0.1 collective-permute-start
  1.3 0.4 %collective-permute-start.2 = (bf16[512,256]{1,0:T(8,128)(2,1)}, bf16[512,256]{1,0:T(8,128)(2,1)S(1)}, u32[]{:S(2)}, u32[]{:S(2)}) collective-permute-start(bf16[512,256]{1,0:T(8,128)(2,1)} %own_ref.3), channel_id=1, source_target_pairs={{0,1},{1,0},{2,3},{3,2},{4,5},{5,4},{6,7},{7,6},{8,9},{9,8},{10,11... | collective-permute-start | bytes 786440 | tf_op jit(solution)/shard_map/ppermute | solution.py:439
  1.8 0.4 collective-permute-done.1.other_gain_ref
  2.2 0.4 collective-permute-done.other_ref.other_tokens_ref
  2.6 0.0 copy-done.3
  2.6 0.0 copy-done.4
  2.6 0.0 copy-done.5
  2.7 0.0 copy-done.7
  2.7 0.0 copy-done.8
  2.7 0.0 copy-done.9
  2.7 0.0 copy-done.10
  2.7 0.0 copy-start.2
  2.7 0.0 copy-start.11
  2.7 0.0 copy-start.12
  2.7 0.0 copy-start.13
  2.7 0.5 %project.1 = bf16[320,128]{1,0:T(8,128)(2,1)S(1)} custom-call(bf16[128,8]{1,0:T(8,128)(2,1)S(1)} %place.1.place_ref, bf16[24,128]{1,0:T(8,128)(2,1)S(1)} %copy-done.7, bf16[1,128]{1,0:T(2,128)(2,1)S(1)} %bitcast.16, bf16[24,128]{1,0:T(8,128)(2,1)S(1)} %collective-permute-done.other_ref.other_tokens_ref, ...), custom_call_target="tpu_custom_call" | custom-call | flops 4000000000 | bytes 8000000 | tf_op jit(solution)/shard_map/project/pallas_call | solution.py:449
  3.2 0.0 collective-permute-done.2.other_ref
  3.2 11.1 %all_to_all.20 = bf16[8,40,128]{2,1,0:T(8,128)(2,1)S(1)} all-to-all(bf16[8,40,128]{2,1,0:T(8,128)(2,1)S(1)} %bitcast.11), channel_id=1, replica_groups={{10,14,12,8,6,2,4,0},{11,15,13,9,7,3,5,1},{26,30,28,24,22,18,20,16},{27..., dimensions={0} | all-to-all | bytes 163840 | tf_op jit(solution)/shard_map/all_to_all | solution.py:141
  14.3 0.0 copy-done.2
  14.3 0.0 copy-done.11
  14.3 0.0 copy-done.12
  14.3 0.0 copy-done.13
  14.3 0.0 copy-start.6
  14.4 0.8 %delta.1 = (bf16[16,16,128]{2,1,0:T(8,128)(2,1)S(1)}, f32[3,4,128,128]{3,2,1,0:T(8,128)S(1)}) custom-call(bf16[320,128]{1,0:T(8,128)(2,1)S(1)} %bitcast.12, f32[3,4,128,128]{3,2,1,0:T(8,128)S(1)} %copy-done.2, f32[1,4]{1,0:T(1,128)S(1)} %bitcast.17, bf16[1,128]{1,0:T(2,128)(2,1)S(1)} %bitcast.18, bf16[1,128]{1,0:T(2,128)(2,1)S(1)} %bitcast.19), custom_call_target="tpu_custom_call" | custom-call | flops 4000000000 | bytes 8000000 | tf_op jit(solution)/shard_map/delta/pallas_call | solution.py:475
  15.1 8.2 %all_to_all.21 = bf16[16,16,128]{2,1,0:T(8,128)(2,1)S(1)} all-to-all(bf16[16,16,128]{2,1,0:T(8,128)(2,1)S(1)} %get-tuple-element.11), channel_id=1, replica_groups={{11,8,13,3,9,0,15,1,10,5,6,2,12,14,7,4},{27,24,29,19,25,16,31,17,26,21,..., dimensions={0} | all-to-all | bytes 131072 | tf_op jit(solution)/shard_map/all_to_all | solution.py:141
  23.3 0.0 copy-done.6
  23.3 0.0 copy-start
  23.3 0.0 copy-start.1
  23.3 0.2 mix.1
  23.5 9.0 %all_to_all.22.got_ref = bf16[8,24,256]{2,1,0:T(8,128)(2,1)S(1)} all-to-all(bf16[8,24,256]{2,1,0:T(8,128)(2,1)S(1)} %get-tuple-element.14), channel_id=1, replica_groups={{10,14,12,8,6,2,4,0},{11,15,13,9,7,3,5,1},{26,30,28,24,22,18,20,16},{27..., dimensions={0} | all-to-all | bytes 196608 | tf_op jit(solution)/shard_map/all_to_all | solution.py:141
  32.6 0.0 copy-done
  32.6 0.0 copy-done.1
  32.6 1.2 %feed.1 = (bf16[16,24,128]{2,1,0:T(8,128)(2,1)S(1)}, f32[3,4,128,128]{3,2,1,0:T(8,128)}) custom-call(bf16[8,24,256]{2,1,0:T(8,128)(2,1)S(1)} %all_to_all.22.got_ref, bf16[256,128]{1,0:T(8,128)(2,1)S(1)} %bitcast.10, bf16[2048,512]{1,0:T(8,128)(2,1)S(1)} %copy-done, bf16[512,2048]{1,0:T(8,128)(2,1)S(1)} %copy-done.1, ...), custom_call_target="tpu_custom_call" | custom-call | tf_op jit(solution)/shard_map/feed/pallas_call | solution.py:499
  33.8 8.6 %all_to_all.23 = bf16[16,24,128]{2,1,0:T(8,128)(2,1)S(1)} all-to-all(bf16[16,24,128]{2,1,0:T(8,128)(2,1)S(1)} %get-tuple-element.16), channel_id=1, replica_groups={{11,8,13,3,9,0,15,1,10,5,6,2,12,14,7,4},{27,24,29,19,25,16,31,17,26,21,..., dimensions={0} | all-to-all | bytes 196608 | tf_op jit(solution)/shard_map/all_to_all | solution.py:141
  42.4 0.6 %add_convert_fusion = bf16[24,128]{1,0:T(8,128)(2,1)} fusion(f32[24,128]{1,0:T(8,128)S(1)} %convert_reduce_fusion, bf16[24,128]{1,0:T(8,128)(2,1)S(1)} %get-tuple-element.13), kind=kLoop, calls=%fused_computation.1 | loop fusion | flops 9216 | bytes 24576 | tf_op jit(solution)/shard_map/convert_element_type | solution.py:509
  (2 shorter events, 0.0 us)
Async XLA Ops:
  0.6 2.0 %copy-start.3 = (bf16[256,512]{1,0:T(8,128)(2,1)S(1)}, bf16[256,512]{1,0:T(8,128)(2,1)}, u32[]{:S(2)}) copy-start(bf16[256,512]{1,0:T(8,128)(2,1)} %wq_ref.1) | copy-start | bytes 786436
  0.6 2.0 %copy-start.4 = (bf16[256,512]{1,0:T(8,128)(2,1)S(1)}, bf16[256,512]{1,0:T(8,128)(2,1)}, u32[]{:S(2)}) copy-start(bf16[256,512]{1,0:T(8,128)(2,1)} %wk_ref.1) | copy-start | bytes 786436
  0.7 2.0 %copy-start.5 = (bf16[256,512]{1,0:T(8,128)(2,1)S(1)}, bf16[256,512]{1,0:T(8,128)(2,1)}, u32[]{:S(2)}) copy-start(bf16[256,512]{1,0:T(8,128)(2,1)} %wv_ref.1) | copy-start | bytes 786436
  0.7 2.0 %copy-start.7 = (bf16[24,128]{1,0:T(8,128)(2,1)S(1)}, bf16[24,128]{1,0:T(8,128)(2,1)}, u32[]{:S(2)}) copy-start(bf16[24,128]{1,0:T(8,128)(2,1)} %tokens_ref.1) | copy-start | bytes 18436
  0.7 2.0 %copy-start.8 = (bf16[256,4]{0,1:T(4,128)(2,1)S(1)}, bf16[256,4]{0,1:T(4,128)(2,1)}, u32[]{:S(2)}) copy-start(bf16[256,4]{0,1:T(4,128)(2,1)} %param.20) | copy-start | bytes 6148
  0.7 2.0 %copy-start.9 = (bf16[256,4]{0,1:T(4,128)(2,1)S(1)}, bf16[256,4]{0,1:T(4,128)(2,1)}, u32[]{:S(2)}) copy-start(bf16[256,4]{0,1:T(4,128)(2,1)} %param.21) | copy-start | bytes 6148
  0.7 2.0 %copy-start.10 = (bf16[128]{0:T(256)(128)(2,1)S(1)}, bf16[128]{0:T(256)(128)(2,1)}, u32[]{:S(2)}) copy-start(bf16[128]{0:T(256)(128)(2,1)} %param.16) | copy-start | bytes 772
  0.7 1.5 %collective-permute-start.1 = (bf16[1,128]{1,0:T(2,128)(2,1)}, bf16[1,128]{1,0:T(2,128)(2,1)S(1)}, u32[]{:S(2)}, u32[]{:S(2)}) collective-permute-start(bf16[1,128]{1,0:T(2,128)(2,1)} %bitcast.15), channel_id=1, source_target_pairs={{0,1},{1,0},{2,3},{3,2},{4,5},{5,4},{6,7},{7,6},{8,9},{9,8},{10,11... | collective-permute-start | bytes 776 | tf_op jit(solution)/shard_map/ppermute | solution.py:437
  1.3 1.4 %collective-permute-start = (bf16[24,128]{1,0:T(8,128)(2,1)}, bf16[24,128]{1,0:T(8,128)(2,1)S(1)}, u32[]{:S(2)}, u32[]{:S(2)}) collective-permute-start(bf16[24,128]{1,0:T(8,128)(2,1)} %tokens_ref.1), channel_id=1, source_target_pairs={{0,1},{1,0},{2,3},{3,2},{4,5},{5,4},{6,7},{7,6},{8,9},{9,8},{10,11... | collective-permute-start | bytes 18440 | tf_op jit(solution)/shard_map/ppermute | solution.py:436
  1.3 1.9 %collective-permute-start.2 = (bf16[512,256]{1,0:T(8,128)(2,1)}, bf16[512,256]{1,0:T(8,128)(2,1)S(1)}, u32[]{:S(2)}, u32[]{:S(2)}) collective-permute-start(bf16[512,256]{1,0:T(8,128)(2,1)} %own_ref.3), channel_id=1, source_target_pairs={{0,1},{1,0},{2,3},{3,2},{4,5},{5,4},{6,7},{7,6},{8,9},{9,8},{10,11... | collective-permute-start | bytes 786440 | tf_op jit(solution)/shard_map/ppermute | solution.py:439
  2.7 11.6 %copy-start.2 = (f32[3,4,128,128]{3,2,1,0:T(8,128)S(1)}, f32[3,4,128,128]{3,2,1,0:T(8,128)}, u32[]{:S(2)}) copy-start(f32[3,4,128,128]{3,2,1,0:T(8,128)} %state_ref.1) | copy-start | bytes 2359300
  2.7 11.6 %copy-start.11 = (f32[4]{0:T(128)S(1)}, f32[4]{0:T(128)}, u32[]{:S(2)}) copy-start(f32[4]{0:T(128)} %param.22) | copy-start | bytes 52
  2.7 11.6 %copy-start.12 = (bf16[128]{0:T(256)(128)(2,1)S(1)}, bf16[128]{0:T(256)(128)(2,1)}, u32[]{:S(2)}) copy-start(bf16[128]{0:T(256)(128)(2,1)} %param.23) | copy-start | bytes 772
  2.7 11.6 %copy-start.13 = (bf16[128]{0:T(256)(128)(2,1)S(1)}, bf16[128]{0:T(256)(128)(2,1)}, u32[]{:S(2)}) copy-start(bf16[128]{0:T(256)(128)(2,1)} %param.25) | copy-start | bytes 772
  14.3 9.0 %copy-start.6 = (bf16[512,256]{1,0:T(8,128)(2,1)S(1)}, bf16[512,256]{1,0:T(8,128)(2,1)}, u32[]{:S(2)}) copy-start(bf16[512,256]{1,0:T(8,128)(2,1)} %own_ref.3) | copy-start | bytes 786436
  23.3 9.2 %copy-start = (bf16[2048,512]{1,0:T(8,128)(2,1)S(1)}, bf16[2048,512]{1,0:T(8,128)(2,1)}, u32[]{:S(2)}) copy-start(bf16[2048,512]{1,0:T(8,128)(2,1)} %up_ref.1) | copy-start | bytes 6291460
  23.3 9.2 %copy-start.1 = (bf16[512,2048]{1,0:T(8,128)(2,1)S(1)}, bf16[512,2048]{1,0:T(8,128)(2,1)}, u32[]{:S(2)}) copy-start(bf16[512,2048]{1,0:T(8,128)(2,1)} %down_ref.1) | copy-start | bytes 6291460

commit v8 on v7

--- a/solution.py
+++ b/solution.py
@@ -125,7 +125,7 @@
 SHIFT = 64
 ORDERS = {
     8: (5, 7, 6, 4, 3, 1, 2, 0),
-    16: (11, 8, 13, 3, 9, 0, 15, 1, 10, 5, 6, 2, 12, 14, 7, 4),
+    16: (11, 12, 13, 5, 8, 0, 9, 15, 3, 2, 1, 7, 4, 14, 10, 6),
 }
 
 

time: 43.2 us -> 42.5 us (0.984)
  blocking collectives: 36.9 us -> 36.1 us
    all_to_all x4, blocking collectives: 36.9 us -> 36.1 us  [exchange(): lax.all_to_all(blocks, axes, 0, 0, tiled=False, axis_index_groups=[group])]
where the time goes in v8:
time: 42.5 us; the launch traced here: 42.3 us
  blocking collectives  36.1 us (85%)
  Pallas kernels  2.7 us (6%)
  starting transfers between devices  1.07 us (3%)
  waiting for transfers between devices  0.86 us (2%)
  between operations  0.82 us (2%)
  other arithmetic  0.62 us (1%)
    all_to_all x4, blocking collectives, exchange(): lax.all_to_all(blocks, axes, 0, 0, tiled=False, axis_index_groups=[group])  36.1 us
    pallas_call x1, Pallas kernels, fused(): pl.pallas_call(functools.partial(feed_kernel, gain_line=seq * heads, mode...  1.24 us
  transfers between devices with their start and end apart: 3, of which 2 were waited for; matrix products, arithmetic and copies ran while one was open for 0% of the time, Pallas kernels for 1%

profile of v8, /device:TPU:0, one launch (start us, length us, event | category | flops | bytes accessed | tf_op | source)
XLA Modules:
  0.0 42.3 jit_solution(1359696417035960501)
XLA Ops:
  0.6 0.0 copy-start.3
  0.6 0.0 copy-start.4
  0.7 0.0 copy-start.5
  0.7 0.0 copy-start.7
  0.7 0.0 copy-start.8
  0.7 0.0 copy-start.9
  0.7 0.0 copy-start.10
  0.7 0.6 %collective-permute-start.1 = (bf16[1,128]{1,0:T(2,128)(2,1)}, bf16[1,128]{1,0:T(2,128)(2,1)S(1)}, u32[]{:S(2)}, u32[]{:S(2)}) collective-permute-start(bf16[1,128]{1,0:T(2,128)(2,1)} %bitcast.15), channel_id=1, source_target_pairs={{0,1},{1,0},{2,3},{3,2},{4,5},{5,4},{6,7},{7,6},{8,9},{9,8},{10,11... | collective-permute-start | bytes 776 | tf_op jit(solution)/shard_map/ppermute | solution.py:437
  1.3 0.1 collective-permute-start
  1.3 0.4 %collective-permute-start.2 = (bf16[512,256]{1,0:T(8,128)(2,1)}, bf16[512,256]{1,0:T(8,128)(2,1)S(1)}, u32[]{:S(2)}, u32[]{:S(2)}) collective-permute-start(bf16[512,256]{1,0:T(8,128)(2,1)} %own_ref.3), channel_id=1, source_target_pairs={{0,1},{1,0},{2,3},{3,2},{4,5},{5,4},{6,7},{7,6},{8,9},{9,8},{10,11... | collective-permute-start | bytes 786440 | tf_op jit(solution)/shard_map/ppermute | solution.py:439
  1.8 0.4 %collective-permute-done.1.other_gain_ref = bf16[1,128]{1,0:T(2,128)(2,1)S(1)} collective-permute-done((bf16[1,128]{1,0:T(2,128)(2,1)}, bf16[1,128]{1,0:T(2,128)(2,1)S(1)}, u32[]{:S(2)}, u32[]{:S(2)}) %collective-permute-start.1) | collective-permute-done | bytes 288 | tf_op jit(solution)/shard_map/ppermute | solution.py:437
  2.2 0.4 %collective-permute-done.other_ref.other_tokens_ref = bf16[24,128]{1,0:T(8,128)(2,1)S(1)} collective-permute-done((bf16[24,128]{1,0:T(8,128)(2,1)}, bf16[24,128]{1,0:T(8,128)(2,1)S(1)}, u32[]{:S(2)}, u32[]{:S(2)}) %collective-permute-start) | collective-permute-done | bytes 6176 | tf_op jit(solution)/shard_map/ppermute | solution.py:436
  2.6 0.0 copy-done.3
  2.6 0.0 copy-done.4
  2.6 0.0 copy-done.5
  2.7 0.0 copy-done.7
  2.7 0.0 copy-done.8
  2.7 0.0 copy-done.9
  2.7 0.0 copy-done.10
  2.7 0.0 copy-start.2
  2.7 0.0 copy-start.11
  2.7 0.0 copy-start.12
  2.7 0.0 copy-start.13
  2.7 0.5 %project.1 = bf16[320,128]{1,0:T(8,128)(2,1)S(1)} custom-call(bf16[128,8]{1,0:T(8,128)(2,1)S(1)} %place.1.place_ref, bf16[24,128]{1,0:T(8,128)(2,1)S(1)} %copy-done.7, bf16[1,128]{1,0:T(2,128)(2,1)S(1)} %bitcast.16, bf16[24,128]{1,0:T(8,128)(2,1)S(1)} %collective-permute-done.other_ref.other_tokens_ref, ...), custom_call_target="tpu_custom_call" | custom-call | flops 4000000000 | bytes 8000000 | tf_op jit(solution)/shard_map/project/pallas_call | solution.py:449
  3.2 0.0 collective-permute-done.2.other_ref
  3.2 11.1 %all_to_all.20 = bf16[8,40,128]{2,1,0:T(8,128)(2,1)S(1)} all-to-all(bf16[8,40,128]{2,1,0:T(8,128)(2,1)S(1)} %bitcast.11), channel_id=1, replica_groups={{10,14,12,8,6,2,4,0},{11,15,13,9,7,3,5,1},{26,30,28,24,22,18,20,16},{27..., dimensions={0} | all-to-all | bytes 163840 | tf_op jit(solution)/shard_map/all_to_all | solution.py:141
  14.3 0.0 copy-done.2
  14.3 0.0 copy-done.11
  14.3 0.0 copy-done.12
  14.3 0.0 copy-done.13
  14.3 0.0 copy-start.6
  14.4 0.8 %delta.1 = (bf16[16,16,128]{2,1,0:T(8,128)(2,1)S(1)}, f32[3,4,128,128]{3,2,1,0:T(8,128)S(1)}) custom-call(bf16[320,128]{1,0:T(8,128)(2,1)S(1)} %bitcast.12, f32[3,4,128,128]{3,2,1,0:T(8,128)S(1)} %copy-done.2, f32[1,4]{1,0:T(1,128)S(1)} %bitcast.17, bf16[1,128]{1,0:T(2,128)(2,1)S(1)} %bitcast.18, bf16[1,128]{1,0:T(2,128)(2,1)S(1)} %bitcast.19), custom_call_target="tpu_custom_call" | custom-call | flops 4000000000 | bytes 8000000 | tf_op jit(solution)/shard_map/delta/pallas_call | solution.py:475
  15.1 7.9 %all_to_all.21 = bf16[16,16,128]{2,1,0:T(8,128)(2,1)S(1)} all-to-all(bf16[16,16,128]{2,1,0:T(8,128)(2,1)S(1)} %get-tuple-element.11), channel_id=1, replica_groups={{11,12,13,5,8,0,9,15,3,2,1,7,4,14,10,6},{27,28,29,21,24,16,25,31,19,18,..., dimensions={0} | all-to-all | bytes 131072 | tf_op jit(solution)/shard_map/all_to_all | solution.py:141
  23.0 0.0 copy-done.6
  23.0 0.0 copy-start
  23.1 0.0 copy-start.1
  23.1 0.2 mix.1
  23.3 9.0 %all_to_all.22.got_ref = bf16[8,24,256]{2,1,0:T(8,128)(2,1)S(1)} all-to-all(bf16[8,24,256]{2,1,0:T(8,128)(2,1)S(1)} %get-tuple-element.14), channel_id=1, replica_groups={{10,14,12,8,6,2,4,0},{11,15,13,9,7,3,5,1},{26,30,28,24,22,18,20,16},{27..., dimensions={0} | all-to-all | bytes 196608 | tf_op jit(solution)/shard_map/all_to_all | solution.py:141
  32.3 0.0 copy-done
  32.3 0.0 copy-done.1
  32.3 1.2 %feed.1 = (bf16[16,24,128]{2,1,0:T(8,128)(2,1)S(1)}, f32[3,4,128,128]{3,2,1,0:T(8,128)}) custom-call(bf16[8,24,256]{2,1,0:T(8,128)(2,1)S(1)} %all_to_all.22.got_ref, bf16[256,128]{1,0:T(8,128)(2,1)S(1)} %bitcast.10, bf16[2048,512]{1,0:T(8,128)(2,1)S(1)} %copy-done, bf16[512,2048]{1,0:T(8,128)(2,1)S(1)} %copy-done.1, ...), custom_call_target="tpu_custom_call" | custom-call | tf_op jit(solution)/shard_map/feed/pallas_call | solution.py:499
  33.5 8.1 %all_to_all.23 = bf16[16,24,128]{2,1,0:T(8,128)(2,1)S(1)} all-to-all(bf16[16,24,128]{2,1,0:T(8,128)(2,1)S(1)} %get-tuple-element.16), channel_id=1, replica_groups={{11,12,13,5,8,0,9,15,3,2,1,7,4,14,10,6},{27,28,29,21,24,16,25,31,19,18,..., dimensions={0} | all-to-all | bytes 196608 | tf_op jit(solution)/shard_map/all_to_all | solution.py:141
  41.7 0.6 %add_convert_fusion = bf16[24,128]{1,0:T(8,128)(2,1)} fusion(f32[24,128]{1,0:T(8,128)S(1)} %convert_reduce_fusion, bf16[24,128]{1,0:T(8,128)(2,1)S(1)} %get-tuple-element.13), kind=kLoop, calls=%fused_computation.1 | loop fusion | flops 9216 | bytes 24576 | tf_op jit(solution)/shard_map/convert_element_type | solution.py:509
  (2 shorter events, 0.0 us)
Async XLA Ops:
  0.6 2.0 %copy-start.3 = (bf16[256,512]{1,0:T(8,128)(2,1)S(1)}, bf16[256,512]{1,0:T(8,128)(2,1)}, u32[]{:S(2)}) copy-start(bf16[256,512]{1,0:T(8,128)(2,1)} %wq_ref.1) | copy-start | bytes 786436
  0.6 2.0 %copy-start.4 = (bf16[256,512]{1,0:T(8,128)(2,1)S(1)}, bf16[256,512]{1,0:T(8,128)(2,1)}, u32[]{:S(2)}) copy-start(bf16[256,512]{1,0:T(8,128)(2,1)} %wk_ref.1) | copy-start | bytes 786436
  0.7 2.0 %copy-start.5 = (bf16[256,512]{1,0:T(8,128)(2,1)S(1)}, bf16[256,512]{1,0:T(8,128)(2,1)}, u32[]{:S(2)}) copy-start(bf16[256,512]{1,0:T(8,128)(2,1)} %wv_ref.1) | copy-start | bytes 786436
  0.7 2.0 %copy-start.7 = (bf16[24,128]{1,0:T(8,128)(2,1)S(1)}, bf16[24,128]{1,0:T(8,128)(2,1)}, u32[]{:S(2)}) copy-start(bf16[24,128]{1,0:T(8,128)(2,1)} %tokens_ref.1) | copy-start | bytes 18436
  0.7 2.0 %copy-start.8 = (bf16[256,4]{0,1:T(4,128)(2,1)S(1)}, bf16[256,4]{0,1:T(4,128)(2,1)}, u32[]{:S(2)}) copy-start(bf16[256,4]{0,1:T(4,128)(2,1)} %param.20) | copy-start | bytes 6148
  0.7 2.0 %copy-start.9 = (bf16[256,4]{0,1:T(4,128)(2,1)S(1)}, bf16[256,4]{0,1:T(4,128)(2,1)}, u32[]{:S(2)}) copy-start(bf16[256,4]{0,1:T(4,128)(2,1)} %param.21) | copy-start | bytes 6148
  0.7 2.0 %copy-start.10 = (bf16[128]{0:T(256)(128)(2,1)S(1)}, bf16[128]{0:T(256)(128)(2,1)}, u32[]{:S(2)}) copy-start(bf16[128]{0:T(256)(128)(2,1)} %param.16) | copy-start | bytes 772
  0.7 1.5 %collective-permute-start.1 = (bf16[1,128]{1,0:T(2,128)(2,1)}, bf16[1,128]{1,0:T(2,128)(2,1)S(1)}, u32[]{:S(2)}, u32[]{:S(2)}) collective-permute-start(bf16[1,128]{1,0:T(2,128)(2,1)} %bitcast.15), channel_id=1, source_target_pairs={{0,1},{1,0},{2,3},{3,2},{4,5},{5,4},{6,7},{7,6},{8,9},{9,8},{10,11... | collective-permute-start | bytes 776 | tf_op jit(solution)/shard_map/ppermute | solution.py:437
  1.3 1.4 %collective-permute-start = (bf16[24,128]{1,0:T(8,128)(2,1)}, bf16[24,128]{1,0:T(8,128)(2,1)S(1)}, u32[]{:S(2)}, u32[]{:S(2)}) collective-permute-start(bf16[24,128]{1,0:T(8,128)(2,1)} %tokens_ref.1), channel_id=1, source_target_pairs={{0,1},{1,0},{2,3},{3,2},{4,5},{5,4},{6,7},{7,6},{8,9},{9,8},{10,11... | collective-permute-start | bytes 18440 | tf_op jit(solution)/shard_map/ppermute | solution.py:436
  1.3 1.9 %collective-permute-start.2 = (bf16[512,256]{1,0:T(8,128)(2,1)}, bf16[512,256]{1,0:T(8,128)(2,1)S(1)}, u32[]{:S(2)}, u32[]{:S(2)}) collective-permute-start(bf16[512,256]{1,0:T(8,128)(2,1)} %own_ref.3), channel_id=1, source_target_pairs={{0,1},{1,0},{2,3},{3,2},{4,5},{5,4},{6,7},{7,6},{8,9},{9,8},{10,11... | collective-permute-start | bytes 786440 | tf_op jit(solution)/shard_map/ppermute | solution.py:439
  2.7 11.6 %copy-start.2 = (f32[3,4,128,128]{3,2,1,0:T(8,128)S(1)}, f32[3,4,128,128]{3,2,1,0:T(8,128)}, u32[]{:S(2)}) copy-start(f32[3,4,128,128]{3,2,1,0:T(8,128)} %state_ref.1) | copy-start | bytes 2359300
  2.7 11.6 %copy-start.11 = (f32[4]{0:T(128)S(1)}, f32[4]{0:T(128)}, u32[]{:S(2)}) copy-start(f32[4]{0:T(128)} %param.22) | copy-start | bytes 52
  2.7 11.6 %copy-start.12 = (bf16[128]{0:T(256)(128)(2,1)S(1)}, bf16[128]{0:T(256)(128)(2,1)}, u32[]{:S(2)}) copy-start(bf16[128]{0:T(256)(128)(2,1)} %param.23) | copy-start | bytes 772
  2.7 11.6 %copy-start.13 = (bf16[128]{0:T(256)(128)(2,1)S(1)}, bf16[128]{0:T(256)(128)(2,1)}, u32[]{:S(2)}) copy-start(bf16[128]{0:T(256)(128)(2,1)} %param.25) | copy-start | bytes 772
  14.3 8.7 %copy-start.6 = (bf16[512,256]{1,0:T(8,128)(2,1)S(1)}, bf16[512,256]{1,0:T(8,128)(2,1)}, u32[]{:S(2)}) copy-start(bf16[512,256]{1,0:T(8,128)(2,1)} %own_ref.3) | copy-start | bytes 786436
  23.0 9.2 %copy-start = (bf16[2048,512]{1,0:T(8,128)(2,1)S(1)}, bf16[2048,512]{1,0:T(8,128)(2,1)}, u32[]{:S(2)}) copy-start(bf16[2048,512]{1,0:T(8,128)(2,1)} %up_ref.1) | copy-start | bytes 6291460
  23.1 9.2 %copy-start.1 = (bf16[512,2048]{1,0:T(8,128)(2,1)S(1)}, bf16[512,2048]{1,0:T(8,128)(2,1)}, u32[]{:S(2)}) copy-start(bf16[512,2048]{1,0:T(8,128)(2,1)} %down_ref.1) | copy-start | bytes 6291460

commit v9 on v8

--- a/solution.py
+++ b/solution.py
@@ -470,8 +470,8 @@
         w_beta.T,
         w_decay.T,
     )
-    sent, other_out = lax.optimization_barrier((sent, other_out))
     got = exchange(sent.reshape(n_kv, packet, LANES), "kv", True)
+    got, other_out = lax.optimization_barrier((got, other_out))
     spread, new_state = pl.pallas_call(
         functools.partial(delta_kernel, n_kv=n_kv, seq=seq, heads=heads, model=model),
         out_shape=(shape((n_all, lines, LANES), BF), shape(state.shape, F32)),

time: 42.5 us -> 42.4 us (level)
  no operation moved by 1% of the time
where the time goes in v9:
time: 42.4 us; the launch traced here: 42.1 us
  blocking collectives  36 us (85%)
  Pallas kernels  2.69 us (6%)
  starting transfers between devices  1.07 us (3%)
  waiting for transfers between devices  0.86 us (2%)
  between operations  0.82 us (2%)
  other arithmetic  0.62 us (1%)
    all_to_all x4, blocking collectives, exchange(): lax.all_to_all(blocks, axes, 0, 0, tiled=False, axis_index_groups=[group])  36 us
    pallas_call x1, Pallas kernels, fused(): pl.pallas_call(functools.partial(feed_kernel, gain_line=seq * heads, mode...  1.23 us
  transfers between devices with their start and end apart: 3, of which 2 were waited for; matrix products, arithmetic and copies ran while one was open for 0% of the time, Pallas kernels for 1%

profile of v9, /device:TPU:0, one launch (start us, length us, event | category | flops | bytes accessed | tf_op | source)
XLA Modules:
  0.0 42.1 jit_solution(15164368969237022847)
XLA Ops:
  0.6 0.0 copy-start.3
  0.6 0.0 copy-start.4
  0.7 0.0 copy-start.5
  0.7 0.0 copy-start.7
  0.7 0.0 copy-start.8
  0.7 0.0 copy-start.9
  0.7 0.0 copy-start.10
  0.7 0.6 %collective-permute-start.1 = (bf16[1,128]{1,0:T(2,128)(2,1)}, bf16[1,128]{1,0:T(2,128)(2,1)S(1)}, u32[]{:S(2)}, u32[]{:S(2)}) collective-permute-start(bf16[1,128]{1,0:T(2,128)(2,1)} %bitcast.15), channel_id=1, source_target_pairs={{0,1},{1,0},{2,3},{3,2},{4,5},{5,4},{6,7},{7,6},{8,9},{9,8},{10,11... | collective-permute-start | bytes 776 | tf_op jit(solution)/shard_map/ppermute | solution.py:437
  1.3 0.1 collective-permute-start
  1.3 0.4 %collective-permute-start.2 = (bf16[512,256]{1,0:T(8,128)(2,1)}, bf16[512,256]{1,0:T(8,128)(2,1)S(1)}, u32[]{:S(2)}, u32[]{:S(2)}) collective-permute-start(bf16[512,256]{1,0:T(8,128)(2,1)} %own_ref.3), channel_id=1, source_target_pairs={{0,1},{1,0},{2,3},{3,2},{4,5},{5,4},{6,7},{7,6},{8,9},{9,8},{10,11... | collective-permute-start | bytes 786440 | tf_op jit(solution)/shard_map/ppermute | solution.py:439
  1.8 0.4 %collective-permute-done.1.other_gain_ref = bf16[1,128]{1,0:T(2,128)(2,1)S(1)} collective-permute-done((bf16[1,128]{1,0:T(2,128)(2,1)}, bf16[1,128]{1,0:T(2,128)(2,1)S(1)}, u32[]{:S(2)}, u32[]{:S(2)}) %collective-permute-start.1) | collective-permute-done | bytes 288 | tf_op jit(solution)/shard_map/ppermute | solution.py:437
  2.2 0.4 %collective-permute-done.other_ref.other_tokens_ref = bf16[24,128]{1,0:T(8,128)(2,1)S(1)} collective-permute-done((bf16[24,128]{1,0:T(8,128)(2,1)}, bf16[24,128]{1,0:T(8,128)(2,1)S(1)}, u32[]{:S(2)}, u32[]{:S(2)}) %collective-permute-start) | collective-permute-done | bytes 6176 | tf_op jit(solution)/shard_map/ppermute | solution.py:436
  2.6 0.0 copy-done.3
  2.6 0.0 copy-done.4
  2.6 0.0 copy-done.5
  2.7 0.0 copy-done.7
  2.7 0.0 copy-done.8
  2.7 0.0 copy-done.9
  2.7 0.0 copy-done.10
  2.7 0.0 copy-start.2
  2.7 0.0 copy-start.11
  2.7 0.0 copy-start.12
  2.7 0.0 copy-start.13
  2.7 0.5 %project.1 = bf16[320,128]{1,0:T(8,128)(2,1)S(1)} custom-call(bf16[128,8]{1,0:T(8,128)(2,1)S(1)} %place.1.place_ref, bf16[24,128]{1,0:T(8,128)(2,1)S(1)} %copy-done.7, bf16[1,128]{1,0:T(2,128)(2,1)S(1)} %bitcast.16, bf16[24,128]{1,0:T(8,128)(2,1)S(1)} %collective-permute-done.other_ref.other_tokens_ref, ...), custom_call_target="tpu_custom_call" | custom-call | flops 4000000000 | bytes 8000000 | tf_op jit(solution)/shard_map/project/pallas_call | solution.py:449
  3.2 11.0 %all_to_all.20 = bf16[8,40,128]{2,1,0:T(8,128)(2,1)S(1)} all-to-all(bf16[8,40,128]{2,1,0:T(8,128)(2,1)S(1)} %bitcast.12), channel_id=1, replica_groups={{10,14,12,8,6,2,4,0},{11,15,13,9,7,3,5,1},{26,30,28,24,22,18,20,16},{27..., dimensions={0} | all-to-all | bytes 163840 | tf_op jit(solution)/shard_map/all_to_all | solution.py:141
  14.2 0.0 collective-permute-done.2.other_ref
  14.2 0.0 copy-done.2
  14.2 0.0 copy-done.11
  14.2 0.0 copy-done.12
  14.2 0.0 copy-done.13
  14.2 0.0 copy-start.6
  14.2 0.8 %delta.1 = (bf16[16,16,128]{2,1,0:T(8,128)(2,1)S(1)}, f32[3,4,128,128]{3,2,1,0:T(8,128)S(1)}) custom-call(bf16[320,128]{1,0:T(8,128)(2,1)S(1)} %bitcast.11, f32[3,4,128,128]{3,2,1,0:T(8,128)S(1)} %copy-done.2, f32[1,4]{1,0:T(1,128)S(1)} %bitcast.17, bf16[1,128]{1,0:T(2,128)(2,1)S(1)} %bitcast.18, bf16[1,128]{1,0:T(2,128)(2,1)S(1)} %bitcast.19), custom_call_target="tpu_custom_call" | custom-call | flops 4000000000 | bytes 8000000 | tf_op jit(solution)/shard_map/delta/pallas_call | solution.py:475
  15.0 7.9 %all_to_all.21 = bf16[16,16,128]{2,1,0:T(8,128)(2,1)S(1)} all-to-all(bf16[16,16,128]{2,1,0:T(8,128)(2,1)S(1)} %get-tuple-element.11), channel_id=1, replica_groups={{11,12,13,5,8,0,9,15,3,2,1,7,4,14,10,6},{27,28,29,21,24,16,25,31,19,18,..., dimensions={0} | all-to-all | bytes 131072 | tf_op jit(solution)/shard_map/all_to_all | solution.py:141
  22.9 0.0 copy-done.6
  22.9 0.0 copy-start
  22.9 0.0 copy-start.1
  22.9 0.2 mix.1
  23.2 9.0 %all_to_all.22.got_ref = bf16[8,24,256]{2,1,0:T(8,128)(2,1)S(1)} all-to-all(bf16[8,24,256]{2,1,0:T(8,128)(2,1)S(1)} %get-tuple-element.14), channel_id=1, replica_groups={{10,14,12,8,6,2,4,0},{11,15,13,9,7,3,5,1},{26,30,28,24,22,18,20,16},{27..., dimensions={0} | all-to-all | bytes 196608 | tf_op jit(solution)/shard_map/all_to_all | solution.py:141
  32.2 0.0 copy-done
  32.2 0.0 copy-done.1
  32.2 1.2 %feed.1 = (bf16[16,24,128]{2,1,0:T(8,128)(2,1)S(1)}, f32[3,4,128,128]{3,2,1,0:T(8,128)}) custom-call(bf16[8,24,256]{2,1,0:T(8,128)(2,1)S(1)} %all_to_all.22.got_ref, bf16[256,128]{1,0:T(8,128)(2,1)S(1)} %bitcast.10, bf16[2048,512]{1,0:T(8,128)(2,1)S(1)} %copy-done, bf16[512,2048]{1,0:T(8,128)(2,1)S(1)} %copy-done.1, ...), custom_call_target="tpu_custom_call" | custom-call | tf_op jit(solution)/shard_map/feed/pallas_call | solution.py:499
  33.4 8.1 %all_to_all.23 = bf16[16,24,128]{2,1,0:T(8,128)(2,1)S(1)} all-to-all(bf16[16,24,128]{2,1,0:T(8,128)(2,1)S(1)} %get-tuple-element.16), channel_id=1, replica_groups={{11,12,13,5,8,0,9,15,3,2,1,7,4,14,10,6},{27,28,29,21,24,16,25,31,19,18,..., dimensions={0} | all-to-all | bytes 196608 | tf_op jit(solution)/shard_map/all_to_all | solution.py:141
  41.5 0.6 %add_convert_fusion = bf16[24,128]{1,0:T(8,128)(2,1)} fusion(f32[24,128]{1,0:T(8,128)S(1)} %convert_reduce_fusion, bf16[24,128]{1,0:T(8,128)(2,1)S(1)} %get-tuple-element.13), kind=kLoop, calls=%fused_computation.1 | loop fusion | flops 9216 | bytes 24576 | tf_op jit(solution)/shard_map/convert_element_type | solution.py:509
  (2 shorter events, 0.0 us)
Async XLA Ops:
  0.6 2.0 %copy-start.3 = (bf16[256,512]{1,0:T(8,128)(2,1)S(1)}, bf16[256,512]{1,0:T(8,128)(2,1)}, u32[]{:S(2)}) copy-start(bf16[256,512]{1,0:T(8,128)(2,1)} %wq_ref.1) | copy-start | bytes 786436
  0.6 2.0 %copy-start.4 = (bf16[256,512]{1,0:T(8,128)(2,1)S(1)}, bf16[256,512]{1,0:T(8,128)(2,1)}, u32[]{:S(2)}) copy-start(bf16[256,512]{1,0:T(8,128)(2,1)} %wk_ref.1) | copy-start | bytes 786436
  0.7 2.0 %copy-start.5 = (bf16[256,512]{1,0:T(8,128)(2,1)S(1)}, bf16[256,512]{1,0:T(8,128)(2,1)}, u32[]{:S(2)}) copy-start(bf16[256,512]{1,0:T(8,128)(2,1)} %wv_ref.1) | copy-start | bytes 786436
  0.7 2.0 %copy-start.7 = (bf16[24,128]{1,0:T(8,128)(2,1)S(1)}, bf16[24,128]{1,0:T(8,128)(2,1)}, u32[]{:S(2)}) copy-start(bf16[24,128]{1,0:T(8,128)(2,1)} %tokens_ref.1) | copy-start | bytes 18436
  0.7 2.0 %copy-start.8 = (bf16[256,4]{0,1:T(4,128)(2,1)S(1)}, bf16[256,4]{0,1:T(4,128)(2,1)}, u32[]{:S(2)}) copy-start(bf16[256,4]{0,1:T(4,128)(2,1)} %param.20) | copy-start | bytes 6148
  0.7 2.0 %copy-start.9 = (bf16[256,4]{0,1:T(4,128)(2,1)S(1)}, bf16[256,4]{0,1:T(4,128)(2,1)}, u32[]{:S(2)}) copy-start(bf16[256,4]{0,1:T(4,128)(2,1)} %param.21) | copy-start | bytes 6148
  0.7 2.0 %copy-start.10 = (bf16[128]{0:T(256)(128)(2,1)S(1)}, bf16[128]{0:T(256)(128)(2,1)}, u32[]{:S(2)}) copy-start(bf16[128]{0:T(256)(128)(2,1)} %param.16) | copy-start | bytes 772
  0.7 1.5 %collective-permute-start.1 = (bf16[1,128]{1,0:T(2,128)(2,1)}, bf16[1,128]{1,0:T(2,128)(2,1)S(1)}, u32[]{:S(2)}, u32[]{:S(2)}) collective-permute-start(bf16[1,128]{1,0:T(2,128)(2,1)} %bitcast.15), channel_id=1, source_target_pairs={{0,1},{1,0},{2,3},{3,2},{4,5},{5,4},{6,7},{7,6},{8,9},{9,8},{10,11... | collective-permute-start | bytes 776 | tf_op jit(solution)/shard_map/ppermute | solution.py:437
  1.3 1.4 %collective-permute-start = (bf16[24,128]{1,0:T(8,128)(2,1)}, bf16[24,128]{1,0:T(8,128)(2,1)S(1)}, u32[]{:S(2)}, u32[]{:S(2)}) collective-permute-start(bf16[24,128]{1,0:T(8,128)(2,1)} %tokens_ref.1), channel_id=1, source_target_pairs={{0,1},{1,0},{2,3},{3,2},{4,5},{5,4},{6,7},{7,6},{8,9},{9,8},{10,11... | collective-permute-start | bytes 18440 | tf_op jit(solution)/shard_map/ppermute | solution.py:436
  1.3 12.9 %collective-permute-start.2 = (bf16[512,256]{1,0:T(8,128)(2,1)}, bf16[512,256]{1,0:T(8,128)(2,1)S(1)}, u32[]{:S(2)}, u32[]{:S(2)}) collective-permute-start(bf16[512,256]{1,0:T(8,128)(2,1)} %own_ref.3), channel_id=1, source_target_pairs={{0,1},{1,0},{2,3},{3,2},{4,5},{5,4},{6,7},{7,6},{8,9},{9,8},{10,11... | collective-permute-start | bytes 786440 | tf_op jit(solution)/shard_map/ppermute | solution.py:439
  2.7 11.5 %copy-start.2 = (f32[3,4,128,128]{3,2,1,0:T(8,128)S(1)}, f32[3,4,128,128]{3,2,1,0:T(8,128)}, u32[]{:S(2)}) copy-start(f32[3,4,128,128]{3,2,1,0:T(8,128)} %state_ref.1) | copy-start | bytes 2359300
  2.7 11.5 %copy-start.11 = (f32[4]{0:T(128)S(1)}, f32[4]{0:T(128)}, u32[]{:S(2)}) copy-start(f32[4]{0:T(128)} %param.22) | copy-start | bytes 52
  2.7 11.5 %copy-start.12 = (bf16[128]{0:T(256)(128)(2,1)S(1)}, bf16[128]{0:T(256)(128)(2,1)}, u32[]{:S(2)}) copy-start(bf16[128]{0:T(256)(128)(2,1)} %param.23) | copy-start | bytes 772
  2.7 11.5 %copy-start.13 = (bf16[128]{0:T(256)(128)(2,1)S(1)}, bf16[128]{0:T(256)(128)(2,1)}, u32[]{:S(2)}) copy-start(bf16[128]{0:T(256)(128)(2,1)} %param.25) | copy-start | bytes 772
  14.2 8.7 %copy-start.6 = (bf16[512,256]{1,0:T(8,128)(2,1)S(1)}, bf16[512,256]{1,0:T(8,128)(2,1)}, u32[]{:S(2)}) copy-start(bf16[512,256]{1,0:T(8,128)(2,1)} %own_ref.3) | copy-start | bytes 786436
  22.9 9.2 %copy-start = (bf16[2048,512]{1,0:T(8,128)(2,1)S(1)}, bf16[2048,512]{1,0:T(8,128)(2,1)}, u32[]{:S(2)}) copy-start(bf16[2048,512]{1,0:T(8,128)(2,1)} %up_ref.1) | copy-start | bytes 6291460
  22.9 9.2 %copy-start.1 = (bf16[512,2048]{1,0:T(8,128)(2,1)S(1)}, bf16[512,2048]{1,0:T(8,128)(2,1)}, u32[]{:S(2)}) copy-start(bf16[512,2048]{1,0:T(8,128)(2,1)} %down_ref.1) | copy-start | bytes 6291460
